TPU v7x, 128 devices: a whole 4x4x4 slice. The times are simulated.
128 devices in a mesh: sp: 64 (over z, y, x), tp: 2 (over core).
Axes of the slice: x: 4, y: 4, z: 4, core: 2. Of those that a mesh axis runs over, the one named last changes fastest.
Arguments:
- stream: bfloat16 [16384, 2048], P('sp', 'tp'), may hold values from -80 to 80
- norm_gain: float32 [2048], P('tp'), may hold values from 0.1 to 1.9
- cotangent: bfloat16 [16384, 2048], P('sp', 'tp'), may hold values from -16 to 16
- route_weights: float32 [16384, 2], P('sp'), may hold values from 0.1 to 1.5
- routes: int32 [16384, 2], P('sp'), may hold values from 0 to 63, all different within a row; in each aligned block of 256 rows (0 to 255, 256 to 511, ...) at most 16 rows name the same one
- conv_input: bfloat16 [16384, 1024], P('sp', 'tp'), may hold values from -6 to 6
- conv_bgate: bfloat16 [16384, 1024], P('sp', 'tp'), may hold values from -6 to 6
- conv_cgate: bfloat16 [16384, 1024], P('sp', 'tp'), may hold values from -6 to 6
- conv_taps: float32 [3, 1024], P(None, 'tp'), may hold values from -3 to 3
- out_proj: bfloat16 [2048, 1024], P(None, 'tp'), may hold values from -0.1875 to 0.1875
- gate_weight: bfloat16 [64, 2048, 1024], P('sp', None, 'tp'), may hold values from -0.125 to 0.125
- up_weight: bfloat16 [64, 2048, 1024], P('sp', None, 'tp'), may hold values from -0.125 to 0.125
- down_weight: bfloat16 [64, 1024, 2048], P('sp', 'tp'), may hold values from -0.1875 to 0.1875
Outputs:
- stream_grad: bfloat16 [16384, 2048], P('sp', 'tp')
- proj_grad: float32 [2048, 1024], P('sp', 'tp')
- input_grad: bfloat16 [16384, 1024], P('sp', 'tp')
- bgate_grad: bfloat16 [16384, 1024], P('sp', 'tp')
- cgate_grad: bfloat16 [16384, 1024], P('sp', 'tp')
- gate_grad: float32 [64, 2048, 1024], P('sp', None, 'tp')
- up_grad: float32 [64, 2048, 1024], P('sp', None, 'tp')
- down_grad: float32 [64, 1024, 2048], P('sp', 'tp')
Inputs may be any that keep to these rules, and one draw needn't show every extreme that they name: `routes`: the 2 experts of a token differ. Among the tokens of one index of sp, no expert is named more than 16 times, a bound that some block reaches.
All inputs are finite; a program needn't handle non-finite values.
Results may differ from a plain program's by a relative error of at most 0.003.
The roundings to bfloat16 on the way count: a program that leaves them out, or rounds other values in their place, can miss the bound.
Values may be sent and summed in bfloat16 or wider, within the bound.
No kernel may reach another device: no remote copies, remote signals or barrier semaphores. Data moves between devices by JAX's collectives and lax.ppermute only.
A program may use at most 128 MiB of HBM per device.

v0:
```python
import jax
import jax.numpy as jnp
from jax import lax
from jax.sharding import Mesh
from jax.sharding import PartitionSpec as P

D = 2048
SP = ("sp_0", "sp_1", "sp_2")


EPSILON = 1e-06


def gathered_total(array, axis):
    return lax.all_gather(array, axis).sum(0)


def side_by_side(arrays, axis, split_dim, concat_dim, along):
    both = jnp.concatenate(arrays, axis=along)
    whole, at, outs = (
        lax.all_to_all(both, axis, split_axis=split_dim, concat_axis=concat_dim, tiled=True),
        0,
        [],
    )
    for a in arrays:
        outs.append(lax.slice_in_dim(whole, at, at + a.shape[along], axis=along))
        at += a.shape[along]
    return tuple(outs)


def sent_together(arrays, axis, dim, along):
    ends, at = ([], 0)
    for a in arrays[:-1]:
        at += a.shape[along]
        ends.append(at)
    both = jnp.concatenate(arrays, axis=along)
    return tuple(jnp.split(lax.all_gather(both, axis, axis=dim, tiled=True), ends, axis=along))


def in_blocks(array, dim, length):
    dims = array.shape
    parts = array.reshape(*dims[:dim], length, dims[dim] // length, *dims[dim + 1 :])
    return jnp.moveaxis(parts, dim, 0)


def sent_and_summed(array, axis, dim):
    parts = in_blocks(array, dim, lax.axis_size(axis))
    arrived = lax.all_to_all(parts, axis, split_axis=0, concat_axis=0, tiled=True)
    return arrived.astype(jnp.float32).sum(axis=0)


def joined_along(parts, dim):
    dims = list(parts.shape[1:])
    dims[dim] *= parts.shape[0]
    return jnp.moveaxis(parts, 0, dim).reshape(dims)


def from_everyone(array, axis):
    copies = jnp.broadcast_to(array, (lax.axis_size(axis), *array.shape))
    return lax.all_to_all(copies, axis, split_axis=0, concat_axis=0, tiled=True)


def gathered_copies(array, axis, dim):
    return joined_along(from_everyone(array, axis), dim)


def shifted(value, axis, steps):
    count = lax.axis_size(axis)
    leading, last = (max(0, -steps), min(count, count - steps))
    return lax.ppermute(value, axis, [(source, source + steps) for source in range(leading, last)])


def sum_by_axis(subtotal, axes):
    for axis in axes:
        subtotal = lax.psum_scatter(subtotal, axis, scatter_dimension=0, tiled=True)
    return subtotal


def slot_matrix(routes, experts, capacity):
    assigned = routes.reshape(-1)
    onehot = (assigned[:, None] == jnp.arange(experts, dtype=jnp.int32)[None, :]).astype(jnp.int32)
    earlier = jnp.cumsum(onehot, axis=0) - onehot
    position = jnp.sum(earlier * onehot, axis=1)
    target = assigned * capacity + position
    places = jnp.arange(experts * capacity, dtype=jnp.int32)
    return (places[:, None] == target[None, :]).astype(jnp.bfloat16)


def select_rows(selector, values):
    return jnp.dot(selector, values, preferred_element_type=jnp.float32).astype(jnp.bfloat16)


def contract_rows(left, right):
    return lax.dot_general(
        left, right, (((0,), (0,)), ((), ())), preferred_element_type=jnp.float32
    )


def contract_cols(left, right):
    return lax.dot_general(
        left, right, (((1,), (1,)), ((), ())), preferred_element_type=jnp.float32
    )


def local(
    stream,
    norm_gain,
    cotangent,
    route_weights,
    routes,
    conv_input,
    conv_bgate,
    conv_cgate,
    conv_taps,
    out_proj,
    gate_weight,
    up_weight,
    down_weight,
):
    experts = lax.axis_size(SP)
    tok_count = stream.shape[0]
    top_count = routes.shape[1]
    capacity = 2 * tok_count * top_count // experts
    stream_float = stream.astype(jnp.float32)
    square_sum = gathered_total(jnp.sum(stream_float * stream_float, axis=1), "tp")
    inverse = lax.rsqrt(square_sum / D + EPSILON)[:, None]
    gain_row = norm_gain[None, :]
    normed = (stream_float * inverse * gain_row).astype(jnp.bfloat16)
    cot_float = cotangent.astype(jnp.float32)
    weighted = (route_weights[:, :, None] * cot_float[:, None, :]).astype(jnp.bfloat16)
    weighted = weighted.reshape(tok_count * top_count, -1)
    selector = slot_matrix(routes, experts, capacity)
    token_select = jnp.sum(selector.reshape(experts * capacity, tok_count, top_count), axis=2)
    send_inputs = select_rows(token_select, normed)
    send_grads = select_rows(selector, weighted)
    half_inputs, half_grads = side_by_side((send_inputs, send_grads), SP, 0, 0, 1)
    recv_inputs, recv_grads = sent_together((half_inputs, half_grads), "tp", 1, 0)
    gate_w = gate_weight[0]
    up_w = up_weight[0]
    down_w = down_weight[0]
    gate_lin = jnp.dot(recv_inputs, gate_w, preferred_element_type=jnp.float32)
    up_lin = jnp.dot(recv_inputs, up_w, preferred_element_type=jnp.float32)
    sigmoid_gate = jax.nn.sigmoid(gate_lin)
    silu_gate = gate_lin * sigmoid_gate
    hidden = (silu_gate * up_lin).astype(jnp.bfloat16)
    down_g = contract_rows(hidden, recv_grads)
    hidden_grad = contract_cols(recv_grads, down_w)
    gate_pre = (
        hidden_grad * up_lin * sigmoid_gate * (1.0 + gate_lin * (1.0 - sigmoid_gate))
    ).astype(jnp.bfloat16)
    up_pre = (hidden_grad * silu_gate).astype(jnp.bfloat16)
    gate_g = contract_rows(recv_inputs, gate_pre)
    up_g = contract_rows(recv_inputs, up_pre)
    partial_value = contract_cols(gate_pre, gate_w) + contract_cols(up_pre, up_w)
    rounded = lax.optimization_barrier(partial_value.astype(jnp.bfloat16))
    summed = sent_and_summed(rounded.astype(jnp.float32).astype(jnp.bfloat16), "tp", 1)
    row_grads = summed.astype(jnp.bfloat16)
    returned = lax.all_to_all(row_grads, SP, split_axis=0, concat_axis=0, tiled=True)
    normed_grad = contract_rows(token_select, returned)
    cross = gathered_total(jnp.sum(stream_float * gain_row * normed_grad, axis=1), "tp")
    stream_grad = (
        cot_float
        + inverse * gain_row * normed_grad
        - stream_float * inverse * inverse * inverse * cross[:, None] / D
    ).astype(jnp.bfloat16)
    grad_whole = gathered_copies(stream_grad, "tp", 1)
    input_float = conv_input.astype(jnp.float32)
    cgate_float = conv_cgate.astype(jnp.float32)
    bgate_float = conv_bgate.astype(jnp.float32)
    rim_rows = shifted(jnp.stack([conv_input[-2:], conv_cgate[-2:]]), SP, 1)
    rim_gated = rim_rows[1].astype(jnp.float32) * rim_rows[0].astype(jnp.float32)
    gated = cgate_float * input_float
    extended = jnp.concatenate([rim_gated, gated], axis=0)
    conv_out = (
        conv_taps[0][None, :] * extended[:-2]
        + conv_taps[1][None, :] * extended[1:-1]
        + conv_taps[2][None, :] * extended[2:]
    )
    mixer_out = (bgate_float * conv_out).astype(jnp.bfloat16)
    proj_grad = sum_by_axis(contract_rows(grad_whole, mixer_out), SP)
    mixer_grad = jnp.dot(grad_whole, out_proj, preferred_element_type=jnp.float32)
    delta = mixer_grad * bgate_float
    next_rim = shifted(delta[:2], SP, -1)
    extended_back = jnp.concatenate([delta, next_rim], axis=0)
    gated_grad = (
        conv_taps[2][None, :] * extended_back[:-2]
        + conv_taps[1][None, :] * extended_back[1:-1]
        + conv_taps[0][None, :] * extended_back[2:]
    )
    bgate_grad = (mixer_grad * conv_out).astype(jnp.bfloat16)
    input_grad = (gated_grad * cgate_float).astype(jnp.bfloat16)
    cgate_grad = (gated_grad * input_float).astype(jnp.bfloat16)
    return (
        stream_grad,
        proj_grad,
        input_grad,
        bgate_grad,
        cgate_grad,
        gate_g[None],
        up_g[None],
        down_g[None],
    )


def solution(mesh):
    finer = Mesh(mesh.devices.reshape(4, 4, 4, mesh.shape["tp"]), ("sp_0", "sp_1", "sp_2", "tp"))
    return jax.shard_map(
        local,
        mesh=finer,
        in_specs=(
            P(SP, "tp"),
            P("tp"),
            P(SP, "tp"),
            P(SP, None),
            P(SP, None),
            P(SP, "tp"),
            P(SP, "tp"),
            P(SP, "tp"),
            P(None, "tp"),
            P(None, "tp"),
            P(SP, None, "tp"),
            P(SP, None, "tp"),
            P(SP, "tp", None),
        ),
        out_specs=(
            P(SP, "tp"),
            P(SP, "tp"),
            P(SP, "tp"),
            P(SP, "tp"),
            P(SP, "tp"),
            P(SP, None, "tp"),
            P(SP, None, "tp"),
            P(SP, "tp", None),
        ),
        check_vma=False,
    )
```

profile of v0, /device:TPU:0, one launch (start us, length us, event | category | flops | bytes accessed | tf_op | source)
XLA Modules:
  0.0 303.7 jit_solution(6799366992860196564)
XLA Ops:
  10.3 2.9 mul.206
  13.2 3.7 %mul.207 = f32[512,1024]{1,0:T(8,128)} reshape(f32[256,2,1024]{2,1,0:T(2,128)} %mul.206) | data formatting | bytes 4194304 | tf_op jit(solution)/shard_map/mul | solution.py:130
  19.8 3.0 fusion.22
  23.6 2.5 pad_maximum_fusion
  26.1 6.4 %copy.54 = bf16[1024,2048]{1,0:T(8,128)(2,1)} copy(bf16[1024,2048]{0,1:T(8,128)(2,1)} %pad_maximum_fusion) | data formatting | bytes 8388608 | tf_op jit(solution)/shard_map/concatenate | solution.py:19
  32.5 64.4 %all_to_all.34 = bf16[64,16,2048]{2,1,0:T(8,128)(2,1)S(1)} all-to-all(bf16[64,16,2048]{2,1,0:T(8,128)(2,1)} %bitcast.76), channel_id=1, replica_groups=mesh['sp_0'=4,'sp_1'=4,'sp_2'=4,'tp'=2] {'sp_0','sp_1','sp_2'}, dimensions={0} | all-to-all | bytes 8388608 | tf_op jit(solution)/shard_map/all_to_all | solution.py:21
  97.4 2.5 pad_maximum_fusion.1
  99.8 19.3 %all-gather.6.cloned.1.call-done = bf16[2048,2048]{1,0:T(8,128)(2,1)} async-done(((bf16[2048,1024]{1,0:T(8,128)(2,1)}), bf16[2048,2048]{1,0:T(8,128)(2,1)}) %all-gather.6.cloned.1.call-update) | async-done | bytes 8388624 | tf_op jit(solution)/shard_map/all_gather | solution.py:37
  119.2 5.3 %fusion.11 = f32[1024,512]{1,0:T(8,128)S(1)} fusion(bf16[2048,2048]{1,0:T(8,128)(2,1)} %all-gather.6.cloned.1.call-done, bf16[1,2048,512]{2,1,0:T(8,128)(2,1)} %param.24), kind=kOutput, calls=%fused_computation.15 | convolution fusion | flops 2147483648 | bytes 8388608 | tf_op jit(solution)/shard_map/dot_general | solution.py:142
  126.9 3.0 multiply_convert_fusion.1
  135.2 8.2 %all_to_all.35 = bf16[2,1024,1024]{2,1,0:T(8,128)(2,1)} all-to-all(bf16[2,1024,1024]{2,1,0:T(8,128)(2,1)S(1)} %bitcast.77), channel_id=1, replica_groups=mesh['sp_0'=4,'sp_1'=4,'sp_2'=4,'tp'=2] {'tp'}, dimensions={0} | all-to-all | bytes 8388608 | tf_op jit(solution)/shard_map/all_to_all | solution.py:48
  143.4 5.2 %reduce_sum.76 = bf16[1024,1024]{1,0:T(8,128)(2,1)} reduce(bf16[2,1024,1024]{2,1,0:T(8,128)(2,1)} %all_to_all.35, bf16[]{:T(256)} %constant.20.clone.1), dimensions={0}, to_apply=%region_6.7 | reduce | flops 1048576 | bytes 6291458 | tf_op jit(solution)/shard_map/reduce_sum | solution.py:49
  148.6 10.6 %all-to-all-start.2 = ((bf16[64,16,1024]{2,1,0:T(8,128)(2,1)}), bf16[64,16,1024]{2,1,0:T(8,128)(2,1)S(1)}, u32[]{:S(2)}, u32[]{:S(2)}) async-start(bf16[64,16,1024]{2,1,0:T(8,128)(2,1)} %bitcast.8), calls=%async_computation.2 | async-start | bytes 4194304 | tf_op jit(solution)/shard_map/all_to_all | solution.py:158
  159.9 3.5 %collective-permute-start = (bf16[2,2,512]{2,1,0:T(2,128)(2,1)S(1)}, bf16[2,2,512]{2,1,0:T(2,128)(2,1)S(1)}, u32[]{:S(2)}, u32[]{:S(2)}) collective-permute-start(bf16[2,2,512]{2,1,0:T(2,128)(2,1)S(1)} %pad_maximum_fusion.4), channel_id=1, source_target_pairs={{0,2},{2,4},{4,6},{6,8},{8,10},{10,12},{12,14},{14,16},{16,18},{18... | collective-permute-start | bytes 12296 | tf_op jit(solution)/shard_map/ppermute | solution.py:70
  165.3 16.5 %collective-permute-done = bf16[2,2,512]{2,1,0:T(2,128)(2,1)S(1)} collective-permute-done((bf16[2,2,512]{2,1,0:T(2,128)(2,1)S(1)}, bf16[2,2,512]{2,1,0:T(2,128)(2,1)S(1)}, u32[]{:S(2)}, u32[]{:S(2)}) %collective-permute-start) | collective-permute-done | bytes 4128 | tf_op jit(solution)/shard_map/ppermute | solution.py:70
  181.8 7.8 %all-to-all-done.2 = bf16[64,16,1024]{2,1,0:T(8,128)(2,1)S(1)} async-done(((bf16[64,16,1024]{2,1,0:T(8,128)(2,1)}), bf16[64,16,1024]{2,1,0:T(8,128)(2,1)S(1)}, u32[]{:S(2)}, u32[]{:S(2)}) %all-to-all-start.2) | async-done | bytes 2097184 | tf_op jit(solution)/shard_map/all_to_all | solution.py:158
  195.3 4.7 %all_to_all.36 = bf16[2,256,1024]{1,2,0:T(8,128)(2,1)S(1)} all-to-all(bf16[2,256,1024]{1,2,0:T(8,128)(2,1)S(1)} %broadcast_in_dim.8), channel_id=1, replica_groups=mesh['sp_0'=4,'sp_1'=4,'sp_2'=4,'tp'=2] {'tp'}, dimensions={0} | all-to-all | bytes 2097152 | tf_op jit(solution)/shard_map/all_to_all | solution.py:60
  201.6 2.7 fusion.54
  204.4 43.7 %reduce-scatter.4.cloned.1.call-done = f32[512,512]{1,0:T(8,128)} async-done(((f32[2048,512]{1,0:T(8,128)}), f32[512,512]{1,0:T(8,128)}) %reduce-scatter.4.cloned.1.call-update) | async-done | bytes 1048592 | tf_op jit(solution)/shard_map/reduce_scatter | solution.py:75
  248.2 6.7 %convolution_bitcast_fusion = f32[1,2048,512]{2,1,0:T(8,128)} fusion(bf16[1024,512]{1,0:T(8,128)(2,1)S(1)} %copy-done.17, bf16[2048,2048]{1,0:T(8,128)(2,1)} %all-gather.6.cloned.1.call-done), kind=kOutput, calls=%fused_computation.9 | convolution fusion | flops 2147483648 | bytes 9437184 | tf_op jit(solution)/shard_map/dot_general | solution.py:94
  254.9 6.7 %fusion.4 = f32[1,512,2048]{2,1,0:T(8,128)} fusion(bf16[2048,2048]{1,0:T(8,128)(2,1)} %all-gather.6.cloned.1.call-done, f32[1024,512]{1,0:T(8,128)S(1)} %copy-done.20, f32[1024,512]{1,0:T(8,128)S(1)} %copy-done.22), kind=kOutput, calls=%fused_computation.8 | convolution fusion | flops 2150629376 | bytes 12582912 | tf_op jit(solution)/shard_map/dot_general | solution.py:94
  263.1 10.7 %reduce-scatter.6.cloned.1.call-done = f32[128,512]{1,0:T(8,128)} async-done(((f32[512,512]{1,0:T(8,128)}), f32[128,512]{1,0:T(8,128)}) %reduce-scatter.6.cloned.1.call-update) | async-done | bytes 262160 | tf_op jit(solution)/shard_map/reduce_scatter | solution.py:75
  273.9 7.0 %convolution_bitcast_fusion.1 = f32[1,2048,512]{2,1,0:T(8,128)} fusion(bf16[1024,512]{1,0:T(8,128)(2,1)} %copy-done.18, bf16[2048,2048]{1,0:T(8,128)(2,1)} %all-gather.6.cloned.1.call-done), kind=kOutput, calls=%fused_computation.10 | convolution fusion | flops 2147483648 | bytes 9437184 | tf_op jit(solution)/shard_map/dot_general | solution.py:94
  282.6 14.5 %reduce-scatter.8.cloned.1.call-done = f32[32,512]{1,0:T(8,128)} async-done(((f32[128,512]{1,0:T(8,128)}), f32[32,512]{1,0:T(8,128)}) %reduce-scatter.8.cloned.1.call-update) | async-done | bytes 65552 | tf_op jit(solution)/shard_map/reduce_scatter | solution.py:75
  (97 shorter events, 27.9 us)
Async XLA Ops:
  7.2 117.4 %copy-start = (bf16[1,2048,512]{2,1,0:T(8,128)(2,1)S(1)}, bf16[1,2048,512]{2,1,0:T(8,128)(2,1)}, u32[]{:S(2)}) copy-start(bf16[1,2048,512]{2,1,0:T(8,128)(2,1)} %param.23) | copy-start | bytes 6291460
  7.2 112.0 %all-gather.6.cloned.1.call-start = ((), (), s32[]{:S(2)}) async-start(), calls=%async_computation.7 | async-start | bytes 12582912 | tf_op jit(solution)/shard_map/all_gather | solution.py:37
  13.2 3.7 %copy-start.12 = (f32[256,2]{0,1:T(2,128)S(1)}, f32[256,2]{0,1:T(2,128)}, u32[]{:S(2)}) copy-start(f32[256,2]{0,1:T(2,128)} %param.16) | copy-start | bytes 6148
  13.2 4.1 %copy-start.10 = (s32[256,2]{0,1:T(2,128)S(1)}, s32[256,2]{0,1:T(2,128)}, u32[]{:S(2)}) copy-start(s32[256,2]{0,1:T(2,128)} %param.17) | copy-start | bytes 6148
  13.2 4.6 %copy-start.2 = (bf16[256,1024]{1,0:T(8,128)(2,1)S(1)}, bf16[256,1024]{1,0:T(8,128)(2,1)}, u32[]{:S(2)}) copy-start(bf16[256,1024]{1,0:T(8,128)(2,1)} %param.13) | copy-start | bytes 1572868
  119.2 5.3 %copy-start.13 = (bf16[2048,2048]{1,0:T(8,128)(2,1)S(1)}, bf16[2048,2048]{1,0:T(8,128)(2,1)}, u32[]{:S(2)}) copy-start(bf16[2048,2048]{1,0:T(8,128)(2,1)} %all-gather.6.cloned.1.call-done) | copy-start | bytes 25165828
  126.9 3.0 copy-start.21
  148.6 10.6 %copy-start.6 = (bf16[256,512]{1,0:T(8,128)(2,1)S(1)}, bf16[256,512]{1,0:T(8,128)(2,1)}, u32[]{:S(2)}) copy-start(bf16[256,512]{1,0:T(8,128)(2,1)} %param.18) | copy-start | bytes 786436
  148.6 16.7 %copy-start.11 = (f32[3,512]{1,0:T(4,128)S(1)}, f32[3,512]{1,0:T(4,128)}, u32[]{:S(2)}) copy-start(f32[3,512]{1,0:T(4,128)} %param.21) | copy-start | bytes 18436
  148.6 41.1 %all-to-all-start.2 = ((bf16[64,16,1024]{2,1,0:T(8,128)(2,1)}), bf16[64,16,1024]{2,1,0:T(8,128)(2,1)S(1)}, u32[]{:S(2)}, u32[]{:S(2)}) async-start(bf16[64,16,1024]{2,1,0:T(8,128)(2,1)} %bitcast.8), calls=%async_computation.2 | async-start | bytes 4194304 | tf_op jit(solution)/shard_map/all_to_all | solution.py:158
  159.1 89.0 %reduce-scatter.4.cloned.1.call-start = ((), (), s32[]{:S(2)}) async-start(), calls=%async_computation.8 | async-start | bytes 5242880 | tf_op jit(solution)/shard_map/reduce_scatter | solution.py:75
  159.9 21.9 %collective-permute-start = (bf16[2,2,512]{2,1,0:T(2,128)(2,1)S(1)}, bf16[2,2,512]{2,1,0:T(2,128)(2,1)S(1)}, u32[]{:S(2)}, u32[]{:S(2)}) collective-permute-start(bf16[2,2,512]{2,1,0:T(2,128)(2,1)S(1)} %pad_maximum_fusion.4), channel_id=1, source_target_pairs={{0,2},{2,4},{4,6},{6,8},{8,10},{10,12},{12,14},{14,16},{16,18},{18... | collective-permute-start | bytes 12296 | tf_op jit(solution)/shard_map/ppermute | solution.py:70
  195.0 5.0 %copy-start.5 = (bf16[256,1024]{1,0:T(8,128)(2,1)}, bf16[256,1024]{1,0:T(8,128)(2,1)S(1)}, u32[]{:S(2)}) copy-start(bf16[256,1024]{1,0:T(8,128)(2,1)S(1)} %fusion.30) | copy-start | bytes 1572868
  195.2 4.8 %copy-start.3 = (f32[256,512]{1,0:T(8,128)S(1)}, f32[256,512]{1,0:T(8,128)}, u32[]{:S(2)}) copy-start(f32[256,512]{1,0:T(8,128)} %convert_multiply_fusion.4) | copy-start | bytes 1572868
  195.2 4.8 %copy-start.4 = (bf16[2048,512]{1,0:T(8,128)(2,1)S(1)}, bf16[2048,512]{1,0:T(8,128)(2,1)}, u32[]{:S(2)}) copy-start(bf16[2048,512]{1,0:T(8,128)(2,1)} %param.22) | copy-start | bytes 6291460
  195.2 4.8 %copy-start.8 = (bf16[256,512]{1,0:T(8,128)(2,1)S(1)}, bf16[256,512]{1,0:T(8,128)(2,1)}, u32[]{:S(2)}) copy-start(bf16[256,512]{1,0:T(8,128)(2,1)} %param.19) | copy-start | bytes 786436
  204.3 43.8 %copy-start.17 = (bf16[1024,512]{1,0:T(8,128)(2,1)S(1)}, bf16[1024,512]{1,0:T(8,128)(2,1)}, u32[]{:S(2)}) copy-start(bf16[1024,512]{1,0:T(8,128)(2,1)} %copy-done.16) | copy-start | bytes 3145732
  204.3 69.5 %reduce-scatter.6.cloned.1.call-start = ((), (), s32[]{:S(2)}) async-start(), calls=%async_computation.9 | async-start | bytes 1310720 | tf_op jit(solution)/shard_map/reduce_scatter | solution.py:75
  248.1 49.0 %reduce-scatter.8.cloned.1.call-start = ((), (), s32[]{:S(2)}) async-start(), calls=%async_computation.10 | async-start | bytes 327680 | tf_op jit(solution)/shard_map/reduce_scatter | solution.py:75
  248.2 6.8 %copy-start.20 = (f32[1024,512]{1,0:T(8,128)S(1)}, f32[1024,512]{1,0:T(8,128)}, u32[]{:S(2)}) copy-start(f32[1024,512]{1,0:T(8,128)} %copy-done.19) | copy-start | bytes 6291460
  248.2 6.7 %copy-start.22 = (f32[1024,512]{1,0:T(8,128)S(1)}, f32[1024,512]{1,0:T(8,128)}, u32[]{:S(2)}) copy-start(f32[1024,512]{1,0:T(8,128)} %copy-done.21) | copy-start | bytes 6291460
  261.6 19.3 %collective-permute-start.1 = (f32[2,512]{1,0:T(2,128)S(1)}, f32[2,512]{1,0:T(2,128)S(1)}, u32[]{:S(2)}, u32[]{:S(2)}) collective-permute-start(f32[2,512]{1,0:T(2,128)S(1)} %slice.74), channel_id=1, source_target_pairs={{2,0},{4,2},{6,4},{8,6},{10,8},{12,10},{14,12},{16,14},{18,16},{20... | collective-permute-start | bytes 12296 | tf_op jit(solution)/shard_map/ppermute | solution.py:70
  273.9 8.0 %copy-start.7 = (bf16[256,512]{1,0:T(8,128)(2,1)S(1)}, bf16[256,512]{1,0:T(8,128)(2,1)}, u32[]{:S(2)}) copy-start(bf16[256,512]{1,0:T(8,128)(2,1)} %param.20) | copy-start | bytes 786436
  273.9 23.3 %copy-start.1 = (bf16[1,2048,512]{2,1,0:T(8,128)(2,1)S(1)}, bf16[1,2048,512]{2,1,0:T(8,128)(2,1)}, u32[]{:S(2)}) copy-start(bf16[1,2048,512]{2,1,0:T(8,128)(2,1)} %param.23) | copy-start | bytes 6291460
  (6 other events, 14.9 us)
Sparse Core Ops, SparseCore 0:
  100.0 19.1 all-gather.5
  204.5 43.5 reduce-scatter.3
  250.5 23.2 reduce-scatter.5
  276.6 20.4 reduce-scatter.7
where the time goes:
time: 305 us; the launch traced here: 304 us
  waiting for transfers between devices  113 us (37%)
  blocking collectives  80.9 us (27%)
  matrix products  45.6 us (15%)
  other arithmetic  17.5 us (6%)
  local copies, waits for them, and re-layouts  17 us (6%)
  starting transfers between devices  15.7 us (5%)
  between operations  14.2 us (5%)
    reduce_scatter x3, waiting for transfers between devices, sum_by_axis(): subtotal = lax.psum_scatter(subtotal, axis, scatter_dimension=0, tiled=True)  69 us
    all_to_all x1, blocking collectives, side_by_side(): lax.all_to_all(both, axis, split_axis=split_dim, concat_axis=concat_dim,...  64.4 us
    dot_general x5, matrix products, contract_rows(): lax.dot_general(left, right, (((0,), (0,)), ((), ())), preferred_element_...  24.9 us
    all_gather x1, waiting for transfers between devices, sent_together(): lax.all_gather(both, axis, axis=dim, tiled=True)  19.3 us
    ppermute x2, waiting for transfers between devices, shifted(): lax.ppermute(value, axis, [(source, source + steps) for source in range(l...  16.6 us
    all_to_all x1, starting transfers between devices, local(): lax.all_to_all(row_grads, SP, split_axis=0, concat_axis=0, tiled=True)  10.6 us
    all_to_all x1, blocking collectives, sent_and_summed(): lax.all_to_all(parts, axis, split_axis=0, concat_axis=0, tiled=True)  8.18 us
    all_to_all x1, waiting for transfers between devices, local(): lax.all_to_all(row_grads, SP, split_axis=0, concat_axis=0, tiled=True)  7.83 us
  transfers between devices with their start and end apart: 7, of which 6 were waited for; matrix products, arithmetic and copies ran while one was open for 8% of the time, Pallas kernels for 0%

commit v1 on v0

v1 whole, which is shorter than its diff:
```python
import jax
import jax.numpy as jnp
from jax import lax
from jax.experimental import pallas as pl
from jax.experimental.pallas import tpu as pltpu
from jax.sharding import Mesh
from jax.sharding import PartitionSpec as P

D = 2048
SP = ("sp_0", "sp_1", "sp_2")
EPSILON = 1e-06
VMEM = 56 * 1024 * 1024
F32 = jnp.float32
BF16 = jnp.bfloat16


def dot_nn(a, b):
    return lax.dot_general(a, b, (((1,), (0,)), ((), ())), preferred_element_type=F32)


def dot_nt(a, b):
    return lax.dot_general(a, b, (((1,), (1,)), ((), ())), preferred_element_type=F32)


def dot_tn(a, b):
    return lax.dot_general(a, b, (((0,), (0,)), ((), ())), preferred_element_type=F32)


def cost(flops, size):
    return pl.CostEstimate(flops=flops, transcendentals=0, bytes_accessed=size)


def swap(value):
    return lax.ppermute(value, "tp", [(0, 1), (1, 0)])


def exchange(value, axis):
    return lax.all_to_all(value, axis, split_axis=0, concat_axis=0, tiled=True)


def shifted(value, axis, steps):
    count = lax.axis_size(axis)
    leading, last = (max(0, -steps), min(count, count - steps))
    return lax.ppermute(value, axis, [(source, source + steps) for source in range(leading, last)])


def turned(value, axis, steps):
    count = lax.axis_size(axis)
    return lax.ppermute(value, axis, [(i, (i + steps) % count) for i in range(count)])


def slots_body(experts, capacity, stream_ref, routes_ref, squares_ref, target_ref):
    values = stream_ref[...].astype(F32)
    squares = values * values
    high = squares.astype(BF16)
    low = (squares - high.astype(F32)).astype(BF16)
    ones = jnp.ones((8, values.shape[1]), BF16)
    squares_ref[...] = (dot_nt(ones, high) + dot_nt(ones, low))[0:1]
    tokens = values.shape[0]
    first, second = routes_ref[0:1, :], routes_ref[1:2, :]
    ids = lax.broadcasted_iota(jnp.int32, (experts, tokens), 0)
    named_first = (ids == first).astype(F32)
    named_second = (ids == second).astype(F32)
    before = (
        lax.broadcasted_iota(jnp.int32, (tokens, tokens), 0)
        < lax.broadcasted_iota(jnp.int32, (tokens, tokens), 1)
    ).astype(F32)
    earlier = dot_nn((named_first + named_second).astype(BF16), before.astype(BF16))
    rank_first = jnp.sum(named_first * earlier, axis=0, keepdims=True).astype(jnp.int32)
    rank_second = jnp.sum(named_second * earlier, axis=0, keepdims=True).astype(jnp.int32)
    target_ref[0:1, :] = first * capacity + rank_first
    target_ref[1:2, :] = second * capacity + rank_second


def find_slots(stream, routes, experts, capacity):
    tokens = stream.shape[0]

    def body(*refs):
        slots_body(experts, capacity, *refs)

    return pl.pallas_call(
        body,
        out_shape=(
            jax.ShapeDtypeStruct((1, tokens), F32),
            jax.ShapeDtypeStruct((2, tokens), jnp.int32),
        ),
        name="find_slots",
        cost_estimate=cost(10**8, stream.size * 2),
    )(stream, routes)


def rows_body(target_ref, weight_ref, total_ref, stream_ref, cot_ref, gain_ref, out_ref, sel_ref):
    rows, tokens = sel_ref.shape
    width = stream_ref.shape[1]
    slots = lax.broadcasted_iota(jnp.int32, (rows, tokens), 0) + pl.program_id(0) * rows
    first = slots == target_ref[0:1, :]
    second = slots == target_ref[1:2, :]
    inverse = lax.rsqrt(total_ref[...] / D + EPSILON)
    both = jnp.where(first | second, 1.0, 0.0)
    selector = both.astype(BF16)
    scale = jnp.sum(both * inverse, axis=1, keepdims=True)
    weight = jnp.where(first, weight_ref[0:1, :], 0.0) + jnp.where(second, weight_ref[1:2, :], 0.0)
    weight = jnp.sum(weight, axis=1, keepdims=True)
    sel_ref[...] = selector
    inputs = dot_nn(selector, stream_ref[...])
    out_ref[:, :width] = (inputs * scale * gain_ref[...]).astype(BF16)
    grads = dot_nn(selector, cot_ref[...])
    out_ref[:, width:] = (weight * grads).astype(BF16)


def build_rows(target, weights, total, stream, cot, gain, slots):
    tokens, width = stream.shape
    rows = slots // 8

    def whole(*shape):
        return pl.BlockSpec(shape, lambda i: (0, 0))

    return pl.pallas_call(
        rows_body,
        grid=(8,),
        in_specs=[
            whole(2, tokens),
            whole(2, tokens),
            whole(1, tokens),
            whole(tokens, width),
            whole(tokens, width),
            whole(1, width),
        ],
        out_specs=(
            pl.BlockSpec((rows, 2 * width), lambda i: (i, 0)),
            pl.BlockSpec((rows, tokens), lambda i: (i, 0)),
        ),
        out_shape=(
            jax.ShapeDtypeStruct((slots, 2 * width), BF16),
            jax.ShapeDtypeStruct((slots, tokens), BF16),
        ),
        name="build_rows",
        cost_estimate=cost(4 * slots * tokens * width, slots * width * 4),
    )(target, weights, total, stream, cot, gain)


def expert_body(
    core_ref, own_ref, peer_ref, gate_own, gate_peer, up_own, up_peer, down_own, down_peer,
    hidden_ref, gate_ref, up_ref, mine_ref, theirs_ref,
):
    width = gate_own.shape[0]
    own_x, own_y = own_ref[:, :width], own_ref[:, width:]
    peer_x, peer_y = peer_ref[:, :width], peer_ref[:, width:]
    gate_lin = dot_nn(own_x, gate_own[...]) + dot_nn(peer_x, gate_peer[...])
    up_lin = dot_nn(own_x, up_own[...]) + dot_nn(peer_x, up_peer[...])
    hidden_grad = dot_nt(own_y, down_own[...]) + dot_nt(peer_y, down_peer[...])
    sig = jax.nn.sigmoid(gate_lin)
    silu = gate_lin * sig
    hidden_ref[...] = (silu * up_lin).astype(BF16)
    gate_pre = (hidden_grad * up_lin * sig * (1.0 + gate_lin * (1.0 - sig))).astype(BF16)
    up_pre = (hidden_grad * silu).astype(BF16)
    gate_ref[...] = gate_pre
    up_ref[...] = up_pre
    mine_ref[...] = (dot_nt(gate_pre, gate_own[...]) + dot_nt(up_pre, up_own[...])).astype(BF16)
    theirs_ref[...] = (dot_nt(gate_pre, gate_peer[...]) + dot_nt(up_pre, up_peer[...])).astype(BF16)


def expert_rows(core, own, peer, gate_w, up_w, down_w):
    rows, double = own.shape
    width = double // 2
    units = gate_w.shape[1]
    step = 256

    def block(n):
        return pl.BlockSpec((step, n), lambda i, c: (i, 0))

    tall_own = pl.BlockSpec((width, units), lambda i, c: (c[0], 0))
    tall_peer = pl.BlockSpec((width, units), lambda i, c: (1 - c[0], 0))
    wide_own = pl.BlockSpec((units, width), lambda i, c: (0, c[0]))
    wide_peer = pl.BlockSpec((units, width), lambda i, c: (0, 1 - c[0]))
    narrow = jax.ShapeDtypeStruct((rows, units), BF16)
    broad = jax.ShapeDtypeStruct((rows, width), BF16)
    return pl.pallas_call(
        expert_body,
        grid_spec=pltpu.PrefetchScalarGridSpec(
            num_scalar_prefetch=1,
            grid=(rows // step,),
            in_specs=[
                block(double), block(double),
                tall_own, tall_peer, tall_own, tall_peer, wide_own, wide_peer,
            ],
            out_specs=[block(units), block(units), block(units), block(width), block(width)],
        ),
        out_shape=[narrow, narrow, narrow, broad, broad],
        compiler_params=pltpu.CompilerParams(vmem_limit_bytes=VMEM),
        name="expert_rows",
        cost_estimate=cost(20 * rows * width * units, 20 * rows * width),
    )(core, own, peer, gate_w, gate_w, up_w, up_w, down_w, down_w)


def weights_body(
    core_ref, own_x, own_y, peer_x, peer_y, hidden_ref, gate_ref, up_ref,
    gate_out, up_out, down_out,
):
    def emit(x, y):
        gate_out[...] = dot_tn(x, gate_ref[...])
        up_out[...] = dot_tn(x, up_ref[...])
        down_out[...] = dot_tn(hidden_ref[...], y)

    half = pl.num_programs(0) // 2

    @pl.when(pl.program_id(0) < half)
    def _():
        emit(own_x[...], own_y[...])

    @pl.when(pl.program_id(0) >= half)
    def _():
        emit(peer_x[...], peer_y[...])


def weight_grads(core, own, peer, hidden, gate_pre, up_pre):
    rows, double = own.shape
    width = double // 2
    units = hidden.shape[1]
    chunk = 256
    half = width // chunk

    def own_at(base):
        return pl.BlockSpec((rows, chunk), lambda s, c: (0, base + jnp.minimum(s, half - 1)))

    def peer_at(base):
        return pl.BlockSpec((rows, chunk), lambda s, c: (0, base + jnp.maximum(s - half, 0)))

    def place(s, c):
        side = jnp.where(s < half, c[0], 1 - c[0])
        return side * half + jnp.where(s < half, s, s - half)

    whole = pl.BlockSpec((rows, units), lambda s, c: (0, 0))
    tall = pl.BlockSpec((chunk, units), lambda s, c: (place(s, c), 0))
    wide = pl.BlockSpec((units, chunk), lambda s, c: (0, place(s, c)))
    return pl.pallas_call(
        weights_body,
        grid_spec=pltpu.PrefetchScalarGridSpec(
            num_scalar_prefetch=1,
            grid=(2 * half,),
            in_specs=[own_at(0), own_at(half), peer_at(0), peer_at(half), whole, whole, whole],
            out_specs=[tall, tall, wide],
        ),
        out_shape=[
            jax.ShapeDtypeStruct((double, units), F32),
            jax.ShapeDtypeStruct((double, units), F32),
            jax.ShapeDtypeStruct((units, double), F32),
        ],
        compiler_params=pltpu.CompilerParams(vmem_limit_bytes=VMEM),
        name="weight_grads",
        cost_estimate=cost(12 * rows * width * units, 24 * width * units),
    )(core, own, own, peer, peer, hidden, gate_pre, up_pre)


def local(
    stream,
    norm_gain,
    cotangent,
    route_weights,
    routes,
    conv_input,
    conv_bgate,
    conv_cgate,
    conv_taps,
    out_proj,
    gate_weight,
    up_weight,
    down_weight,
):
    experts = lax.axis_size(SP)
    tok_count, width = stream.shape
    top_count = routes.shape[1]
    capacity = 2 * tok_count * top_count // experts
    slots = experts * capacity
    core = lax.axis_index("tp")
    core_arg = core.astype(jnp.int32).reshape(1)
    gain_row = norm_gain[None, :]

    squares, target = find_slots(stream, routes.T, experts, capacity)
    total = squares + swap(squares)
    rows, selector = build_rows(
        target, route_weights.T, total, stream, cotangent, gain_row, slots
    )
    own = exchange(rows.reshape(experts, capacity, 2 * width), SP).reshape(slots, 2 * width)

    input_float = conv_input.astype(F32)
    cgate_float = conv_cgate.astype(F32)
    bgate_float = conv_bgate.astype(F32)
    rim_rows = shifted(jnp.stack([conv_input[-2:], conv_cgate[-2:]]), SP, 1)
    rim_gated = rim_rows[1].astype(F32) * rim_rows[0].astype(F32)
    gated = cgate_float * input_float
    extended = jnp.concatenate([rim_gated, gated], axis=0)
    conv_out = (
        conv_taps[0][None, :] * extended[:-2]
        + conv_taps[1][None, :] * extended[1:-1]
        + conv_taps[2][None, :] * extended[2:]
    )
    mixer_out = (bgate_float * conv_out).astype(BF16)
    line = lax.axis_size("sp_0")
    spot = lax.axis_index("sp_0")
    around = jnp.stack([mixer_out] + [turned(mixer_out, "sp_0", s) for s in range(1, line)])
    mixers = jnp.concatenate(
        [lax.dynamic_slice_in_dim(around, (spot - k) % line, 1, 0) for k in range(line)], axis=0
    )
    token_half = tok_count // 2
    channels = mixer_out.shape[1]

    def half_of(array, which, dim):
        return lax.dynamic_slice_in_dim(array, which * token_half, token_half, dim)

    mixers_mine = half_of(mixers, core, 1).reshape(line * token_half, channels)
    mixers_theirs = half_of(mixers, 1 - core, 1).reshape(line * token_half, channels)

    peer = swap(own)
    hidden, gate_pre, up_pre, part_mine, part_theirs = expert_rows(
        core_arg, own, peer, gate_weight[0], up_weight[0], down_weight[0]
    )
    other = swap(part_theirs)
    row_grads = (part_mine.astype(F32) + other.astype(F32)).astype(BF16)
    returned = exchange(row_grads.reshape(experts, capacity, width), SP).reshape(slots, width)
    gate_g, up_g, down_g = weight_grads(core_arg, own, peer, hidden, gate_pre, up_pre)

    normed_grad = dot_tn(selector, returned)
    stream_float = stream.astype(F32)
    cot_float = cotangent.astype(F32)
    inverse = lax.rsqrt(total[0] / D + EPSILON)[:, None]
    cross_part = jnp.sum(stream_float * gain_row * normed_grad, axis=1)
    cross = cross_part + swap(cross_part)
    stream_grad = (
        cot_float
        + inverse * gain_row * normed_grad
        - stream_float * inverse * inverse * inverse * cross[:, None] / D
    ).astype(BF16)

    grad_peer = swap(stream_grad)
    mine_half, peer_half = half_of(stream_grad, core, 0), half_of(grad_peer, core, 0)
    low = jnp.where(core == 0, mine_half, peer_half)
    high = jnp.where(core == 0, peer_half, mine_half)
    quarter = 2 * width // line
    parts = [low[:, :quarter], low[:, quarter:], high[:, :quarter], high[:, quarter:]]
    sent = jnp.stack(parts)
    grads_mine = exchange(sent, "sp_0").reshape(line * token_half, quarter)
    grads_theirs = swap(grads_mine)
    proj_part = dot_tn(grads_mine, mixers_mine) + dot_tn(grads_theirs, mixers_theirs)
    plane = lax.axis_size(("sp_1", "sp_2"))
    arrived = exchange(proj_part.reshape(plane, quarter // plane, channels), ("sp_1", "sp_2"))
    proj_grad = arrived.sum(axis=0)

    proj_mine = lax.dynamic_slice_in_dim(out_proj, core * width, width, 0)
    proj_peer = lax.dynamic_slice_in_dim(out_proj, (1 - core) * width, width, 0)
    mixer_grad = dot_nn(stream_grad, proj_mine) + dot_nn(grad_peer, proj_peer)
    delta = mixer_grad * bgate_float
    next_rim = shifted(delta[:2], SP, -1)
    extended_back = jnp.concatenate([delta, next_rim], axis=0)
    gated_grad = (
        conv_taps[2][None, :] * extended_back[:-2]
        + conv_taps[1][None, :] * extended_back[1:-1]
        + conv_taps[0][None, :] * extended_back[2:]
    )
    bgate_grad = (mixer_grad * conv_out).astype(BF16)
    input_grad = (gated_grad * cgate_float).astype(BF16)
    cgate_grad = (gated_grad * input_float).astype(BF16)
    return (
        stream_grad,
        proj_grad,
        input_grad,
        bgate_grad,
        cgate_grad,
        gate_g[None],
        up_g[None],
        down_g[None],
    )


def solution(mesh):
    finer = Mesh(mesh.devices.reshape(4, 4, 4, mesh.shape["tp"]), ("sp_0", "sp_1", "sp_2", "tp"))
    return jax.shard_map(
        local,
        mesh=finer,
        in_specs=(
            P(SP, "tp"),
            P("tp"),
            P(SP, "tp"),
            P(SP, None),
            P(SP, None),
            P(SP, "tp"),
            P(SP, "tp"),
            P(SP, "tp"),
            P(None, "tp"),
            P(None, "tp"),
            P(SP, None, "tp"),
            P(SP, None, "tp"),
            P(SP, "tp", None),
        ),
        out_specs=(
            P(SP, "tp"),
            P(SP, "tp"),
            P(SP, "tp"),
            P(SP, "tp"),
            P(SP, "tp"),
            P(SP, None, "tp"),
            P(SP, None, "tp"),
            P(SP, "tp", None),
        ),
        check_vma=False,
    )
```

time: 305 us -> 205 us (0.67)
  waiting for transfers between devices: 113 us -> 54.1 us
  Pallas kernels: 0 us -> 39.5 us
  matrix products: 45.6 us -> 8.97 us
  blocking collectives: 80.9 us -> 64.5 us
  local copies, waits for them, and re-layouts: 17 us -> 1.03 us
  between operations: 14.2 us -> 0.9 us
  starting transfers between devices: 15.7 us -> 22.7 us
  other arithmetic: 17.5 us -> 12.2 us
    reduce_scatter x3 -> x0, waiting for transfers between devices: 69 us -> none  [sum_by_axis(): subtotal = lax.psum_scatter(subtotal, axis, scatter_dimension=0, tiled=True)]
    pallas_call x0 -> x4, Pallas kernels: none -> 39.5 us  [the longest x1 16.7 us: expert_rows(): pl.pallas_call(expert_body, grid_spec=pltpu.PrefetchScalarGridSpec(num_sc...]
    dot_general x13 -> x5, matrix products: 45.6 us -> 8.97 us  [the longest x3 5.61 us: dot_tn(): lax.dot_general(a, b, (((0,), (0,)), ((), ())), preferred_element_type=F32)]
    all_to_all x1 -> x3, waiting for transfers between devices: 7.83 us -> 32.6 us  [exchange(): return lax.all_to_all(value, axis, split_axis=0, concat_axis=0, tiled=True)]
    ppermute x0 -> x9, waiting for transfers between devices: none -> 21.5 us  [the longest x6 14.9 us: swap(): return lax.ppermute(value, 'tp', [(0, 1), (1, 0)])]
    all_gather x1 -> x0, waiting for transfers between devices: 19.3 us -> none  [sent_together(): lax.all_gather(both, axis, axis=dim, tiled=True)]
    ppermute x2, waiting for transfers between devices: 16.6 us -> 0.01 us  [shifted(): lax.ppermute(value, axis, [(source, source + steps) for source in range(l...]
    all_to_all x3 -> x1, blocking collectives: 77.3 us -> 64.5 us  [exchange(): return lax.all_to_all(value, axis, split_axis=0, concat_axis=0, tiled=True)]
  transfers between devices with their start and end apart: 7 -> 14, of which waited for: 6 -> 11; matrix products, arithmetic and copies ran while one was open for 8% -> 6% of each run, Pallas kernels for 0% -> 7%
where the time goes in v1:
time: 205 us; the launch traced here: 204 us
  blocking collectives  64.5 us (31%)
  waiting for transfers between devices  54.1 us (26%)
  Pallas kernels  39.5 us (19%)
  starting transfers between devices  22.7 us (11%)
  other arithmetic  12.2 us (6%)
  matrix products  8.97 us (4%)
    all_to_all x1, blocking collectives, exchange(): return lax.all_to_all(value, axis, split_axis=0, concat_axis=0, tiled=True)  64.5 us
    all_to_all x3, waiting for transfers between devices, exchange(): return lax.all_to_all(value, axis, split_axis=0, concat_axis=0, tiled=True)  32.6 us
    pallas_call x1, Pallas kernels, expert_rows(): pl.pallas_call(expert_body, grid_spec=pltpu.PrefetchScalarGridSpec(num_sc...  16.7 us
    all_to_all x3, starting transfers between devices, exchange(): return lax.all_to_all(value, axis, split_axis=0, concat_axis=0, tiled=True)  15.1 us
    ppermute x6, waiting for transfers between devices, swap(): return lax.ppermute(value, 'tp', [(0, 1), (1, 0)])  14.9 us
    pallas_call x1, Pallas kernels, weight_grads(): pl.pallas_call(weights_body, grid_spec=pltpu.PrefetchScalarGridSpec(num_s...  14.6 us
    ppermute x3, waiting for transfers between devices, turned(): lax.ppermute(value, axis, [(i, (i + steps) % count) for i in range(count)])  6.61 us
    pallas_call x1, Pallas kernels, build_rows(): pl.pallas_call(rows_body, grid=(8,), in_specs=[whole(2, tokens), whole(2,...  6.04 us
  transfers between devices with their start and end apart: 14, of which 11 were waited for; matrix products, arithmetic and copies ran while one was open for 6% of the time, Pallas kernels for 7%

profile of v1, /device:TPU:0, one launch (start us, length us, event | category | flops | bytes accessed | tf_op | source)
XLA Modules:
  0.0 203.9 jit_solution(11835283867764007897)
XLA Ops:
  0.6 2.2 %find_slots.1 = (f32[1,256]{1,0:T(1,128)}, s32[2,256]{1,0:T(2,128)}) custom-call(bf16[256,1024]{1,0:T(8,128)(2,1)} %stream_ref.1, s32[2,256]{1,0:T(2,128)} %bitcast.59), custom_call_target="tpu_custom_call" | custom-call | flops 100000000 | bytes 524288 | tf_op jit(solution)/shard_map/find_slots/pallas_call | solution.py:81
  2.9 1.4 collective-permute-done
  5.5 6.0 %build_rows.1 = (bf16[1024,2048]{1,0:T(8,128)(2,1)}, bf16[1024,256]{1,0:T(8,128)(2,1)}) custom-call(s32[2,256]{1,0:T(2,128)} %get-tuple-element.21.target_ref, f32[2,256]{1,0:T(2,128)} %bitcast.66, f32[1,256]{1,0:T(1,128)} %get-tuple-element.37.total_ref, bf16[256,1024]{1,0:T(8,128)(2,1)} %stream_ref.1, bf16[256,1024]{1,0:T(8,128)(2,1)} %cot_ref.1, ...), custom_call_target="tpu_custom_call" | custom-call | flops 1073741824 | bytes 4194304 | tf_op jit(solution)/shard_map/build_rows/pallas_call | solution.py:118
  11.5 64.5 %all_to_all.20 = bf16[64,16,2048]{2,1,0:T(8,128)(2,1)} all-to-all(bf16[64,16,2048]{2,1,0:T(8,128)(2,1)} %bitcast.49), channel_id=1, replica_groups=mesh['sp_0'=4,'sp_1'=4,'sp_2'=4,'tp'=2] {'sp_0','sp_1','sp_2'}, dimensions={0} | all-to-all | bytes 8388608 | tf_op jit(solution)/shard_map/all_to_all | solution.py:38
  76.0 7.5 %collective-permute-done.1.peer_ref.peer_x.peer_y = bf16[1024,2048]{1,0:T(8,128)(2,1)} collective-permute-done((bf16[1024,2048]{1,0:T(8,128)(2,1)}, bf16[1024,2048]{1,0:T(8,128)(2,1)}, u32[]{:S(2)}, u32[]{:S(2)}) %collective-permute-start.1) | collective-permute-done | bytes 4194336 | tf_op jit(solution)/shard_map/ppermute | solution.py:34
  83.5 16.7 %expert_rows.1 = (bf16[1024,512]{1,0:T(8,128)(2,1)}, bf16[1024,512]{1,0:T(8,128)(2,1)}, bf16[1024,512]{1,0:T(8,128)(2,1)}, bf16[1024,1024]{1,0:T(8,128)(2,1)}, bf16[1024,1024]{1,0:T(8,128)(2,1)}) custom-call(s32[1]{0:T(128)} %bitcast.4.core_ref, bf16[1024,2048]{1,0:T(8,128)(2,1)} %bitcast.6.own_ref.own_x.own_y, ...), custom_call_target="tpu_custom_call" | custom-call | flops 10737418240 | bytes 20971520 | tf_op jit(solution)/shard_map/expert_rows/pallas_call | solution.py:178
  100.3 4.3 %collective-permute-done.2 = bf16[1024,1024]{1,0:T(8,128)(2,1)S(1)} collective-permute-done((bf16[1024,1024]{1,0:T(8,128)(2,1)}, bf16[1024,1024]{1,0:T(8,128)(2,1)S(1)}, u32[]{:S(2)}, u32[]{:S(2)}) %collective-permute-start.2) | collective-permute-done | bytes 2097184 | tf_op jit(solution)/shard_map/ppermute | solution.py:34
  104.6 3.9 %add_convert_fusion = bf16[1024,1024]{1,0:T(8,128)(2,1)} fusion(bf16[1024,1024]{1,0:T(8,128)(2,1)S(1)} %collective-permute-done.2, bf16[1024,1024]{1,0:T(8,128)(2,1)} %get-tuple-element.24), kind=kLoop, calls=%fused_computation | loop fusion | flops 4194304 | bytes 6291456 | tf_op jit(solution)/shard_map/convert_element_type | solution.py:319
  108.5 6.1 %all-to-all-start.1 = ((bf16[64,16,1024]{2,1,0:T(8,128)(2,1)}), bf16[64,16,1024]{2,1,0:T(8,128)(2,1)}, u32[]{:S(2)}, u32[]{:S(2)}) async-start(bf16[64,16,1024]{2,1,0:T(8,128)(2,1)} %bitcast.48), calls=%async_computation.1 | async-start | bytes 4194304 | tf_op jit(solution)/shard_map/all_to_all | solution.py:38
  114.6 3.4 %collective-permute-start.5 = (bf16[2,2,512]{2,1,0:T(2,128)(2,1)S(1)}, bf16[2,2,512]{2,1,0:T(2,128)(2,1)S(1)}, u32[]{:S(2)}, u32[]{:S(2)}) collective-permute-start(bf16[2,2,512]{2,1,0:T(2,128)(2,1)S(1)} %pad_maximum_fusion.5), channel_id=1, source_target_pairs={{0,2},{2,4},{4,6},{6,8},{8,10},{10,12},{12,14},{14,16},{16,18},{18... | collective-permute-start | bytes 12296 | tf_op jit(solution)/shard_map/ppermute | solution.py:44
  118.1 26.8 %all-to-all-done.1 = bf16[64,16,1024]{2,1,0:T(8,128)(2,1)} async-done(((bf16[64,16,1024]{2,1,0:T(8,128)(2,1)}), bf16[64,16,1024]{2,1,0:T(8,128)(2,1)}, u32[]{:S(2)}, u32[]{:S(2)}) %all-to-all-start.1) | async-done | bytes 2097184 | tf_op jit(solution)/shard_map/all_to_all | solution.py:38
  144.9 2.6 %fusion.7 = (f32[256]{0:T(256)S(1)}, f32[256,1024]{1,0:T(8,128)S(1)}) fusion(bf16[256,1024]{1,0:T(8,128)(2,1)S(1)} %copy-done.1, f32[1024]{0:T(1024)S(1)} %copy-done.12, bf16[1024,256]{1,0:T(8,128)(2,1)} %get-tuple-element.22, bf16[1024,1024]{1,0:T(8,128)(2,1)} %bitcast.11), kind=kOutput, calls=%fused_computation.13 | convolution fusion | flops 537919232 | bytes 4199424 | tf_op jit(solution)/shard_map/dot_general | solution.py:26
  152.1 2.9 %multiply_convert_fusion = (bf16[256,512]{1,0:T(8,128)(2,1)}, f32[256,512]{1,0:T(8,128)S(1)}, f32[256,512]{1,0:T(8,128)S(1)}) fusion(f32[256,512]{1,0:T(8,128)} %convert_multiply_fusion.3, f32[512]{0:T(512)S(1)} %bitcast.54, f32[2,512]{1,0:T(2,128)S(1)} %multiply_bitcast_fusion, f32[512]{0:T(512)S(1)} %bitcast.56, f32[512]{0:T(512)S(1)} %bitcast.52, ...), kind=kOutput, calls=%fused_computation.44 | convolution fusion | flops 270008320 | bytes 4204548 | tf_op jit(solution)/shard_map/dot_general | solution.py:18
  156.6 1.7 collective-permute-start.7
  159.3 5.0 %all-to-all-start.2 = ((bf16[4,128,512]{2,1,0:T(8,128)(2,1)}), bf16[4,128,512]{2,1,0:T(8,128)(2,1)}, u32[]{:S(2)}, u32[]{:S(2)}) async-start(bf16[4,128,512]{2,1,0:T(8,128)(2,1)} %pad_maximum_fusion.4), calls=%async_computation.2 | async-start | bytes 1048576 | tf_op jit(solution)/shard_map/all_to_all | solution.py:38
  165.6 2.0 collective-permute-done.7
  167.6 4.6 %collective-permute-done.6 = bf16[256,512]{1,0:T(8,128)(2,1)} collective-permute-done((bf16[256,512]{1,0:T(8,128)(2,1)}, bf16[256,512]{1,0:T(8,128)(2,1)}, u32[]{:S(2)}, u32[]{:S(2)}) %collective-permute-start.6) | collective-permute-done | bytes 262176 | tf_op jit(solution)/shard_map/ppermute | solution.py:49
  172.2 1.3 pad_maximum_fusion
  173.6 4.2 %all-to-all-done.2 = bf16[4,128,512]{2,1,0:T(8,128)(2,1)} async-done(((bf16[4,128,512]{2,1,0:T(8,128)(2,1)}), bf16[4,128,512]{2,1,0:T(8,128)(2,1)}, u32[]{:S(2)}, u32[]{:S(2)}) %all-to-all-start.2) | async-done | bytes 524320 | tf_op jit(solution)/shard_map/all_to_all | solution.py:38
  178.1 1.5 convolution_bitcast_fusion
  179.9 1.5 convolution_add_fusion
  181.4 4.0 %all-to-all-start.3 = ((f32[16,32,512]{2,1,0:T(8,128)}), f32[16,32,512]{2,1,0:T(8,128)S(1)}, u32[]{:S(2)}, u32[]{:S(2)}) async-start(f32[16,32,512]{2,1,0:T(8,128)} %bitcast.29), calls=%async_computation.3 | async-start | bytes 2097152 | tf_op jit(solution)/shard_map/all_to_all | solution.py:38
  185.4 14.6 %weight_grads.1 = (f32[2048,512]{1,0:T(8,128)}, f32[2048,512]{1,0:T(8,128)}, f32[512,2048]{1,0:T(8,128)}) custom-call(s32[1]{0:T(128)} %bitcast.4.core_ref, bf16[1024,2048]{1,0:T(8,128)(2,1)} %bitcast.6.own_ref.own_x.own_y, bf16[1024,2048]{1,0:T(8,128)(2,1)} %bitcast.6.own_ref.own_x.own_y, bf16[1024,2048]{1,0:T(8,128)(2,1)} %collective-permute-done.1.peer_ref.peer_x.peer_y, ...), custom_call_target="tpu_custom_call" | custom-call | flops 6442450944 | bytes 12582912 | tf_op jit(solution)/shard_map/weight_grads/pallas_call | solution.py:236
  201.7 1.5 all-to-all-done.3
  (63 shorter events, 12.7 us)
Async XLA Ops:
  0.6 149.0 %copy-start = (bf16[2048,512]{1,0:T(8,128)(2,1)S(1)}, bf16[2048,512]{1,0:T(8,128)(2,1)}, u32[]{:S(2)}) copy-start(bf16[2048,512]{1,0:T(8,128)(2,1)} %param.22) | copy-start | bytes 6291460
  2.9 1.4 collective-permute-start
  76.0 7.5 %collective-permute-start.1 = (bf16[1024,2048]{1,0:T(8,128)(2,1)}, bf16[1024,2048]{1,0:T(8,128)(2,1)}, u32[]{:S(2)}, u32[]{:S(2)}) collective-permute-start(bf16[1024,2048]{1,0:T(8,128)(2,1)} %bitcast.6.own_ref.own_x.own_y), channel_id=1, source_target_pairs={{0,1},{1,0},{2,3},{3,2},{4,5},{5,4},{6,7},{7,6},{8,9},{9,8},{10,11... | collective-permute-start | bytes 12582920 | tf_op jit(solution)/shard_map/ppermute | solution.py:34
  100.2 4.4 %collective-permute-start.2 = (bf16[1024,1024]{1,0:T(8,128)(2,1)}, bf16[1024,1024]{1,0:T(8,128)(2,1)S(1)}, u32[]{:S(2)}, u32[]{:S(2)}) collective-permute-start(bf16[1024,1024]{1,0:T(8,128)(2,1)} %get-tuple-element.25), channel_id=1, source_target_pairs={{0,1},{1,0},{2,3},{3,2},{4,5},{5,4},{6,7},{7,6},{8,9},{9,8},{10,11... | collective-permute-start | bytes 6291464 | tf_op jit(solution)/shard_map/ppermute | solution.py:34
  108.5 6.1 %copy-start.7 = (bf16[256,512]{1,0:T(8,128)(2,1)S(1)}, bf16[256,512]{1,0:T(8,128)(2,1)}, u32[]{:S(2)}) copy-start(bf16[256,512]{1,0:T(8,128)(2,1)} %param.18) | copy-start | bytes 786436
  108.5 6.1 %copy-start.8 = (bf16[256,512]{1,0:T(8,128)(2,1)S(1)}, bf16[256,512]{1,0:T(8,128)(2,1)}, u32[]{:S(2)}) copy-start(bf16[256,512]{1,0:T(8,128)(2,1)} %param.20) | copy-start | bytes 786436
  108.5 36.4 %copy-start.1 = (bf16[256,1024]{1,0:T(8,128)(2,1)S(1)}, bf16[256,1024]{1,0:T(8,128)(2,1)}, u32[]{:S(2)}) copy-start(bf16[256,1024]{1,0:T(8,128)(2,1)} %stream_ref.1) | copy-start | bytes 1572868
  108.5 36.4 %copy-start.12 = (f32[1024]{0:T(1024)S(1)}, f32[1024]{0:T(1024)}, u32[]{:S(2)}) copy-start(f32[1024]{0:T(1024)} %param.14) | copy-start | bytes 12292
  108.5 36.4 %all-to-all-start.1 = ((bf16[64,16,1024]{2,1,0:T(8,128)(2,1)}), bf16[64,16,1024]{2,1,0:T(8,128)(2,1)}, u32[]{:S(2)}, u32[]{:S(2)}) async-start(bf16[64,16,1024]{2,1,0:T(8,128)(2,1)} %bitcast.48), calls=%async_computation.1 | async-start | bytes 4194304 | tf_op jit(solution)/shard_map/all_to_all | solution.py:38
  114.6 35.0 %collective-permute-start.5 = (bf16[2,2,512]{2,1,0:T(2,128)(2,1)S(1)}, bf16[2,2,512]{2,1,0:T(2,128)(2,1)S(1)}, u32[]{:S(2)}, u32[]{:S(2)}) collective-permute-start(bf16[2,2,512]{2,1,0:T(2,128)(2,1)S(1)} %pad_maximum_fusion.5), channel_id=1, source_target_pairs={{0,2},{2,4},{4,6},{6,8},{8,10},{10,12},{12,14},{14,16},{16,18},{18... | collective-permute-start | bytes 12296 | tf_op jit(solution)/shard_map/ppermute | solution.py:44
  147.5 1.2 collective-permute-start.3
  149.3 9.0 %copy-start.2 = (bf16[256,1024]{1,0:T(8,128)(2,1)}, bf16[256,1024]{1,0:T(8,128)(2,1)S(1)}, u32[]{:S(2)}) copy-start(bf16[256,1024]{1,0:T(8,128)(2,1)S(1)} %fusion.5) | copy-start | bytes 1572868
  149.3 2.0 collective-permute-start.4
  152.1 6.2 %copy-start.6 = (bf16[256,1024]{1,0:T(8,128)(2,1)S(1)}, bf16[256,1024]{1,0:T(8,128)(2,1)}, u32[]{:S(2)}) copy-start(bf16[256,1024]{1,0:T(8,128)(2,1)} %copy-done.5) | copy-start | bytes 1572868
  155.0 9.3 %copy-start.3 = (f32[256,512]{1,0:T(8,128)}, f32[256,512]{1,0:T(8,128)S(1)}, u32[]{:S(2)}) copy-start(f32[256,512]{1,0:T(8,128)S(1)} %get-tuple-element.44) | copy-start | bytes 1572868
  155.9 9.8 %collective-permute-start.8 = (bf16[256,512]{1,0:T(8,128)(2,1)}, bf16[256,512]{1,0:T(8,128)(2,1)}, u32[]{:S(2)}, u32[]{:S(2)}) collective-permute-start(bf16[256,512]{1,0:T(8,128)(2,1)} %fusion.19), channel_id=1, source_target_pairs={{0,96},{32,0},{64,32},{96,64},{1,97},{33,1},{65,33},{97,65},{2,98}... | collective-permute-start | bytes 786440 | tf_op jit(solution)/shard_map/ppermute | solution.py:49
  156.6 11.0 %collective-permute-start.7 = (bf16[256,512]{1,0:T(8,128)(2,1)}, bf16[256,512]{1,0:T(8,128)(2,1)}, u32[]{:S(2)}, u32[]{:S(2)}) collective-permute-start(bf16[256,512]{1,0:T(8,128)(2,1)} %fusion.19), channel_id=1, source_target_pairs={{0,64},{32,96},{64,0},{96,32},{1,65},{33,97},{65,1},{97,33},{2,66}... | collective-permute-start | bytes 786440 | tf_op jit(solution)/shard_map/ppermute | solution.py:49
  158.2 14.0 %collective-permute-start.6 = (bf16[256,512]{1,0:T(8,128)(2,1)}, bf16[256,512]{1,0:T(8,128)(2,1)}, u32[]{:S(2)}, u32[]{:S(2)}) collective-permute-start(bf16[256,512]{1,0:T(8,128)(2,1)} %fusion.19), channel_id=1, source_target_pairs={{0,32},{32,64},{64,96},{96,0},{1,33},{33,65},{65,97},{97,1},{2,34}... | collective-permute-start | bytes 786440 | tf_op jit(solution)/shard_map/ppermute | solution.py:49
  159.3 18.5 %all-to-all-start.2 = ((bf16[4,128,512]{2,1,0:T(8,128)(2,1)}), bf16[4,128,512]{2,1,0:T(8,128)(2,1)}, u32[]{:S(2)}, u32[]{:S(2)}) async-start(bf16[4,128,512]{2,1,0:T(8,128)(2,1)} %pad_maximum_fusion.4), calls=%async_computation.2 | async-start | bytes 1048576 | tf_op jit(solution)/shard_map/all_to_all | solution.py:38
  164.3 35.7 %collective-permute-start.10 = (f32[2,512]{1,0:T(2,128)S(1)}, f32[2,512]{1,0:T(2,128)S(1)}, u32[]{:S(2)}, u32[]{:S(2)}) collective-permute-start(f32[2,512]{1,0:T(2,128)S(1)} %slice.75), channel_id=1, source_target_pairs={{2,0},{4,2},{6,4},{8,6},{10,8},{12,10},{14,12},{16,14},{18,16},{20... | collective-permute-start | bytes 12296 | tf_op jit(solution)/shard_map/ppermute | solution.py:44
  177.8 2.1 %collective-permute-start.9 = (bf16[512,512]{1,0:T(8,128)(2,1)}, bf16[512,512]{1,0:T(8,128)(2,1)S(1)}, u32[]{:S(2)}, u32[]{:S(2)}) collective-permute-start(bf16[512,512]{1,0:T(8,128)(2,1)} %bitcast.27), channel_id=1, source_target_pairs={{0,1},{1,0},{2,3},{3,2},{4,5},{5,4},{6,7},{7,6},{8,9},{9,8},{10,11... | collective-permute-start | bytes 1572872 | tf_op jit(solution)/shard_map/ppermute | solution.py:34
  181.4 21.8 %all-to-all-start.3 = ((f32[16,32,512]{2,1,0:T(8,128)}), f32[16,32,512]{2,1,0:T(8,128)S(1)}, u32[]{:S(2)}, u32[]{:S(2)}) async-start(f32[16,32,512]{2,1,0:T(8,128)} %bitcast.29), calls=%async_computation.3 | async-start | bytes 2097152 | tf_op jit(solution)/shard_map/all_to_all | solution.py:38
  185.4 14.6 %copy-start.4 = (f32[256,512]{1,0:T(8,128)S(1)}, f32[256,512]{1,0:T(8,128)}, u32[]{:S(2)}) copy-start(f32[256,512]{1,0:T(8,128)} %copy-done.3) | copy-start | bytes 1572868
  185.4 15.5 %copy-start.9 = (bf16[256,512]{1,0:T(8,128)(2,1)S(1)}, bf16[256,512]{1,0:T(8,128)(2,1)}, u32[]{:S(2)}) copy-start(bf16[256,512]{1,0:T(8,128)(2,1)} %param.20) | copy-start | bytes 786436
  (4 other events, 9.2 us)

commit v2 on v1

--- a/solution.py
+++ b/solution.py
@@ -6,10 +6,12 @@
 from jax.sharding import Mesh
 from jax.sharding import PartitionSpec as P
 
+
 D = 2048
 SP = ("sp_0", "sp_1", "sp_2")
 EPSILON = 1e-06
 VMEM = 56 * 1024 * 1024
+EXPERT_BLOCKS = 2
 F32 = jnp.float32
 BF16 = jnp.bfloat16
 
@@ -110,14 +112,14 @@
 
 def build_rows(target, weights, total, stream, cot, gain, slots):
     tokens, width = stream.shape
-    rows = slots // 8
+    rows = slots // 4
 
     def whole(*shape):
         return pl.BlockSpec(shape, lambda i: (0, 0))
 
     return pl.pallas_call(
         rows_body,
-        grid=(8,),
+        grid=(4,),
         in_specs=[
             whole(2, tokens),
             whole(2, tokens),
@@ -139,58 +141,162 @@
     )(target, weights, total, stream, cot, gain)
 
 
-def expert_body(
-    core_ref, own_ref, peer_ref, gate_own, gate_peer, up_own, up_peer, down_own, down_peer,
-    hidden_ref, gate_ref, up_ref, mine_ref, theirs_ref,
+def load_body(core_ref, gate_ref, up_ref, down_ref, *refs):
+    outs, sems = refs[:6], refs[6]
+    width = outs[0].shape[0]
+    mine = pl.multiple_of(core_ref[0] * width, width)
+    other = pl.multiple_of((1 - core_ref[0]) * width, width)
+    sources = (
+        gate_ref.at[pl.ds(mine, width), :],
+        gate_ref.at[pl.ds(other, width), :],
+        up_ref.at[pl.ds(mine, width), :],
+        up_ref.at[pl.ds(other, width), :],
+        down_ref.at[:, pl.ds(mine, width)],
+        down_ref.at[:, pl.ds(other, width)],
+    )
+    copies = [
+        pltpu.make_async_copy(source, outs[i], sems.at[i]) for i, source in enumerate(sources)
+    ]
+    for copy in copies:
+        copy.start()
+    for copy in copies:
+        copy.wait()
+
+
+def own_body(own_ref, gate_w, up_w, down_w, gate_out, up_out, hidden_out):
+    rows, double = own_ref.shape
+    width = double // 2
+    step = rows // EXPERT_BLOCKS
+
+    def block(i, carry):
+        at = pl.ds(i * step, step)
+        x, y = own_ref[at, :width], own_ref[at, width:]
+        gate_out[at, :] = dot_nn(x, gate_w[...])
+        up_out[at, :] = dot_nn(x, up_w[...])
+        hidden_out[at, :] = dot_nt(y, down_w[...])
+        return carry
+
+    lax.fori_loop(0, EXPERT_BLOCKS, block, 0)
+
+
+def peer_body(
+    peer_ref, gate_w, up_w, down_w, gate_in, up_in, grad_in,
+    hidden_ref, gate_ref, up_ref, theirs_ref,
 ):
-    width = gate_own.shape[0]
-    own_x, own_y = own_ref[:, :width], own_ref[:, width:]
-    peer_x, peer_y = peer_ref[:, :width], peer_ref[:, width:]
-    gate_lin = dot_nn(own_x, gate_own[...]) + dot_nn(peer_x, gate_peer[...])
-    up_lin = dot_nn(own_x, up_own[...]) + dot_nn(peer_x, up_peer[...])
-    hidden_grad = dot_nt(own_y, down_own[...]) + dot_nt(peer_y, down_peer[...])
-    sig = jax.nn.sigmoid(gate_lin)
-    silu = gate_lin * sig
-    hidden_ref[...] = (silu * up_lin).astype(BF16)
-    gate_pre = (hidden_grad * up_lin * sig * (1.0 + gate_lin * (1.0 - sig))).astype(BF16)
-    up_pre = (hidden_grad * silu).astype(BF16)
-    gate_ref[...] = gate_pre
-    up_ref[...] = up_pre
-    mine_ref[...] = (dot_nt(gate_pre, gate_own[...]) + dot_nt(up_pre, up_own[...])).astype(BF16)
-    theirs_ref[...] = (dot_nt(gate_pre, gate_peer[...]) + dot_nt(up_pre, up_peer[...])).astype(BF16)
-
-
-def expert_rows(core, own, peer, gate_w, up_w, down_w):
-    rows, double = own.shape
+    rows, double = peer_ref.shape
     width = double // 2
-    units = gate_w.shape[1]
-    step = 256
-
-    def block(n):
-        return pl.BlockSpec((step, n), lambda i, c: (i, 0))
-
-    tall_own = pl.BlockSpec((width, units), lambda i, c: (c[0], 0))
-    tall_peer = pl.BlockSpec((width, units), lambda i, c: (1 - c[0], 0))
-    wide_own = pl.BlockSpec((units, width), lambda i, c: (0, c[0]))
-    wide_peer = pl.BlockSpec((units, width), lambda i, c: (0, 1 - c[0]))
-    narrow = jax.ShapeDtypeStruct((rows, units), BF16)
-    broad = jax.ShapeDtypeStruct((rows, width), BF16)
+    step = rows // EXPERT_BLOCKS
+
+    def block(i, carry):
+        at = pl.ds(i * step, step)
+        x, y = peer_ref[at, :width], peer_ref[at, width:]
+        gate_lin = gate_in[at, :] + dot_nn(x, gate_w[...])
+        up_lin = up_in[at, :] + dot_nn(x, up_w[...])
+        hidden_grad = grad_in[at, :] + dot_nt(y, down_w[...])
+        sig = jax.nn.sigmoid(gate_lin)
+        silu = gate_lin * sig
+        hidden_ref[at, :] = (silu * up_lin).astype(BF16)
+        gate_pre = (hidden_grad * up_lin * sig * (1.0 + gate_lin * (1.0 - sig))).astype(BF16)
+        up_pre = (hidden_grad * silu).astype(BF16)
+        gate_ref[at, :] = gate_pre
+        up_ref[at, :] = up_pre
+        theirs_ref[at, :] = (dot_nt(gate_pre, gate_w[...]) + dot_nt(up_pre, up_w[...])).astype(BF16)
+        return carry
+
+    lax.fori_loop(0, EXPERT_BLOCKS, block, 0)
+
+
+def mine_body(gate_ref, up_ref, gate_w, up_w, mine_ref):
+    step = mine_ref.shape[0] // EXPERT_BLOCKS
+
+    def block(i, carry):
+        at = pl.ds(i * step, step)
+        part = dot_nt(gate_ref[at, :], gate_w[...]) + dot_nt(up_ref[at, :], up_w[...])
+        mine_ref[at, :] = part.astype(BF16)
+        return carry
+
+    lax.fori_loop(0, EXPERT_BLOCKS, block, 0)
+
+
+def add_body(mine_ref, other_ref, out_ref, scratch, sems):
+    blocks, step, _ = scratch.shape
+    copies = []
+    for i in range(blocks):
+        at = pl.ds(i * step, step)
+        total = mine_ref[at, :].astype(F32) + other_ref[at, :].astype(F32)
+        scratch[i] = total.astype(BF16)
+        copies.append(pltpu.make_async_copy(scratch.at[i], out_ref.at[at, :], sems.at[i]))
+        copies[-1].start()
+    for copy in copies:
+        copy.wait()
+
+
+IN_VMEM = pl.BlockSpec(memory_space=pltpu.VMEM)
+
+
+def on_chip(body, outs, flops, limit, *args):
     return pl.pallas_call(
-        expert_body,
-        grid_spec=pltpu.PrefetchScalarGridSpec(
-            num_scalar_prefetch=1,
-            grid=(rows // step,),
-            in_specs=[
-                block(double), block(double),
-                tall_own, tall_peer, tall_own, tall_peer, wide_own, wide_peer,
-            ],
-            out_specs=[block(units), block(units), block(units), block(width), block(width)],
-        ),
-        out_shape=[narrow, narrow, narrow, broad, broad],
-        compiler_params=pltpu.CompilerParams(vmem_limit_bytes=VMEM),
-        name="expert_rows",
-        cost_estimate=cost(20 * rows * width * units, 20 * rows * width),
-    )(core, own, peer, gate_w, gate_w, up_w, up_w, down_w, down_w)
+        body,
+        in_specs=[IN_VMEM] * len(args),
+        out_specs=[IN_VMEM] * len(outs),
+        out_shape=[jax.ShapeDtypeStruct(s, d) for s, d in outs],
+        compiler_params=pltpu.CompilerParams(vmem_limit_bytes=limit * 1024 * 1024),
+        cost_estimate=cost(flops, 16 * 1024 * 1024),
+    )(*args)
+
+
+def load_weights(core, gate_w, up_w, down_w):
+    double, units = gate_w.shape
+    width = double // 2
+    shapes = [(width, units)] * 4 + [(units, width)] * 2
+    return pl.pallas_call(
+        load_body,
+        in_specs=[pl.BlockSpec(memory_space=pltpu.SMEM)] + [pl.BlockSpec(memory_space=pl.ANY)] * 3,
+        out_specs=[IN_VMEM] * 6,
+        out_shape=[jax.ShapeDtypeStruct(s, BF16) for s in shapes],
+        scratch_shapes=[pltpu.SemaphoreType.DMA((6,))],
+        name="load_weights",
+        cost_estimate=cost(10**9, 6 * double * units),
+    )(core, gate_w, up_w, down_w)
+
+
+def expert_own(own, gate_w, up_w, down_w):
+    rows, units = own.shape[0], gate_w.shape[1]
+    outs = [((rows, units), F32)] * 3
+    flops = 3 * rows * own.shape[1] * units
+    return on_chip(own_body, outs, flops, 8, own, gate_w, up_w, down_w)
+
+
+def expert_peer(peer, gate_w, up_w, down_w, *parts):
+    rows, units = peer.shape[0], gate_w.shape[1]
+    outs = [((rows, units), BF16)] * 3 + [((rows, peer.shape[1] // 2), BF16)]
+    flops = 5 * rows * peer.shape[1] * units
+    return on_chip(peer_body, outs, flops, 16, peer, gate_w, up_w, down_w, *parts)
+
+
+def expert_mine(gate_pre, up_pre, gate_w, up_w):
+    rows, width = gate_pre.shape[0], gate_w.shape[0]
+    flops = 4 * rows * width * gate_w.shape[1]
+    outs = [((rows, width), BF16)]
+    return on_chip(mine_body, outs, flops, 8, gate_pre, up_pre, gate_w, up_w)[0]
+
+
+def add_parts(mine, other):
+    rows, width = mine.shape
+    blocks = 8
+    return pl.pallas_call(
+        add_body,
+        in_specs=[IN_VMEM] * 2,
+        out_specs=pl.BlockSpec(memory_space=pltpu.HBM),
+        out_shape=jax.ShapeDtypeStruct(mine.shape, BF16),
+        scratch_shapes=[
+            pltpu.VMEM((blocks, rows // blocks, width), BF16),
+            pltpu.SemaphoreType.DMA((blocks,)),
+        ],
+        compiler_params=pltpu.CompilerParams(vmem_limit_bytes=8 * 1024 * 1024),
+        name="add_parts",
+        cost_estimate=cost(mine.size, 6 * mine.size),
+    )(mine, other)
 
 
 def weights_body(
@@ -252,7 +358,7 @@
     )(core, own, own, peer, peer, hidden, gate_pre, up_pre)
 
 
-def local(
+def stage(
     stream,
     norm_gain,
     cotangent,
@@ -296,29 +402,40 @@
         + conv_taps[2][None, :] * extended[2:]
     )
     mixer_out = (bgate_float * conv_out).astype(BF16)
+    weights = load_weights(core_arg, gate_weight[0], up_weight[0], down_weight[0])
+    own, mixer_out, weights = lax.optimization_barrier((own, mixer_out, weights))
+    gate_own, gate_peer, up_own, up_peer, down_own, down_peer = weights
     line = lax.axis_size("sp_0")
     spot = lax.axis_index("sp_0")
-    around = jnp.stack([mixer_out] + [turned(mixer_out, "sp_0", s) for s in range(1, line)])
+    token_half = tok_count // 2
+    channels = mixer_out.shape[1]
+
+    def half_of(array, which, dim):
+        return lax.dynamic_slice_in_dim(array, which * token_half, token_half, dim)
+
+    peer = swap(own)
+    around = [mixer_out]
+    for step in range(1, line):
+        around.append(turned(mixer_out, "sp_0", step))
+    parts = expert_own(own, gate_own, up_own, down_own)
+    hidden, gate_pre, up_pre, part_theirs = expert_peer(
+        peer, gate_peer, up_peer, down_peer, *parts
+    )
+    other = swap(part_theirs)
+    part_mine = expert_mine(gate_pre, up_pre, gate_own, up_own)
+    row_grads = add_parts(part_mine, other)
+    row_grads, around = lax.optimization_barrier((row_grads, around))
+    returned = exchange(row_grads.reshape(experts, capacity, width), SP).reshape(slots, width)
+    grads_w = weight_grads(core_arg, own, peer, hidden, gate_pre, up_pre)
+    around = jnp.stack(around)
     mixers = jnp.concatenate(
         [lax.dynamic_slice_in_dim(around, (spot - k) % line, 1, 0) for k in range(line)], axis=0
     )
-    token_half = tok_count // 2
-    channels = mixer_out.shape[1]
-
-    def half_of(array, which, dim):
-        return lax.dynamic_slice_in_dim(array, which * token_half, token_half, dim)
-
     mixers_mine = half_of(mixers, core, 1).reshape(line * token_half, channels)
     mixers_theirs = half_of(mixers, 1 - core, 1).reshape(line * token_half, channels)
-
-    peer = swap(own)
-    hidden, gate_pre, up_pre, part_mine, part_theirs = expert_rows(
-        core_arg, own, peer, gate_weight[0], up_weight[0], down_weight[0]
-    )
-    other = swap(part_theirs)
-    row_grads = (part_mine.astype(F32) + other.astype(F32)).astype(BF16)
-    returned = exchange(row_grads.reshape(experts, capacity, width), SP).reshape(slots, width)
-    gate_g, up_g, down_g = weight_grads(core_arg, own, peer, hidden, gate_pre, up_pre)
+    returned, (gate_g, up_g, down_g), mixers_mine, mixers_theirs = lax.optimization_barrier(
+        (returned, grads_w, mixers_mine, mixers_theirs)
+    )
 
     normed_grad = dot_tn(selector, returned)
     stream_float = stream.astype(F32)
@@ -342,13 +459,14 @@
     grads_mine = exchange(sent, "sp_0").reshape(line * token_half, quarter)
     grads_theirs = swap(grads_mine)
     proj_part = dot_tn(grads_mine, mixers_mine) + dot_tn(grads_theirs, mixers_theirs)
+    late_grad, late_peer, proj_part = lax.optimization_barrier((stream_grad, grad_peer, proj_part))
     plane = lax.axis_size(("sp_1", "sp_2"))
     arrived = exchange(proj_part.reshape(plane, quarter // plane, channels), ("sp_1", "sp_2"))
     proj_grad = arrived.sum(axis=0)
 
     proj_mine = lax.dynamic_slice_in_dim(out_proj, core * width, width, 0)
     proj_peer = lax.dynamic_slice_in_dim(out_proj, (1 - core) * width, width, 0)
-    mixer_grad = dot_nn(stream_grad, proj_mine) + dot_nn(grad_peer, proj_peer)
+    mixer_grad = dot_nn(late_grad, proj_mine) + dot_nn(late_peer, proj_peer)
     delta = mixer_grad * bgate_float
     next_rim = shifted(delta[:2], SP, -1)
     extended_back = jnp.concatenate([delta, next_rim], axis=0)
@@ -375,7 +493,7 @@
 def solution(mesh):
     finer = Mesh(mesh.devices.reshape(4, 4, 4, mesh.shape["tp"]), ("sp_0", "sp_1", "sp_2", "tp"))
     return jax.shard_map(
-        local,
+        stage,
         mesh=finer,
         in_specs=(
             P(SP, "tp"),

time: 205 us -> 196 us (0.956)
  blocking collectives: 64.5 us -> 12.5 us
  waiting for transfers between devices: 54.1 us -> 81.4 us
  starting transfers between devices: 22.7 us -> 35.3 us
  other arithmetic: 12.2 us -> 5.63 us
  local copies, waits for them, and re-layouts: 1.03 us -> 7.08 us
  Pallas kernels: 39.5 us -> 42.5 us
    all_to_all x1, blocking collectives: 64.5 us -> 12.5 us  [exchange(): return lax.all_to_all(value, axis, split_axis=0, concat_axis=0, tiled=True)]
    ppermute x2, waiting for transfers between devices: 0.01 us -> 46.6 us  [shifted(): lax.ppermute(value, axis, [(source, source + steps) for source in range(l...]
    all_to_all x3, starting transfers between devices: 15.1 us -> 25.7 us  [exchange(): return lax.all_to_all(value, axis, split_axis=0, concat_axis=0, tiled=True)]
    ppermute x6, waiting for transfers between devices: 14.9 us -> 4.67 us  [swap(): return lax.ppermute(value, 'tp', [(0, 1), (1, 0)])]
    all_to_all x3, waiting for transfers between devices: 32.6 us -> 23.1 us  [exchange(): return lax.all_to_all(value, axis, split_axis=0, concat_axis=0, tiled=True)]
    unnamed x28 -> x52, local copies, waits for them, and re-layouts: 0.86 us -> 5.85 us
    convert_element_type x5 -> x4, other arithmetic: 6.89 us -> 3.15 us  [the longest x1 0.99 us: stage(): mixer_out = (bgate_float * conv_out).astype(BF16)]
    pallas_call x2 -> x6, Pallas kernels: 22.7 us -> 25.8 us  [the longest x3 14.8 us: on_chip(): pl.pallas_call(body, in_specs=[IN_VMEM] * len(args), out_specs=[IN_VMEM]...]
  transfers between devices with their start and end apart: 14 -> 14, of which waited for: 11 -> 12; matrix products, arithmetic and copies ran while one was open for 6% -> 4% of each run, Pallas kernels for 7% -> 15%
where the time goes in v2:
time: 196 us; the launch traced here: 195 us
  waiting for transfers between devices  81.4 us (42%)
  Pallas kernels  42.5 us (22%)
  starting transfers between devices  35.3 us (18%)
  blocking collectives  12.5 us (6%)
  matrix products  9.23 us (5%)
  local copies, waits for them, and re-layouts  7.08 us (4%)
  other arithmetic  5.63 us (3%)
    ppermute x2, waiting for transfers between devices, shifted(): lax.ppermute(value, axis, [(source, source + steps) for source in range(l...  46.6 us
    all_to_all x3, starting transfers between devices, exchange(): return lax.all_to_all(value, axis, split_axis=0, concat_axis=0, tiled=True)  25.7 us
    all_to_all x3, waiting for transfers between devices, exchange(): return lax.all_to_all(value, axis, split_axis=0, concat_axis=0, tiled=True)  23.1 us
    pallas_call x3, Pallas kernels, on_chip(): pl.pallas_call(body, in_specs=[IN_VMEM] * len(args), out_specs=[IN_VMEM]...  14.8 us
    pallas_call x1, Pallas kernels, weight_grads(): pl.pallas_call(weights_body, grid_spec=pltpu.PrefetchScalarGridSpec(num_s...  14.5 us
    all_to_all x1, blocking collectives, exchange(): return lax.all_to_all(value, axis, split_axis=0, concat_axis=0, tiled=True)  12.5 us
    ppermute x3, waiting for transfers between devices, turned(): lax.ppermute(value, axis, [(i, (i + steps) % count) for i in range(count)])  7.01 us
    dot_general x3, matrix products, dot_tn(): lax.dot_general(a, b, (((0,), (0,)), ((), ())), preferred_element_type=F32)  6.49 us
  transfers between devices with their start and end apart: 14, of which 12 were waited for; matrix products, arithmetic and copies ran while one was open for 4% of the time, Pallas kernels for 15%

profile of v2, /device:TPU:0, one launch (start us, length us, event | category | flops | bytes accessed | tf_op | source)
XLA Modules:
  0.0 194.8 jit_solution(8101763189974046077)
XLA Ops:
  0.6 2.2 %find_slots.1 = (f32[1,256]{1,0:T(1,128)}, s32[2,256]{1,0:T(2,128)}) custom-call(bf16[256,1024]{1,0:T(8,128)(2,1)} %stream_ref.1, s32[2,256]{1,0:T(2,128)} %bitcast.69), custom_call_target="tpu_custom_call" | custom-call | flops 100000000 | bytes 524288 | tf_op jit(solution)/shard_map/find_slots/pallas_call | solution.py:83
  5.5 4.7 %build_rows.1 = (bf16[1024,2048]{1,0:T(8,128)(2,1)}, bf16[1024,256]{1,0:T(8,128)(2,1)}) custom-call(s32[2,256]{1,0:T(2,128)} %get-tuple-element.51.target_ref, f32[2,256]{1,0:T(2,128)} %bitcast.70, f32[1,256]{1,0:T(1,128)} %get-tuple-element.95.total_ref, bf16[256,1024]{1,0:T(8,128)(2,1)} %stream_ref.1, bf16[256,1024]{1,0:T(8,128)(2,1)} %cot_ref.1, ...), custom_call_target="tpu_custom_call" | custom-call | flops 1073741824 | bytes 4194304 | tf_op jit(solution)/shard_map/build_rows/pallas_call | solution.py:120
  10.2 11.9 %all-to-all-start = ((bf16[64,16,2048]{2,1,0:T(8,128)(2,1)}), bf16[64,16,2048]{2,1,0:T(8,128)(2,1)}, u32[]{:S(2)}, u32[]{:S(2)}) async-start(bf16[64,16,2048]{2,1,0:T(8,128)(2,1)} %bitcast.49), calls=%async_computation | async-start | bytes 8388608 | tf_op jit(solution)/shard_map/all_to_all | solution.py:40
  22.2 3.4 %collective-permute-start.1 = (bf16[2,2,512]{2,1,0:T(2,128)(2,1)S(1)}, bf16[2,2,512]{2,1,0:T(2,128)(2,1)S(1)}, u32[]{:S(2)}, u32[]{:S(2)}) collective-permute-start(bf16[2,2,512]{2,1,0:T(2,128)(2,1)S(1)} %pad_maximum_fusion.5), channel_id=1, source_target_pairs={{0,2},{2,4},{4,6},{6,8},{8,10},{10,12},{12,14},{14,16},{16,18},{18... | collective-permute-start | bytes 12296 | tf_op jit(solution)/shard_map/ppermute | solution.py:46
  25.7 5.5 %load_weights.1 = (bf16[1024,512]{1,0:T(8,128)(2,1)}, bf16[1024,512]{1,0:T(8,128)(2,1)}, bf16[1024,512]{1,0:T(8,128)(2,1)}, bf16[1024,512]{1,0:T(8,128)(2,1)}, b...) custom-call(s32[1]{0:T(128)} %bitcast.12.core_ref, bf16[2048,512]{1,0:T(8,128)(2,1)} %bitcast.50, ...), custom_call_target="tpu_custom_call" | custom-call | flops 1000000000 | bytes 6291456 | tf_op jit(solution)/shard_map/load_weights/pallas_call | solution.py:252
  31.3 36.8 %collective-permute-done.1 = bf16[2,2,512]{2,1,0:T(2,128)(2,1)S(1)} collective-permute-done((bf16[2,2,512]{2,1,0:T(2,128)(2,1)S(1)}, bf16[2,2,512]{2,1,0:T(2,128)(2,1)S(1)}, u32[]{:S(2)}, u32[]{:S(2)}) %collective-permute-start.1) | collective-permute-done | bytes 4128 | tf_op jit(solution)/shard_map/ppermute | solution.py:46
  69.1 7.4 %all-to-all-done = bf16[64,16,2048]{2,1,0:T(8,128)(2,1)} async-done(((bf16[64,16,2048]{2,1,0:T(8,128)(2,1)}), bf16[64,16,2048]{2,1,0:T(8,128)(2,1)}, u32[]{:S(2)}, u32[]{:S(2)}) %all-to-all-start) | async-done | bytes 4194336 | tf_op jit(solution)/shard_map/all_to_all | solution.py:40
  80.2 5.9 %shard_map.188 = (f32[1024,512]{1,0:T(8,128)S(1)}, f32[1024,512]{1,0:T(8,128)S(1)}, f32[1024,512]{1,0:T(8,128)S(1)}) custom-call(bf16[1024,2048]{1,0:T(8,128)(2,1)} %bitcast.5.own_ref.own_x.own_y, bf16[1024,512]{1,0:T(8,128)(2,1)S(1)} %copy-done.3, bf16[1024,512]{1,0:T(8,128)(2,1)S(1)} %copy-done.4, bf16[512,1024]{1,0:T(8,128)(2,1)S(1)} %copy-done.8), custom_call_target="tpu_custom_call" | custom-call | flops 3221225472 | bytes 16777216 | tf_op jit(solution)/shard_map/pallas_call | solution.py:238
  86.2 6.3 %shard_map.189 = (bf16[1024,512]{1,0:T(8,128)(2,1)S(1)}, bf16[1024,512]{1,0:T(8,128)(2,1)S(1)}, bf16[1024,512]{1,0:T(8,128)(2,1)S(1)}, bf16[1024,1024]{1,0:T(8,128)(2,1)S(1)}) custom-call(bf16[1024,2048]{1,0:T(8,128)(2,1)S(1)} %collective-permute-done.2.peer_ref.peer_x.peer_y, bf16[1024,512]{1,0:T(8,128)(2,1)S(1)} %copy-done.5, ...), custom_call_target="tpu_custom_call" | custom-call | flops 5368709120 | bytes 16777216 | tf_op jit(solution)/shard_map/pallas_call | solution.py:238
  94.4 1.9 collective-permute-start.5
  97.1 2.6 %shard_map.190.mine_ref = bf16[1024,1024]{1,0:T(8,128)(2,1)S(1)} custom-call(bf16[1024,512]{1,0:T(8,128)(2,1)S(1)} %get-tuple-element.70.gate_ref, bf16[1024,512]{1,0:T(8,128)(2,1)S(1)} %get-tuple-element.71.up_ref, bf16[1024,512]{1,0:T(8,128)(2,1)S(1)} %copy-done.3, bf16[1024,512]{1,0:T(8,128)(2,1)S(1)} %copy-done.4), custom_call_target="tpu_custom_call" | custom-call | flops 2147483648 | bytes 16777216 | tf_op jit(solution)/shard_map/pallas_call | solution.py:238
  101.8 1.7 collective-permute-done.4
  103.5 4.7 %collective-permute-done.5 = bf16[256,512]{1,0:T(8,128)(2,1)S(1)} collective-permute-done((bf16[256,512]{1,0:T(8,128)(2,1)S(1)}, bf16[256,512]{1,0:T(8,128)(2,1)S(1)}, u32[]{:S(2)}, u32[]{:S(2)}) %collective-permute-start.5) | collective-permute-done | bytes 262176 | tf_op jit(solution)/shard_map/ppermute | solution.py:51
  108.9 9.9 %all-to-all-start.1 = ((bf16[64,16,1024]{2,1,0:T(8,128)(2,1)}), bf16[64,16,1024]{2,1,0:T(8,128)(2,1)}, u32[]{:S(2)}, u32[]{:S(2)}) async-start(bf16[64,16,1024]{2,1,0:T(8,128)(2,1)} %bitcast.48), calls=%async_computation.1 | async-start | bytes 4194304 | tf_op jit(solution)/shard_map/all_to_all | solution.py:40
  118.8 14.5 %weight_grads.1 = (f32[2048,512]{1,0:T(8,128)}, f32[2048,512]{1,0:T(8,128)}, f32[512,2048]{1,0:T(8,128)}) custom-call(s32[1]{0:T(128)} %bitcast.12.core_ref, bf16[1024,2048]{1,0:T(8,128)(2,1)} %bitcast.5.own_ref.own_x.own_y, bf16[1024,2048]{1,0:T(8,128)(2,1)} %bitcast.5.own_ref.own_x.own_y, bf16[1024,2048]{1,0:T(8,128)(2,1)} %copy-done.2, ...), custom_call_target="tpu_custom_call" | custom-call | flops 6442450944 | bytes 12582912 | tf_op jit(solution)/shard_map/weight_grads/pallas_call | solution.py:342
  134.9 13.5 %all-to-all-done.1 = bf16[64,16,1024]{2,1,0:T(8,128)(2,1)} async-done(((bf16[64,16,1024]{2,1,0:T(8,128)(2,1)}), bf16[64,16,1024]{2,1,0:T(8,128)(2,1)}, u32[]{:S(2)}, u32[]{:S(2)}) %all-to-all-start.1) | async-done | bytes 2097184 | tf_op jit(solution)/shard_map/all_to_all | solution.py:40
  148.4 2.5 %fusion.7 = (f32[256]{0:T(256)S(1)}, f32[256,1024]{1,0:T(8,128)S(1)}) fusion(bf16[256,1024]{1,0:T(8,128)(2,1)S(1)} %copy-done.12, f32[1024]{0:T(1024)S(1)} %copy-done.24, bf16[1024,256]{1,0:T(8,128)(2,1)S(1)} %copy-done.22, bf16[1024,1024]{1,0:T(8,128)(2,1)} %bitcast.17), kind=kOutput, calls=%fused_computation.11 | convolution fusion | flops 537919232 | bytes 4199424 | tf_op jit(solution)/shard_map/dot_general | solution.py:28
  152.9 1.7 collective-permute-done.8
  155.5 12.5 %all_to_all.20 = bf16[4,128,512]{2,1,0:T(8,128)(2,1)S(1)} all-to-all(bf16[4,128,512]{2,1,0:T(8,128)(2,1)S(1)} %pad_maximum_fusion.4), channel_id=1, replica_groups=mesh['sp_0'=4,'sp_1'=4,'sp_2'=4,'tp'=2] {'sp_0'}, dimensions={0} | all-to-all | bytes 1048576 | tf_op jit(solution)/shard_map/all_to_all | solution.py:40
  169.9 2.5 %convolution_add_fusion = f32[512,512]{1,0:T(8,128)} fusion(f32[512,512]{1,0:T(8,128)S(1)} %fusion.29, bf16[512,512]{1,0:T(8,128)(2,1)S(1)} %collective-permute-done.9, bf16[512,512]{1,0:T(8,128)(2,1)} %bitcast.55), kind=kOutput, calls=%fused_computation | convolution fusion | flops 268697600 | bytes 3145728 | tf_op jit(solution)/shard_map/dot_general | solution.py:28
  172.4 3.9 %all-to-all-start.3 = ((f32[16,32,512]{2,1,0:T(8,128)}), f32[16,32,512]{2,1,0:T(8,128)S(1)}, u32[]{:S(2)}, u32[]{:S(2)}) async-start(f32[16,32,512]{2,1,0:T(8,128)} %bitcast.29), calls=%async_computation.3 | async-start | bytes 2097152 | tf_op jit(solution)/shard_map/all_to_all | solution.py:40
  176.4 1.6 fusion.8
  180.5 9.8 %collective-permute-done.10 = f32[2,512]{1,0:T(2,128)S(1)} collective-permute-done((f32[2,512]{1,0:T(2,128)S(1)}, f32[2,512]{1,0:T(2,128)S(1)}, u32[]{:S(2)}, u32[]{:S(2)}) %collective-permute-start.10) | collective-permute-done | bytes 4128 | tf_op jit(solution)/shard_map/ppermute | solution.py:46
  191.9 2.2 %all-to-all-done.3 = f32[16,32,512]{2,1,0:T(8,128)S(1)} async-done(((f32[16,32,512]{2,1,0:T(8,128)}), f32[16,32,512]{2,1,0:T(8,128)S(1)}, u32[]{:S(2)}, u32[]{:S(2)}) %all-to-all-start.3) | async-done | bytes 1048608 | tf_op jit(solution)/shard_map/all_to_all | solution.py:40
  (91 shorter events, 23.9 us)
Async XLA Ops:
  0.6 175.7 %copy-start = (bf16[2048,512]{1,0:T(8,128)(2,1)S(1)}, bf16[2048,512]{1,0:T(8,128)(2,1)}, u32[]{:S(2)}) copy-start(bf16[2048,512]{1,0:T(8,128)(2,1)} %param.22) | copy-start | bytes 6291460
  2.9 1.4 collective-permute-start
  10.2 12.0 %copy-start.17 = (bf16[256,512]{1,0:T(8,128)(2,1)S(1)}, bf16[256,512]{1,0:T(8,128)(2,1)}, u32[]{:S(2)}) copy-start(bf16[256,512]{1,0:T(8,128)(2,1)} %param.18) | copy-start | bytes 786436
  10.2 12.0 %copy-start.18 = (bf16[256,512]{1,0:T(8,128)(2,1)S(1)}, bf16[256,512]{1,0:T(8,128)(2,1)}, u32[]{:S(2)}) copy-start(bf16[256,512]{1,0:T(8,128)(2,1)} %param.20) | copy-start | bytes 786436
  10.2 15.4 %copy-start.25 = (f32[3,512]{1,0:T(4,128)S(1)}, f32[3,512]{1,0:T(4,128)}, u32[]{:S(2)}) copy-start(f32[3,512]{1,0:T(4,128)} %param.21) | copy-start | bytes 18436
  10.2 66.3 %all-to-all-start = ((bf16[64,16,2048]{2,1,0:T(8,128)(2,1)}), bf16[64,16,2048]{2,1,0:T(8,128)(2,1)}, u32[]{:S(2)}, u32[]{:S(2)}) async-start(bf16[64,16,2048]{2,1,0:T(8,128)(2,1)} %bitcast.49), calls=%async_computation | async-start | bytes 8388608 | tf_op jit(solution)/shard_map/all_to_all | solution.py:40
  22.2 45.9 %collective-permute-start.1 = (bf16[2,2,512]{2,1,0:T(2,128)(2,1)S(1)}, bf16[2,2,512]{2,1,0:T(2,128)(2,1)S(1)}, u32[]{:S(2)}, u32[]{:S(2)}) collective-permute-start(bf16[2,2,512]{2,1,0:T(2,128)(2,1)S(1)} %pad_maximum_fusion.5), channel_id=1, source_target_pairs={{0,2},{2,4},{4,6},{6,8},{8,10},{10,12},{12,14},{14,16},{16,18},{18... | collective-permute-start | bytes 12296 | tf_op jit(solution)/shard_map/ppermute | solution.py:46
  25.7 42.4 %copy-start.20 = (bf16[256,512]{1,0:T(8,128)(2,1)S(1)}, bf16[256,512]{1,0:T(8,128)(2,1)}, u32[]{:S(2)}) copy-start(bf16[256,512]{1,0:T(8,128)(2,1)} %param.19) | copy-start | bytes 786436
  76.5 9.6 %collective-permute-start.2 = (bf16[1024,2048]{1,0:T(8,128)(2,1)}, bf16[1024,2048]{1,0:T(8,128)(2,1)S(1)}, u32[]{:S(2)}, u32[]{:S(2)}) collective-permute-start(bf16[1024,2048]{1,0:T(8,128)(2,1)} %bitcast.5.own_ref.own_x.own_y), channel_id=1, source_target_pairs={{0,1},{1,0},{2,3},{3,2},{4,5},{5,4},{6,7},{7,6},{8,9},{9,8},{10,11... | collective-permute-start | bytes 12582920 | tf_op jit(solution)/shard_map/ppermute | solution.py:36
  92.5 7.1 %collective-permute-start.3 = (bf16[1024,1024]{1,0:T(8,128)(2,1)S(1)}, bf16[1024,1024]{1,0:T(8,128)(2,1)S(1)}, u32[]{:S(2)}, u32[]{:S(2)}) collective-permute-start(bf16[1024,1024]{1,0:T(8,128)(2,1)S(1)} %get-tuple-element.72), channel_id=1, source_target_pairs={{0,1},{1,0},{2,3},{3,2},{4,5},{5,4},{6,7},{7,6},{8,9},{9,8},{10,11... | collective-permute-start | bytes 6291464 | tf_op jit(solution)/shard_map/ppermute | solution.py:36
  93.1 10.4 %collective-permute-start.4 = (bf16[256,512]{1,0:T(8,128)(2,1)S(1)}, bf16[256,512]{1,0:T(8,128)(2,1)S(1)}, u32[]{:S(2)}, u32[]{:S(2)}) collective-permute-start(bf16[256,512]{1,0:T(8,128)(2,1)S(1)} %get-tuple-element.79), channel_id=1, source_target_pairs={{0,32},{32,64},{64,96},{96,0},{1,33},{33,65},{65,97},{97,1},{2,34}... | collective-permute-start | bytes 786440 | tf_op jit(solution)/shard_map/ppermute | solution.py:51
  94.4 13.9 %collective-permute-start.5 = (bf16[256,512]{1,0:T(8,128)(2,1)S(1)}, bf16[256,512]{1,0:T(8,128)(2,1)S(1)}, u32[]{:S(2)}, u32[]{:S(2)}) collective-permute-start(bf16[256,512]{1,0:T(8,128)(2,1)S(1)} %get-tuple-element.79), channel_id=1, source_target_pairs={{0,64},{32,96},{64,0},{96,32},{1,65},{33,97},{65,1},{97,33},{2,66}... | collective-permute-start | bytes 786440 | tf_op jit(solution)/shard_map/ppermute | solution.py:51
  96.3 12.5 %collective-permute-start.6 = (bf16[256,512]{1,0:T(8,128)(2,1)S(1)}, bf16[256,512]{1,0:T(8,128)(2,1)S(1)}, u32[]{:S(2)}, u32[]{:S(2)}) collective-permute-start(bf16[256,512]{1,0:T(8,128)(2,1)S(1)} %get-tuple-element.79), channel_id=1, source_target_pairs={{0,96},{32,0},{64,32},{96,64},{1,97},{33,1},{65,33},{97,65},{2,98}... | collective-permute-start | bytes 786440 | tf_op jit(solution)/shard_map/ppermute | solution.py:51
  108.9 39.5 %all-to-all-start.1 = ((bf16[64,16,1024]{2,1,0:T(8,128)(2,1)}), bf16[64,16,1024]{2,1,0:T(8,128)(2,1)}, u32[]{:S(2)}, u32[]{:S(2)}) async-start(bf16[64,16,1024]{2,1,0:T(8,128)(2,1)} %bitcast.48), calls=%async_computation.1 | async-start | bytes 4194304 | tf_op jit(solution)/shard_map/all_to_all | solution.py:40
  133.6 14.8 %copy-start.12 = (bf16[256,1024]{1,0:T(8,128)(2,1)S(1)}, bf16[256,1024]{1,0:T(8,128)(2,1)}, u32[]{:S(2)}) copy-start(bf16[256,1024]{1,0:T(8,128)(2,1)} %stream_ref.1) | copy-start | bytes 1572868
  133.6 14.8 %copy-start.24 = (f32[1024]{0:T(1024)S(1)}, f32[1024]{0:T(1024)}, u32[]{:S(2)}) copy-start(f32[1024]{0:T(1024)} %param.14) | copy-start | bytes 12292
  133.8 14.6 %copy-start.22 = (bf16[1024,256]{1,0:T(8,128)(2,1)S(1)}, bf16[1024,256]{1,0:T(8,128)(2,1)}, u32[]{:S(2)}) copy-start(bf16[1024,256]{1,0:T(8,128)(2,1)} %get-tuple-element.52) | copy-start | bytes 1572868
  150.9 1.2 collective-permute-start.7
  152.6 15.4 %copy-start.13 = (bf16[256,1024]{1,0:T(8,128)(2,1)}, bf16[256,1024]{1,0:T(8,128)(2,1)S(1)}, u32[]{:S(2)}) copy-start(bf16[256,1024]{1,0:T(8,128)(2,1)S(1)} %fusion.5) | copy-start | bytes 1572868
  152.6 2.0 %collective-permute-start.8 = (bf16[256,1024]{1,0:T(8,128)(2,1)S(1)}, bf16[256,1024]{1,0:T(8,128)(2,1)S(1)}, u32[]{:S(2)}, u32[]{:S(2)}) collective-permute-start(bf16[256,1024]{1,0:T(8,128)(2,1)S(1)} %fusion.5), channel_id=1, source_target_pairs={{0,1},{1,0},{2,3},{3,2},{4,5},{5,4},{6,7},{7,6},{8,9},{9,8},{10,11... | collective-permute-start | bytes 1572872 | tf_op jit(solution)/shard_map/ppermute | solution.py:36
  168.0 1.9 collective-permute-start.9
  172.4 21.7 %all-to-all-start.3 = ((f32[16,32,512]{2,1,0:T(8,128)}), f32[16,32,512]{2,1,0:T(8,128)S(1)}, u32[]{:S(2)}, u32[]{:S(2)}) async-start(f32[16,32,512]{2,1,0:T(8,128)} %bitcast.29), calls=%async_computation.3 | async-start | bytes 2097152 | tf_op jit(solution)/shard_map/all_to_all | solution.py:40
  178.0 13.2 %copy-start.19 = (bf16[256,512]{1,0:T(8,128)(2,1)S(1)}, bf16[256,512]{1,0:T(8,128)(2,1)}, u32[]{:S(2)}) copy-start(bf16[256,512]{1,0:T(8,128)(2,1)} %param.20) | copy-start | bytes 786436
  179.2 11.1 %collective-permute-start.10 = (f32[2,512]{1,0:T(2,128)S(1)}, f32[2,512]{1,0:T(2,128)S(1)}, u32[]{:S(2)}, u32[]{:S(2)}) collective-permute-start(f32[2,512]{1,0:T(2,128)S(1)} %slice.75), channel_id=1, source_target_pairs={{2,0},{4,2},{6,4},{8,6},{10,8},{12,10},{14,12},{16,14},{18,16},{20... | collective-permute-start | bytes 12296 | tf_op jit(solution)/shard_map/ppermute | solution.py:46
  (16 other events, 60.1 us)

commit v3 on v2

--- a/solution.py
+++ b/solution.py
@@ -91,92 +91,111 @@
     )(stream, routes)
 
 
-def rows_body(target_ref, weight_ref, total_ref, stream_ref, cot_ref, gain_ref, out_ref, sel_ref):
+def grads_body(target_ref, weight_ref, cot_ref, out_ref, sel_ref):
     rows, tokens = sel_ref.shape
-    width = stream_ref.shape[1]
     slots = lax.broadcasted_iota(jnp.int32, (rows, tokens), 0) + pl.program_id(0) * rows
     first = slots == target_ref[0:1, :]
     second = slots == target_ref[1:2, :]
-    inverse = lax.rsqrt(total_ref[...] / D + EPSILON)
-    both = jnp.where(first | second, 1.0, 0.0)
-    selector = both.astype(BF16)
-    scale = jnp.sum(both * inverse, axis=1, keepdims=True)
+    selector = jnp.where(first | second, 1.0, 0.0).astype(BF16)
     weight = jnp.where(first, weight_ref[0:1, :], 0.0) + jnp.where(second, weight_ref[1:2, :], 0.0)
     weight = jnp.sum(weight, axis=1, keepdims=True)
     sel_ref[...] = selector
+    out_ref[...] = (weight * dot_nn(selector, cot_ref[...])).astype(BF16)
+
+
+def inputs_body(own_ref, peer_ref, sel_ref, stream_ref, gain_ref, rows_ref, out_ref):
+    inverse = lax.rsqrt((own_ref[...] + peer_ref[...]) / D + EPSILON)
+    selector = sel_ref[...]
+    scale = jnp.sum(selector.astype(F32) * inverse, axis=1, keepdims=True)
     inputs = dot_nn(selector, stream_ref[...])
-    out_ref[:, :width] = (inputs * scale * gain_ref[...]).astype(BF16)
-    grads = dot_nn(selector, cot_ref[...])
-    out_ref[:, width:] = (weight * grads).astype(BF16)
-
-
-def build_rows(target, weights, total, stream, cot, gain, slots):
-    tokens, width = stream.shape
-    rows = slots // 4
-
-    def whole(*shape):
-        return pl.BlockSpec(shape, lambda i: (0, 0))
-
-    return pl.pallas_call(
-        rows_body,
-        grid=(4,),
-        in_specs=[
-            whole(2, tokens),
-            whole(2, tokens),
-            whole(1, tokens),
-            whole(tokens, width),
-            whole(tokens, width),
-            whole(1, width),
-        ],
+    out_ref[...] = (inputs * scale * gain_ref[...]).astype(BF16)
+
+
+def whole_block(*shape):
+    return pl.BlockSpec(shape, lambda i: (0, 0))
+
+
+def grad_rows(target, weights, cot, slots, steps):
+    tokens, width = cot.shape
+    rows = slots // steps
+    return pl.pallas_call(
+        grads_body,
+        grid=(steps,),
+        in_specs=[whole_block(2, tokens), whole_block(2, tokens), whole_block(tokens, width)],
         out_specs=(
-            pl.BlockSpec((rows, 2 * width), lambda i: (i, 0)),
+            pl.BlockSpec((rows, width), lambda i: (i, 1)),
             pl.BlockSpec((rows, tokens), lambda i: (i, 0)),
         ),
         out_shape=(
             jax.ShapeDtypeStruct((slots, 2 * width), BF16),
             jax.ShapeDtypeStruct((slots, tokens), BF16),
         ),
-        name="build_rows",
-        cost_estimate=cost(4 * slots * tokens * width, slots * width * 4),
-    )(target, weights, total, stream, cot, gain)
-
-
-def load_body(core_ref, gate_ref, up_ref, down_ref, *refs):
-    outs, sems = refs[:6], refs[6]
-    width = outs[0].shape[0]
+        name="grad_rows",
+        cost_estimate=cost(2 * slots * tokens * width, slots * width * 2),
+    )(target, weights, cot)
+
+
+def input_rows(own_squares, peer_squares, selector, stream, gain, rows_in, steps):
+    tokens, width = stream.shape
+    slots = selector.shape[0]
+    rows = slots // steps
+    return pl.pallas_call(
+        inputs_body,
+        grid=(steps,),
+        in_specs=[
+            whole_block(1, tokens),
+            whole_block(1, tokens),
+            pl.BlockSpec((rows, tokens), lambda i: (i, 0)),
+            whole_block(tokens, width),
+            whole_block(1, width),
+            pl.BlockSpec(memory_space=pl.ANY),
+        ],
+        out_specs=pl.BlockSpec((rows, width), lambda i: (i, 0)),
+        out_shape=jax.ShapeDtypeStruct((slots, 2 * width), BF16),
+        input_output_aliases={5: 0},
+        name="input_rows",
+        cost_estimate=cost(2 * slots * tokens * width, slots * width * 2),
+    )(own_squares, peer_squares, selector, stream, gain, rows_in)
+
+
+def own_body(
+    core_ref, own_hbm, gate_hbm, up_hbm, down_hbm,
+    gate_out, up_out, grad_out, gate_own, up_own, gate_peer, up_peer, down_peer,
+    own_ref, down_own, sems,
+):
+    _, step, double = own_ref.shape
+    width = double // 2
     mine = pl.multiple_of(core_ref[0] * width, width)
     other = pl.multiple_of((1 - core_ref[0]) * width, width)
-    sources = (
-        gate_ref.at[pl.ds(mine, width), :],
-        gate_ref.at[pl.ds(other, width), :],
-        up_ref.at[pl.ds(mine, width), :],
-        up_ref.at[pl.ds(other, width), :],
-        down_ref.at[:, pl.ds(mine, width)],
-        down_ref.at[:, pl.ds(other, width)],
-    )
-    copies = [
-        pltpu.make_async_copy(source, outs[i], sems.at[i]) for i, source in enumerate(sources)
-    ]
-    for copy in copies:
+    moves = (
+        (gate_hbm.at[pl.ds(mine, width), :], gate_own),
+        (own_hbm.at[pl.ds(0, step), :], own_ref.at[0]),
+        (up_hbm.at[pl.ds(mine, width), :], up_own),
+        (down_hbm.at[:, pl.ds(mine, width)], down_own),
+        (own_hbm.at[pl.ds(step, step), :], own_ref.at[1]),
+        (gate_hbm.at[pl.ds(other, width), :], gate_peer),
+        (up_hbm.at[pl.ds(other, width), :], up_peer),
+        (down_hbm.at[:, pl.ds(other, width)], down_peer),
+    )
+    copies = [pltpu.make_async_copy(a, b, sems.at[i]) for i, (a, b) in enumerate(moves)]
+    for copy in copies[:5]:
         copy.start()
-    for copy in copies:
+    first, second = pl.ds(0, step), pl.ds(step, step)
+    copies[0].wait()
+    copies[1].wait()
+    gate_out[first, :] = dot_nn(own_ref[0, :, :width], gate_own[...])
+    for copy in copies[5:]:
+        copy.start()
+    copies[2].wait()
+    up_out[first, :] = dot_nn(own_ref[0, :, :width], up_own[...])
+    copies[3].wait()
+    grad_out[first, :] = dot_nt(own_ref[0, :, width:], down_own[...])
+    copies[4].wait()
+    gate_out[second, :] = dot_nn(own_ref[1, :, :width], gate_own[...])
+    up_out[second, :] = dot_nn(own_ref[1, :, :width], up_own[...])
+    grad_out[second, :] = dot_nt(own_ref[1, :, width:], down_own[...])
+    for copy in copies[5:]:
         copy.wait()
-
-
-def own_body(own_ref, gate_w, up_w, down_w, gate_out, up_out, hidden_out):
-    rows, double = own_ref.shape
-    width = double // 2
-    step = rows // EXPERT_BLOCKS
-
-    def block(i, carry):
-        at = pl.ds(i * step, step)
-        x, y = own_ref[at, :width], own_ref[at, width:]
-        gate_out[at, :] = dot_nn(x, gate_w[...])
-        up_out[at, :] = dot_nn(x, up_w[...])
-        hidden_out[at, :] = dot_nt(y, down_w[...])
-        return carry
-
-    lax.fori_loop(0, EXPERT_BLOCKS, block, 0)
 
 
 def peer_body(
@@ -234,6 +253,10 @@
 IN_VMEM = pl.BlockSpec(memory_space=pltpu.VMEM)
 
 
+def in_hbm(array):
+    return pltpu.with_memory_space_constraint(array, pltpu.HBM)
+
+
 def on_chip(body, outs, flops, limit, *args):
     return pl.pallas_call(
         body,
@@ -245,26 +268,25 @@
     )(*args)
 
 
-def load_weights(core, gate_w, up_w, down_w):
-    double, units = gate_w.shape
+def expert_own(core, own, gate_w, up_w, down_w):
+    rows, double = own.shape
+    units = gate_w.shape[1]
     width = double // 2
-    shapes = [(width, units)] * 4 + [(units, width)] * 2
-    return pl.pallas_call(
-        load_body,
-        in_specs=[pl.BlockSpec(memory_space=pltpu.SMEM)] + [pl.BlockSpec(memory_space=pl.ANY)] * 3,
-        out_specs=[IN_VMEM] * 6,
-        out_shape=[jax.ShapeDtypeStruct(s, BF16) for s in shapes],
-        scratch_shapes=[pltpu.SemaphoreType.DMA((6,))],
-        name="load_weights",
-        cost_estimate=cost(10**9, 6 * double * units),
-    )(core, gate_w, up_w, down_w)
-
-
-def expert_own(own, gate_w, up_w, down_w):
-    rows, units = own.shape[0], gate_w.shape[1]
-    outs = [((rows, units), F32)] * 3
-    flops = 3 * rows * own.shape[1] * units
-    return on_chip(own_body, outs, flops, 8, own, gate_w, up_w, down_w)
+    shapes = [((rows, units), F32)] * 3 + [((width, units), BF16)] * 4 + [((units, width), BF16)]
+    return pl.pallas_call(
+        own_body,
+        in_specs=[pl.BlockSpec(memory_space=pltpu.SMEM)] + [pl.BlockSpec(memory_space=pl.ANY)] * 4,
+        out_specs=[IN_VMEM] * len(shapes),
+        out_shape=[jax.ShapeDtypeStruct(s, d) for s, d in shapes],
+        scratch_shapes=[
+            pltpu.VMEM((2, rows // 2, double), BF16),
+            pltpu.VMEM((units, width), BF16),
+            pltpu.SemaphoreType.DMA((8,)),
+        ],
+        compiler_params=pltpu.CompilerParams(vmem_limit_bytes=12 * 1024 * 1024),
+        name="expert_own",
+        cost_estimate=cost(3 * rows * double * units, 10 * double * units),
+    )(core, *[in_hbm(array) for array in (own, gate_w, up_w, down_w)])
 
 
 def expert_peer(peer, gate_w, up_w, down_w, *parts):
@@ -288,7 +310,7 @@
         add_body,
         in_specs=[IN_VMEM] * 2,
         out_specs=pl.BlockSpec(memory_space=pltpu.HBM),
-        out_shape=jax.ShapeDtypeStruct(mine.shape, BF16),
+        out_shape=pltpu.HBM(mine.shape, BF16),
         scratch_shapes=[
             pltpu.VMEM((blocks, rows // blocks, width), BF16),
             pltpu.SemaphoreType.DMA((blocks,)),
@@ -297,6 +319,48 @@
         name="add_parts",
         cost_estimate=cost(mine.size, 6 * mine.size),
     )(mine, other)
+
+
+def product_body(left_ref, right_ref, out_ref):
+    out_ref[...] = dot_tn(left_ref[...], right_ref[...])
+
+
+def product_more_body(left_ref, right_ref, part_ref, out_ref):
+    out_ref[...] = part_ref[...] + dot_tn(left_ref[...], right_ref[...])
+
+
+def product(left, right, *part):
+    body = product_more_body if part else product_body
+    outs = [((left.shape[1], right.shape[1]), F32)]
+    flops = 2 * left.size * right.shape[1]
+    return on_chip(body, outs, flops, 8, left, right, *part)[0]
+
+
+def mixer_body(core_ref, grad_ref, peer_ref, proj_ref, gate_ref, conv_ref, delta_ref, out_ref):
+    width = grad_ref.shape[1]
+    mine = pl.multiple_of(core_ref[0] * width, width)
+    other = pl.multiple_of((1 - core_ref[0]) * width, width)
+    mixer_grad = dot_nn(grad_ref[...], proj_ref[pl.ds(mine, width), :])
+    mixer_grad = mixer_grad + dot_nn(peer_ref[...], proj_ref[pl.ds(other, width), :])
+    delta_ref[...] = mixer_grad * gate_ref[...].astype(F32)
+    out_ref[...] = (mixer_grad * conv_ref[...]).astype(BF16)
+
+
+def mixer_back(core, grad, peer, proj, gate, conv):
+    rows, width = grad.shape
+    channels = proj.shape[1]
+    return pl.pallas_call(
+        mixer_body,
+        in_specs=[pl.BlockSpec(memory_space=pltpu.SMEM)] + [IN_VMEM] * 5,
+        out_specs=[IN_VMEM] * 2,
+        out_shape=[
+            jax.ShapeDtypeStruct((rows, channels), F32),
+            jax.ShapeDtypeStruct((rows, channels), BF16),
+        ],
+        compiler_params=pltpu.CompilerParams(vmem_limit_bytes=12 * 1024 * 1024),
+        name="mixer_back",
+        cost_estimate=cost(4 * rows * width * channels, 8 * 1024 * 1024),
+    )(core, grad, peer, proj, gate, conv)
 
 
 def weights_body(
@@ -383,10 +447,9 @@
     gain_row = norm_gain[None, :]
 
     squares, target = find_slots(stream, routes.T, experts, capacity)
-    total = squares + swap(squares)
-    rows, selector = build_rows(
-        target, route_weights.T, total, stream, cotangent, gain_row, slots
-    )
+    peer_squares = swap(squares)
+    rows, selector = grad_rows(target, route_weights.T, cotangent, slots, 4)
+    rows = input_rows(squares, peer_squares, selector, stream, gain_row, rows, 4)
     own = exchange(rows.reshape(experts, capacity, 2 * width), SP).reshape(slots, 2 * width)
 
     input_float = conv_input.astype(F32)
@@ -402,9 +465,7 @@
         + conv_taps[2][None, :] * extended[2:]
     )
     mixer_out = (bgate_float * conv_out).astype(BF16)
-    weights = load_weights(core_arg, gate_weight[0], up_weight[0], down_weight[0])
-    own, mixer_out, weights = lax.optimization_barrier((own, mixer_out, weights))
-    gate_own, gate_peer, up_own, up_peer, down_own, down_peer = weights
+    own, mixer_out = lax.optimization_barrier((own, mixer_out))
     line = lax.axis_size("sp_0")
     spot = lax.axis_index("sp_0")
     token_half = tok_count // 2
@@ -417,14 +478,15 @@
     around = [mixer_out]
     for step in range(1, line):
         around.append(turned(mixer_out, "sp_0", step))
-    parts = expert_own(own, gate_own, up_own, down_own)
+    gate_part, up_part, grad_part, gate_own, up_own, gate_peer, up_peer, down_peer = expert_own(
+        core_arg, own, gate_weight[0], up_weight[0], down_weight[0]
+    )
     hidden, gate_pre, up_pre, part_theirs = expert_peer(
-        peer, gate_peer, up_peer, down_peer, *parts
+        peer, gate_peer, up_peer, down_peer, gate_part, up_part, grad_part
     )
     other = swap(part_theirs)
     part_mine = expert_mine(gate_pre, up_pre, gate_own, up_own)
     row_grads = add_parts(part_mine, other)
-    row_grads, around = lax.optimization_barrier((row_grads, around))
     returned = exchange(row_grads.reshape(experts, capacity, width), SP).reshape(slots, width)
     grads_w = weight_grads(core_arg, own, peer, hidden, gate_pre, up_pre)
     around = jnp.stack(around)
@@ -440,7 +502,7 @@
     normed_grad = dot_tn(selector, returned)
     stream_float = stream.astype(F32)
     cot_float = cotangent.astype(F32)
-    inverse = lax.rsqrt(total[0] / D + EPSILON)[:, None]
+    inverse = lax.rsqrt((squares + peer_squares)[0] / D + EPSILON)[:, None]
     cross_part = jnp.sum(stream_float * gain_row * normed_grad, axis=1)
     cross = cross_part + swap(cross_part)
     stream_grad = (
@@ -458,16 +520,12 @@
     sent = jnp.stack(parts)
     grads_mine = exchange(sent, "sp_0").reshape(line * token_half, quarter)
     grads_theirs = swap(grads_mine)
-    proj_part = dot_tn(grads_mine, mixers_mine) + dot_tn(grads_theirs, mixers_theirs)
-    late_grad, late_peer, proj_part = lax.optimization_barrier((stream_grad, grad_peer, proj_part))
+    proj_part = product(grads_theirs, mixers_theirs, product(grads_mine, mixers_mine))
     plane = lax.axis_size(("sp_1", "sp_2"))
     arrived = exchange(proj_part.reshape(plane, quarter // plane, channels), ("sp_1", "sp_2"))
     proj_grad = arrived.sum(axis=0)
 
-    proj_mine = lax.dynamic_slice_in_dim(out_proj, core * width, width, 0)
-    proj_peer = lax.dynamic_slice_in_dim(out_proj, (1 - core) * width, width, 0)
-    mixer_grad = dot_nn(late_grad, proj_mine) + dot_nn(late_peer, proj_peer)
-    delta = mixer_grad * bgate_float
+    delta, bgate_grad = mixer_back(core_arg, stream_grad, grad_peer, out_proj, conv_bgate, conv_out)
     next_rim = shifted(delta[:2], SP, -1)
     extended_back = jnp.concatenate([delta, next_rim], axis=0)
     gated_grad = (
@@ -475,7 +533,6 @@
         + conv_taps[1][None, :] * extended_back[1:-1]
         + conv_taps[0][None, :] * extended_back[2:]
     )
-    bgate_grad = (mixer_grad * conv_out).astype(BF16)
     input_grad = (gated_grad * cgate_float).astype(BF16)
     cgate_grad = (gated_grad * input_float).astype(BF16)
     return (

time: 196 us -> 213 us (1.087)
  waiting for transfers between devices: 81.4 us -> 104 us
  matrix products: 9.23 us -> 2.47 us
  local copies, waits for them, and re-layouts: 7.08 us -> 2.8 us
  Pallas kernels: 42.5 us -> 46.6 us
  starting transfers between devices: 35.3 us -> 37.5 us
    ppermute x3, waiting for transfers between devices: 7.01 us -> 33.2 us  [turned(): lax.ppermute(value, axis, [(i, (i + steps) % count) for i in range(count)])]
    all_to_all x3, waiting for transfers between devices: 23.1 us -> 8.19 us  [exchange(): return lax.all_to_all(value, axis, split_axis=0, concat_axis=0, tiled=True)]
    ppermute x2, waiting for transfers between devices: 46.6 us -> 55.3 us  [shifted(): lax.ppermute(value, axis, [(source, source + steps) for source in range(l...]
    pallas_call x2 -> x4, Pallas kernels: 10.2 us -> 15.4 us  [the longest x1 5.95 us: expert_own(): pl.pallas_call(own_body, in_specs=[pl.BlockSpec(memory_space=pltpu.SMEM)]...]
    unnamed x52 -> x43, local copies, waits for them, and re-layouts: 5.85 us -> 1.72 us
    dot_general x3 -> x1, matrix products: 6.49 us -> 2.47 us  [dot_tn(): lax.dot_general(a, b, (((0,), (0,)), ((), ())), preferred_element_type=F32)]
    dot_general x2 -> x0, matrix products: 2.74 us -> none  [dot_nn(): lax.dot_general(a, b, (((1,), (0,)), ((), ())), preferred_element_type=F32)]
    ppermute x6, waiting for transfers between devices: 4.67 us -> 7.26 us  [swap(): return lax.ppermute(value, 'tp', [(0, 1), (1, 0)])]
  transfers between devices with their start and end apart: 14 -> 14, of which waited for: 12 -> 12; matrix products, arithmetic and copies ran while one was open for 4% -> 2% of each run, Pallas kernels for 15% -> 14%
where the time goes in v3:
time: 213 us; the launch traced here: 212 us
  waiting for transfers between devices  104 us (49%)
  Pallas kernels  46.6 us (22%)
  starting transfers between devices  37.5 us (18%)
  blocking collectives  12.6 us (6%)
  other arithmetic  4.83 us (2%)
  local copies, waits for them, and re-layouts  2.8 us (1%)
  matrix products  2.47 us (1%)
    ppermute x2, waiting for transfers between devices, shifted(): lax.ppermute(value, axis, [(source, source + steps) for source in range(l...  55.3 us
    ppermute x3, waiting for transfers between devices, turned(): lax.ppermute(value, axis, [(i, (i + steps) % count) for i in range(count)])  33.2 us
    all_to_all x3, starting transfers between devices, exchange(): return lax.all_to_all(value, axis, split_axis=0, concat_axis=0, tiled=True)  27.5 us
    pallas_call x1, Pallas kernels, weight_grads(): pl.pallas_call(weights_body, grid_spec=pltpu.PrefetchScalarGridSpec(num_s...  14.6 us
    pallas_call x4, Pallas kernels, on_chip(): pl.pallas_call(body, in_specs=[IN_VMEM] * len(args), out_specs=[IN_VMEM]...  13 us
    all_to_all x1, blocking collectives, exchange(): return lax.all_to_all(value, axis, split_axis=0, concat_axis=0, tiled=True)  12.6 us
    all_to_all x3, waiting for transfers between devices, exchange(): return lax.all_to_all(value, axis, split_axis=0, concat_axis=0, tiled=True)  8.19 us
    ppermute x6, waiting for transfers between devices, swap(): return lax.ppermute(value, 'tp', [(0, 1), (1, 0)])  7.26 us
  transfers between devices with their start and end apart: 14, of which 12 were waited for; matrix products, arithmetic and copies ran while one was open for 2% of the time, Pallas kernels for 14%

profile of v3, /device:TPU:0, one launch (start us, length us, event | category | flops | bytes accessed | tf_op | source)
XLA Modules:
  0.0 211.7 jit_solution(6920556008608564888)
XLA Ops:
  0.6 2.1 find_slots.1
  2.7 3.7 %grad_rows.1 = (bf16[1024,2048]{1,0:T(8,128)(2,1)}, bf16[1024,256]{1,0:T(8,128)(2,1)}) custom-call(s32[2,256]{1,0:T(2,128)} %get-tuple-element.38.target_ref, f32[2,256]{1,0:T(2,128)} %bitcast.64, bf16[256,1024]{1,0:T(8,128)(2,1)} %cot_ref.1), custom_call_target="tpu_custom_call" | custom-call | flops 536870912 | bytes 2097152 | tf_op jit(solution)/shard_map/grad_rows/pallas_call | solution.py:121
  7.0 4.3 %input_rows.1 = bf16[1024,2048]{1,0:T(8,128)(2,1)} custom-call(f32[1,256]{1,0:T(1,128)} %get-tuple-element.37.own_ref, f32[1,256]{1,0:T(1,128)} %copy-done.19, bf16[1024,256]{1,0:T(8,128)(2,1)} %get-tuple-element.39.sel_ref, bf16[256,1024]{1,0:T(8,128)(2,1)} %stream_ref.1, f32[1,1024]{1,0:T(1,128)} %bitcast.52, ...), custom_call_target="tpu_custom_call", output_to_operand_aliasing={{}: (5, {})} | custom-call | flops 536870912 | bytes 2097152 | tf_op jit(solution)/shard_map/input_rows/pallas_call | solution.py:142
  11.3 11.9 %all-to-all-start = ((bf16[64,16,2048]{2,1,0:T(8,128)(2,1)}), bf16[64,16,2048]{2,1,0:T(8,128)(2,1)}, u32[]{:S(2)}, u32[]{:S(2)}) async-start(bf16[64,16,2048]{2,1,0:T(8,128)(2,1)} %bitcast.46), calls=%async_computation | async-start | bytes 8388608 | tf_op jit(solution)/shard_map/all_to_all | solution.py:40
  23.3 3.4 %collective-permute-start.1 = (bf16[2,2,512]{2,1,0:T(2,128)(2,1)S(1)}, bf16[2,2,512]{2,1,0:T(2,128)(2,1)S(1)}, u32[]{:S(2)}, u32[]{:S(2)}) collective-permute-start(bf16[2,2,512]{2,1,0:T(2,128)(2,1)S(1)} %pad_maximum_fusion.4), channel_id=1, source_target_pairs={{0,2},{2,4},{4,6},{6,8},{8,10},{10,12},{12,14},{14,16},{16,18},{18... | collective-permute-start | bytes 12296 | tf_op jit(solution)/shard_map/ppermute | solution.py:46
  26.8 45.4 %collective-permute-done.1 = bf16[2,2,512]{2,1,0:T(2,128)(2,1)S(1)} collective-permute-done((bf16[2,2,512]{2,1,0:T(2,128)(2,1)S(1)}, bf16[2,2,512]{2,1,0:T(2,128)(2,1)S(1)}, u32[]{:S(2)}, u32[]{:S(2)}) %collective-permute-start.1) | collective-permute-done | bytes 4128 | tf_op jit(solution)/shard_map/ppermute | solution.py:46
  72.4 5.9 %all-to-all-done = bf16[64,16,2048]{2,1,0:T(8,128)(2,1)} async-done(((bf16[64,16,2048]{2,1,0:T(8,128)(2,1)}), bf16[64,16,2048]{2,1,0:T(8,128)(2,1)}, u32[]{:S(2)}, u32[]{:S(2)}) %all-to-all-start) | async-done | bytes 4194336 | tf_op jit(solution)/shard_map/all_to_all | solution.py:40
  78.3 5.9 %expert_own.1 = (f32[1024,512]{1,0:T(8,128)S(1)}, f32[1024,512]{1,0:T(8,128)S(1)}, f32[1024,512]{1,0:T(8,128)S(1)}, bf16[1024,512]{1,0:T(8,128)(2,1)S(1)}, bf16[...) custom-call(s32[1]{0:T(128)} %bitcast.12.core_ref, ...), custom_call_target="tpu_custom_call" | custom-call | flops 3221225472 | bytes 10485760 | tf_op jit(solution)/shard_map/expert_own/pallas_call | solution.py:276
  85.8 8.5 %shard_map.188 = (bf16[1024,512]{1,0:T(8,128)(2,1)S(1)}, bf16[1024,512]{1,0:T(8,128)(2,1)S(1)}, bf16[1024,512]{1,0:T(8,128)(2,1)S(1)}, bf16[1024,1024]{1,0:T(8,128)(2,1)S(1)}) custom-call(bf16[1024,2048]{1,0:T(8,128)(2,1)} %collective-permute-done.2.peer_ref.peer_x.peer_y, bf16[1024,512]{1,0:T(8,128)(2,1)S(1)} %get-tuple-element.42.gate_w, ...), custom_call_target="tpu_custom_call" | custom-call | flops 5368709120 | bytes 16777216 | tf_op jit(solution)/shard_map/pallas_call | solution.py:261
  94.5 2.6 %shard_map.189.mine_ref = bf16[1024,1024]{1,0:T(8,128)(2,1)S(1)} custom-call(bf16[1024,512]{1,0:T(8,128)(2,1)S(1)} %get-tuple-element.48.gate_ref, bf16[1024,512]{1,0:T(8,128)(2,1)S(1)} %get-tuple-element.49.up_ref, bf16[1024,512]{1,0:T(8,128)(2,1)S(1)} %get-tuple-element.50.gate_w, bf16[1024,512]{1,0:T(8,128)(2,1)S(1)} %get-tuple-element.51.up_w), custom_call_target="tpu_custom_call" | custom-call | flops 2147483648 | bytes 16777216 | tf_op jit(solution)/shard_map/pallas_call | solution.py:261
  98.6 1.5 add_parts.1
  100.1 9.6 %all-to-all-start.1 = ((bf16[64,16,1024]{2,1,0:T(8,128)(2,1)}), bf16[64,16,1024]{2,1,0:T(8,128)(2,1)}, u32[]{:S(2)}, u32[]{:S(2)}) async-start(bf16[64,16,1024]{2,1,0:T(8,128)(2,1)} %bitcast.47), calls=%async_computation.1 | async-start | bytes 4194304 | tf_op jit(solution)/shard_map/all_to_all | solution.py:40
  109.7 3.0 %collective-permute-start.6 = (bf16[256,512]{1,0:T(8,128)(2,1)S(1)}, bf16[256,512]{1,0:T(8,128)(2,1)S(1)}, u32[]{:S(2)}, u32[]{:S(2)}) collective-permute-start(bf16[256,512]{1,0:T(8,128)(2,1)S(1)} %get-tuple-element.57), channel_id=1, source_target_pairs={{0,96},{32,0},{64,32},{96,64},{1,97},{33,1},{65,33},{97,65},{2,98}... | collective-permute-start | bytes 786440 | tf_op jit(solution)/shard_map/ppermute | solution.py:51
  114.3 26.2 %collective-permute-done.6 = bf16[256,512]{1,0:T(8,128)(2,1)S(1)} collective-permute-done((bf16[256,512]{1,0:T(8,128)(2,1)S(1)}, bf16[256,512]{1,0:T(8,128)(2,1)S(1)}, u32[]{:S(2)}, u32[]{:S(2)}) %collective-permute-start.6) | collective-permute-done | bytes 262176 | tf_op jit(solution)/shard_map/ppermute | solution.py:51
  140.5 1.8 collective-permute-done.5
  142.3 5.1 %collective-permute-done.4 = bf16[256,512]{1,0:T(8,128)(2,1)S(1)} collective-permute-done((bf16[256,512]{1,0:T(8,128)(2,1)S(1)}, bf16[256,512]{1,0:T(8,128)(2,1)S(1)}, u32[]{:S(2)}, u32[]{:S(2)}) %collective-permute-start.4) | collective-permute-done | bytes 262176 | tf_op jit(solution)/shard_map/ppermute | solution.py:51
  148.8 14.6 %weight_grads.1 = (f32[2048,512]{1,0:T(8,128)}, f32[2048,512]{1,0:T(8,128)}, f32[512,2048]{1,0:T(8,128)}) custom-call(s32[1]{0:T(128)} %bitcast.12.core_ref, bf16[1024,2048]{1,0:T(8,128)(2,1)} %bitcast.5.own_hbm.own_x.own_y, bf16[1024,2048]{1,0:T(8,128)(2,1)} %bitcast.5.own_hbm.own_x.own_y, bf16[1024,2048]{1,0:T(8,128)(2,1)} %collective-permute-done.2.peer_ref.peer_x.peer_y, ...), custom_call_target="tpu_custom_call" | custom-call | flops 6442450944 | bytes 12582912 | tf_op jit(solution)/shard_map/weight_grads/pallas_call | solution.py:406
  163.4 2.5 %fusion.7 = (f32[256]{0:T(256)S(1)}, f32[256,1024]{1,0:T(8,128)S(1)}) fusion(bf16[256,1024]{1,0:T(8,128)(2,1)S(1)} %copy-done.9, f32[1024]{0:T(1024)S(1)} %copy-done.16, bf16[1024,256]{1,0:T(8,128)(2,1)S(1)} %copy-done.10, bf16[1024,1024]{1,0:T(8,128)(2,1)} %bitcast.17), kind=kOutput, calls=%fused_computation.9 | convolution fusion | flops 537919232 | bytes 4199424 | tf_op jit(solution)/shard_map/dot_general | solution.py:28
  167.9 1.7 collective-permute-done.8.peer_ref
  169.9 12.6 %all_to_all.20 = bf16[4,128,512]{2,1,0:T(8,128)(2,1)S(1)} all-to-all(bf16[4,128,512]{2,1,0:T(8,128)(2,1)S(1)} %pad_maximum_fusion.3), channel_id=1, replica_groups=mesh['sp_0'=4,'sp_1'=4,'sp_2'=4,'tp'=2] {'sp_0'}, dimensions={0} | all-to-all | bytes 1048576 | tf_op jit(solution)/shard_map/all_to_all | solution.py:40
  185.9 6.0 %all-to-all-start.3 = ((f32[16,32,512]{2,1,0:T(8,128)}), f32[16,32,512]{2,1,0:T(8,128)}, u32[]{:S(2)}, u32[]{:S(2)}) async-start(f32[16,32,512]{2,1,0:T(8,128)} %bitcast.29), calls=%async_computation.3 | async-start | bytes 2097152 | tf_op jit(solution)/shard_map/all_to_all | solution.py:40
  195.9 9.9 %collective-permute-done.10 = f32[2,512]{1,0:T(2,128)S(1)} collective-permute-done((f32[2,512]{1,0:T(2,128)S(1)}, f32[2,512]{1,0:T(2,128)S(1)}, u32[]{:S(2)}, u32[]{:S(2)}) %collective-permute-start.10) | collective-permute-done | bytes 4128 | tf_op jit(solution)/shard_map/ppermute | solution.py:46
  207.5 2.3 %all-to-all-done.3 = f32[16,32,512]{2,1,0:T(8,128)} async-done(((f32[16,32,512]{2,1,0:T(8,128)}), f32[16,32,512]{2,1,0:T(8,128)}, u32[]{:S(2)}, u32[]{:S(2)}) %all-to-all-start.3) | async-done | bytes 1048608 | tf_op jit(solution)/shard_map/all_to_all | solution.py:40
  209.8 1.9 reduce_sum.19
  (82 shorter events, 18.2 us)
Async XLA Ops:
  2.7 3.7 %collective-permute-start = (f32[1,256]{1,0:T(1,128)}, f32[1,256]{1,0:T(1,128)S(1)}, u32[]{:S(2)}, u32[]{:S(2)}) collective-permute-start(f32[1,256]{1,0:T(1,128)} %get-tuple-element.37.own_ref), channel_id=1, source_target_pairs={{0,1},{1,0},{2,3},{3,2},{4,5},{5,4},{6,7},{7,6},{8,9},{9,8},{10,11... | collective-permute-start | bytes 3080 | tf_op jit(solution)/shard_map/ppermute | solution.py:36
  11.3 15.5 %copy-start.17 = (f32[3,512]{1,0:T(4,128)S(1)}, f32[3,512]{1,0:T(4,128)}, u32[]{:S(2)}) copy-start(f32[3,512]{1,0:T(4,128)} %param.21) | copy-start | bytes 18436
  11.3 60.9 %copy-start.5 = (bf16[256,512]{1,0:T(8,128)(2,1)S(1)}, bf16[256,512]{1,0:T(8,128)(2,1)}, u32[]{:S(2)}) copy-start(bf16[256,512]{1,0:T(8,128)(2,1)} %gate_ref.1) | copy-start | bytes 786436
  11.3 67.0 %all-to-all-start = ((bf16[64,16,2048]{2,1,0:T(8,128)(2,1)}), bf16[64,16,2048]{2,1,0:T(8,128)(2,1)}, u32[]{:S(2)}, u32[]{:S(2)}) async-start(bf16[64,16,2048]{2,1,0:T(8,128)(2,1)} %bitcast.46), calls=%async_computation | async-start | bytes 8388608 | tf_op jit(solution)/shard_map/all_to_all | solution.py:40
  23.3 48.9 %collective-permute-start.1 = (bf16[2,2,512]{2,1,0:T(2,128)(2,1)S(1)}, bf16[2,2,512]{2,1,0:T(2,128)(2,1)S(1)}, u32[]{:S(2)}, u32[]{:S(2)}) collective-permute-start(bf16[2,2,512]{2,1,0:T(2,128)(2,1)S(1)} %pad_maximum_fusion.4), channel_id=1, source_target_pairs={{0,2},{2,4},{4,6},{6,8},{8,10},{10,12},{12,14},{14,16},{16,18},{18... | collective-permute-start | bytes 12296 | tf_op jit(solution)/shard_map/ppermute | solution.py:46
  78.3 7.5 %collective-permute-start.2 = (bf16[1024,2048]{1,0:T(8,128)(2,1)}, bf16[1024,2048]{1,0:T(8,128)(2,1)}, u32[]{:S(2)}, u32[]{:S(2)}) collective-permute-start(bf16[1024,2048]{1,0:T(8,128)(2,1)} %bitcast.5.own_hbm.own_x.own_y), channel_id=1, source_target_pairs={{0,1},{1,0},{2,3},{3,2},{4,5},{5,4},{6,7},{7,6},{8,9},{9,8},{10,11... | collective-permute-start | bytes 12582920 | tf_op jit(solution)/shard_map/ppermute | solution.py:36
  94.3 4.2 %collective-permute-start.3 = (bf16[1024,1024]{1,0:T(8,128)(2,1)S(1)}, bf16[1024,1024]{1,0:T(8,128)(2,1)S(1)}, u32[]{:S(2)}, u32[]{:S(2)}) collective-permute-start(bf16[1024,1024]{1,0:T(8,128)(2,1)S(1)} %get-tuple-element.52), channel_id=1, source_target_pairs={{0,1},{1,0},{2,3},{3,2},{4,5},{5,4},{6,7},{7,6},{8,9},{9,8},{10,11... | collective-permute-start | bytes 6291464 | tf_op jit(solution)/shard_map/ppermute | solution.py:36
  100.1 63.2 %all-to-all-start.1 = ((bf16[64,16,1024]{2,1,0:T(8,128)(2,1)}), bf16[64,16,1024]{2,1,0:T(8,128)(2,1)}, u32[]{:S(2)}, u32[]{:S(2)}) async-start(bf16[64,16,1024]{2,1,0:T(8,128)(2,1)} %bitcast.47), calls=%async_computation.1 | async-start | bytes 4194304 | tf_op jit(solution)/shard_map/all_to_all | solution.py:40
  109.7 30.8 %collective-permute-start.6 = (bf16[256,512]{1,0:T(8,128)(2,1)S(1)}, bf16[256,512]{1,0:T(8,128)(2,1)S(1)}, u32[]{:S(2)}, u32[]{:S(2)}) collective-permute-start(bf16[256,512]{1,0:T(8,128)(2,1)S(1)} %get-tuple-element.57), channel_id=1, source_target_pairs={{0,96},{32,0},{64,32},{96,64},{1,97},{33,1},{65,33},{97,65},{2,98}... | collective-permute-start | bytes 786440 | tf_op jit(solution)/shard_map/ppermute | solution.py:51
  112.7 29.6 %collective-permute-start.5 = (bf16[256,512]{1,0:T(8,128)(2,1)S(1)}, bf16[256,512]{1,0:T(8,128)(2,1)S(1)}, u32[]{:S(2)}, u32[]{:S(2)}) collective-permute-start(bf16[256,512]{1,0:T(8,128)(2,1)S(1)} %get-tuple-element.57), channel_id=1, source_target_pairs={{0,64},{32,96},{64,0},{96,32},{1,65},{33,97},{65,1},{97,33},{2,66}... | collective-permute-start | bytes 786440 | tf_op jit(solution)/shard_map/ppermute | solution.py:51
  113.3 34.1 %collective-permute-start.4 = (bf16[256,512]{1,0:T(8,128)(2,1)S(1)}, bf16[256,512]{1,0:T(8,128)(2,1)S(1)}, u32[]{:S(2)}, u32[]{:S(2)}) collective-permute-start(bf16[256,512]{1,0:T(8,128)(2,1)S(1)} %get-tuple-element.57), channel_id=1, source_target_pairs={{0,32},{32,64},{64,96},{96,0},{1,33},{33,65},{65,97},{97,1},{2,34}... | collective-permute-start | bytes 786440 | tf_op jit(solution)/shard_map/ppermute | solution.py:51
  148.7 14.6 %copy-start.9 = (bf16[256,1024]{1,0:T(8,128)(2,1)S(1)}, bf16[256,1024]{1,0:T(8,128)(2,1)}, u32[]{:S(2)}) copy-start(bf16[256,1024]{1,0:T(8,128)(2,1)} %stream_ref.1) | copy-start | bytes 1572868
  148.7 14.6 %copy-start.10 = (bf16[1024,256]{1,0:T(8,128)(2,1)S(1)}, bf16[1024,256]{1,0:T(8,128)(2,1)}, u32[]{:S(2)}) copy-start(bf16[1024,256]{1,0:T(8,128)(2,1)} %get-tuple-element.39.sel_ref) | copy-start | bytes 1572868
  148.7 14.6 %copy-start.16 = (f32[1024]{0:T(1024)S(1)}, f32[1024]{0:T(1024)}, u32[]{:S(2)}) copy-start(f32[1024]{0:T(1024)} %param.14) | copy-start | bytes 12292
  165.9 1.2 collective-permute-start.7
  167.6 24.3 %copy-start = (bf16[256,1024]{1,0:T(8,128)(2,1)}, bf16[256,1024]{1,0:T(8,128)(2,1)S(1)}, u32[]{:S(2)}) copy-start(bf16[256,1024]{1,0:T(8,128)(2,1)S(1)} %fusion.5.grad_ref) | copy-start | bytes 1572868
  167.6 2.0 collective-permute-start.8
  169.6 12.9 %copy-start.3 = (bf16[256,1024]{1,0:T(8,128)(2,1)}, bf16[256,1024]{1,0:T(8,128)(2,1)S(1)}, u32[]{:S(2)}) copy-start(bf16[256,1024]{1,0:T(8,128)(2,1)S(1)} %collective-permute-done.8.peer_ref) | copy-start | bytes 1572868
  169.8 14.6 %copy-start.2 = (bf16[4,128,512]{2,1,0:T(8,128)(2,1)S(1)}, bf16[4,128,512]{2,1,0:T(8,128)(2,1)}, u32[]{:S(2)}) copy-start(bf16[4,128,512]{2,1,0:T(8,128)(2,1)} %get-tuple-element.72) | copy-start | bytes 1572868
  182.5 1.9 collective-permute-start.9
  185.9 23.9 %all-to-all-start.3 = ((f32[16,32,512]{2,1,0:T(8,128)}), f32[16,32,512]{2,1,0:T(8,128)}, u32[]{:S(2)}, u32[]{:S(2)}) async-start(f32[16,32,512]{2,1,0:T(8,128)} %bitcast.29), calls=%async_computation.3 | async-start | bytes 2097152 | tf_op jit(solution)/shard_map/all_to_all | solution.py:40
  193.0 12.8 %copy-start.12 = (bf16[256,512]{1,0:T(8,128)(2,1)S(1)}, bf16[256,512]{1,0:T(8,128)(2,1)}, u32[]{:S(2)}) copy-start(bf16[256,512]{1,0:T(8,128)(2,1)} %param.18) | copy-start | bytes 786436
  194.4 12.3 %copy-start.14 = (bf16[256,512]{1,0:T(8,128)(2,1)S(1)}, bf16[256,512]{1,0:T(8,128)(2,1)}, u32[]{:S(2)}) copy-start(bf16[256,512]{1,0:T(8,128)(2,1)} %param.20) | copy-start | bytes 786436
  194.4 11.4 %collective-permute-start.10 = (f32[2,512]{1,0:T(2,128)S(1)}, f32[2,512]{1,0:T(2,128)S(1)}, u32[]{:S(2)}, u32[]{:S(2)}) collective-permute-start(f32[2,512]{1,0:T(2,128)S(1)} %slice.64), channel_id=1, source_target_pairs={{2,0},{4,2},{6,4},{8,6},{10,8},{12,10},{14,12},{16,14},{18,16},{20... | collective-permute-start | bytes 12296 | tf_op jit(solution)/shard_map/ppermute | solution.py:46
  (11 other events, 51.9 us)

commit v4 on v3

--- a/solution.py
+++ b/solution.py
@@ -11,9 +11,11 @@
 SP = ("sp_0", "sp_1", "sp_2")
 EPSILON = 1e-06
 VMEM = 56 * 1024 * 1024
-EXPERT_BLOCKS = 2
 F32 = jnp.float32
 BF16 = jnp.bfloat16
+IN_VMEM = pl.BlockSpec(memory_space=pltpu.VMEM)
+IN_HBM = pl.BlockSpec(memory_space=pl.ANY)
+IN_SMEM = pl.BlockSpec(memory_space=pltpu.SMEM)
 
 
 def dot_nn(a, b):
@@ -91,71 +93,62 @@
     )(stream, routes)
 
 
-def grads_body(target_ref, weight_ref, cot_ref, out_ref, sel_ref):
+def rows_body(
+    target_ref, weight_ref, own_ref, peer_ref, stream_ref, cot_ref, gain_ref,
+    out_ref, sel_ref, inverse_ref,
+):
     rows, tokens = sel_ref.shape
+    width = stream_ref.shape[1]
     slots = lax.broadcasted_iota(jnp.int32, (rows, tokens), 0) + pl.program_id(0) * rows
     first = slots == target_ref[0:1, :]
     second = slots == target_ref[1:2, :]
-    selector = jnp.where(first | second, 1.0, 0.0).astype(BF16)
+    inverse = lax.rsqrt((own_ref[...] + peer_ref[...]) / D + EPSILON)
+    inverse_ref[...] = inverse
+    both = jnp.where(first | second, 1.0, 0.0)
+    selector = both.astype(BF16)
+    scale = jnp.sum(both * inverse, axis=1, keepdims=True)
     weight = jnp.where(first, weight_ref[0:1, :], 0.0) + jnp.where(second, weight_ref[1:2, :], 0.0)
     weight = jnp.sum(weight, axis=1, keepdims=True)
     sel_ref[...] = selector
-    out_ref[...] = (weight * dot_nn(selector, cot_ref[...])).astype(BF16)
-
-
-def inputs_body(own_ref, peer_ref, sel_ref, stream_ref, gain_ref, rows_ref, out_ref):
-    inverse = lax.rsqrt((own_ref[...] + peer_ref[...]) / D + EPSILON)
-    selector = sel_ref[...]
-    scale = jnp.sum(selector.astype(F32) * inverse, axis=1, keepdims=True)
     inputs = dot_nn(selector, stream_ref[...])
-    out_ref[...] = (inputs * scale * gain_ref[...]).astype(BF16)
-
-
-def whole_block(*shape):
-    return pl.BlockSpec(shape, lambda i: (0, 0))
-
-
-def grad_rows(target, weights, cot, slots, steps):
-    tokens, width = cot.shape
+    out_ref[:, :width] = (inputs * scale * gain_ref[...]).astype(BF16)
+    grads = dot_nn(selector, cot_ref[...])
+    out_ref[:, width:] = (weight * grads).astype(BF16)
+
+
+def build_rows(target, weights, own_squares, peer_squares, stream, cot, gain, slots):
+    tokens, width = stream.shape
+    steps = 4
     rows = slots // steps
-    return pl.pallas_call(
-        grads_body,
+
+    def whole(*shape):
+        return pl.BlockSpec(shape, lambda i: (0, 0))
+
+    return pl.pallas_call(
+        rows_body,
         grid=(steps,),
-        in_specs=[whole_block(2, tokens), whole_block(2, tokens), whole_block(tokens, width)],
+        in_specs=[
+            IN_VMEM,
+            IN_VMEM,
+            IN_VMEM,
+            IN_VMEM,
+            whole(tokens, width),
+            whole(tokens, width),
+            whole(1, width),
+        ],
         out_specs=(
-            pl.BlockSpec((rows, width), lambda i: (i, 1)),
+            pl.BlockSpec((rows, 2 * width), lambda i: (i, 0)),
             pl.BlockSpec((rows, tokens), lambda i: (i, 0)),
+            whole(1, tokens),
         ),
         out_shape=(
             jax.ShapeDtypeStruct((slots, 2 * width), BF16),
             jax.ShapeDtypeStruct((slots, tokens), BF16),
+            jax.ShapeDtypeStruct((1, tokens), F32),
         ),
-        name="grad_rows",
-        cost_estimate=cost(2 * slots * tokens * width, slots * width * 2),
-    )(target, weights, cot)
-
-
-def input_rows(own_squares, peer_squares, selector, stream, gain, rows_in, steps):
-    tokens, width = stream.shape
-    slots = selector.shape[0]
-    rows = slots // steps
-    return pl.pallas_call(
-        inputs_body,
-        grid=(steps,),
-        in_specs=[
-            whole_block(1, tokens),
-            whole_block(1, tokens),
-            pl.BlockSpec((rows, tokens), lambda i: (i, 0)),
-            whole_block(tokens, width),
-            whole_block(1, width),
-            pl.BlockSpec(memory_space=pl.ANY),
-        ],
-        out_specs=pl.BlockSpec((rows, width), lambda i: (i, 0)),
-        out_shape=jax.ShapeDtypeStruct((slots, 2 * width), BF16),
-        input_output_aliases={5: 0},
-        name="input_rows",
-        cost_estimate=cost(2 * slots * tokens * width, slots * width * 2),
-    )(own_squares, peer_squares, selector, stream, gain, rows_in)
+        name="build_rows",
+        cost_estimate=cost(4 * slots * tokens * width, slots * width * 4),
+    )(target, weights, own_squares, peer_squares, stream, cot, gain)
 
 
 def own_body(
@@ -199,58 +192,59 @@
 
 
 def peer_body(
-    peer_ref, gate_w, up_w, down_w, gate_in, up_in, grad_in,
-    hidden_ref, gate_ref, up_ref, theirs_ref,
+    start, peer_hbm, gate_w, up_w, down_w, gate_in, up_in, grad_in,
+    hidden_hbm, gate_ref, up_ref, theirs_ref, peer_ref, hidden_ref, sems,
 ):
     rows, double = peer_ref.shape
     width = double // 2
-    step = rows // EXPERT_BLOCKS
-
-    def block(i, carry):
-        at = pl.ds(i * step, step)
-        x, y = peer_ref[at, :width], peer_ref[at, width:]
-        gate_lin = gate_in[at, :] + dot_nn(x, gate_w[...])
-        up_lin = up_in[at, :] + dot_nn(x, up_w[...])
-        hidden_grad = grad_in[at, :] + dot_nt(y, down_w[...])
-        sig = jax.nn.sigmoid(gate_lin)
-        silu = gate_lin * sig
-        hidden_ref[at, :] = (silu * up_lin).astype(BF16)
-        gate_pre = (hidden_grad * up_lin * sig * (1.0 + gate_lin * (1.0 - sig))).astype(BF16)
-        up_pre = (hidden_grad * silu).astype(BF16)
-        gate_ref[at, :] = gate_pre
-        up_ref[at, :] = up_pre
-        theirs_ref[at, :] = (dot_nt(gate_pre, gate_w[...]) + dot_nt(up_pre, up_w[...])).astype(BF16)
-        return carry
-
-    lax.fori_loop(0, EXPERT_BLOCKS, block, 0)
-
-
-def mine_body(gate_ref, up_ref, gate_w, up_w, mine_ref):
-    step = mine_ref.shape[0] // EXPERT_BLOCKS
-
-    def block(i, carry):
-        at = pl.ds(i * step, step)
-        part = dot_nt(gate_ref[at, :], gate_w[...]) + dot_nt(up_ref[at, :], up_w[...])
-        mine_ref[at, :] = part.astype(BF16)
-        return carry
-
-    lax.fori_loop(0, EXPERT_BLOCKS, block, 0)
-
-
-def add_body(mine_ref, other_ref, out_ref, scratch, sems):
+    half = rows // 2
+    copies = []
+    for i in range(2):
+        source = peer_hbm.at[pl.ds(start + i * half, half), :]
+        copies.append(
+            pltpu.make_async_copy(source, peer_ref.at[pl.ds(i * half, half), :], sems.at[i])
+        )
+        copies[i].start()
+    for copy in copies:
+        copy.wait()
+    at = pl.ds(start, rows)
+    x, y = peer_ref[:, :width], peer_ref[:, width:]
+    gate_lin = gate_in[at, :] + dot_nn(x, gate_w[...])
+    up_lin = up_in[at, :] + dot_nn(x, up_w[...])
+    hidden_grad = grad_in[at, :] + dot_nt(y, down_w[...])
+    sig = jax.nn.sigmoid(gate_lin)
+    silu = gate_lin * sig
+    hidden_ref[...] = (silu * up_lin).astype(BF16)
+    keep = pltpu.make_async_copy(hidden_ref, hidden_hbm, sems.at[2])
+    keep.start()
+    gate_pre = (hidden_grad * up_lin * sig * (1.0 + gate_lin * (1.0 - sig))).astype(BF16)
+    up_pre = (hidden_grad * silu).astype(BF16)
+    gate_ref[...] = gate_pre
+    up_ref[...] = up_pre
+    theirs_ref[...] = (dot_nt(gate_pre, gate_w[...]) + dot_nt(up_pre, up_w[...])).astype(BF16)
+    keep.wait()
+
+
+def mine_body(gate_a, gate_b, up_a, up_b, gate_w, up_w, mine_ref):
+    half = mine_ref.shape[0] // 2
+    for i, (gate_ref, up_ref) in enumerate(((gate_a, up_a), (gate_b, up_b))):
+        part = dot_nt(gate_ref[...], gate_w[...]) + dot_nt(up_ref[...], up_w[...])
+        mine_ref[pl.ds(i * half, half), :] = part.astype(BF16)
+
+
+def add_body(mine_ref, other_a, other_b, out_ref, scratch, sems):
     blocks, step, _ = scratch.shape
     copies = []
     for i in range(blocks):
         at = pl.ds(i * step, step)
-        total = mine_ref[at, :].astype(F32) + other_ref[at, :].astype(F32)
+        other = (other_a, other_b)[2 * i // blocks]
+        from_other = pl.ds(i % (blocks // 2) * step, step)
+        total = mine_ref[at, :].astype(F32) + other[from_other, :].astype(F32)
         scratch[i] = total.astype(BF16)
         copies.append(pltpu.make_async_copy(scratch.at[i], out_ref.at[at, :], sems.at[i]))
         copies[-1].start()
     for copy in copies:
         copy.wait()
-
-
-IN_VMEM = pl.BlockSpec(memory_space=pltpu.VMEM)
 
 
 def in_hbm(array):
@@ -275,7 +269,7 @@
     shapes = [((rows, units), F32)] * 3 + [((width, units), BF16)] * 4 + [((units, width), BF16)]
     return pl.pallas_call(
         own_body,
-        in_specs=[pl.BlockSpec(memory_space=pltpu.SMEM)] + [pl.BlockSpec(memory_space=pl.ANY)] * 4,
+        in_specs=[IN_SMEM] + [IN_HBM] * 4,
         out_specs=[IN_VMEM] * len(shapes),
         out_shape=[jax.ShapeDtypeStruct(s, d) for s, d in shapes],
         scratch_shapes=[
@@ -289,26 +283,43 @@
     )(core, *[in_hbm(array) for array in (own, gate_w, up_w, down_w)])
 
 
-def expert_peer(peer, gate_w, up_w, down_w, *parts):
-    rows, units = peer.shape[0], gate_w.shape[1]
-    outs = [((rows, units), BF16)] * 3 + [((rows, peer.shape[1] // 2), BF16)]
-    flops = 5 * rows * peer.shape[1] * units
-    return on_chip(peer_body, outs, flops, 16, peer, gate_w, up_w, down_w, *parts)
-
-
-def expert_mine(gate_pre, up_pre, gate_w, up_w):
-    rows, width = gate_pre.shape[0], gate_w.shape[0]
+def expert_peer(start, peer, gate_w, up_w, down_w, *parts):
+    rows, double = peer.shape[0] // 2, peer.shape[1]
+    units = gate_w.shape[1]
+    outs = [((rows, units), BF16)] * 2 + [((rows, double // 2), BF16)]
+
+    def body(*refs):
+        peer_body(start, *refs)
+
+    return pl.pallas_call(
+        body,
+        in_specs=[IN_HBM] + [IN_VMEM] * 6,
+        out_specs=[IN_HBM] + [IN_VMEM] * len(outs),
+        out_shape=[pltpu.HBM((rows, units), BF16)] + [jax.ShapeDtypeStruct(s, d) for s, d in outs],
+        scratch_shapes=[
+            pltpu.VMEM((rows, double), BF16),
+            pltpu.VMEM((rows, units), BF16),
+            pltpu.SemaphoreType.DMA((3,)),
+        ],
+        compiler_params=pltpu.CompilerParams(vmem_limit_bytes=16 * 1024 * 1024),
+        name="expert_peer",
+        cost_estimate=cost(5 * rows * double * units, 8 * rows * double),
+    )(in_hbm(peer), gate_w, up_w, down_w, *parts)
+
+
+def expert_mine(gate_a, gate_b, up_a, up_b, gate_w, up_w):
+    rows, width = 2 * gate_a.shape[0], gate_w.shape[0]
     flops = 4 * rows * width * gate_w.shape[1]
     outs = [((rows, width), BF16)]
-    return on_chip(mine_body, outs, flops, 8, gate_pre, up_pre, gate_w, up_w)[0]
-
-
-def add_parts(mine, other):
+    return on_chip(mine_body, outs, flops, 8, gate_a, gate_b, up_a, up_b, gate_w, up_w)[0]
+
+
+def add_parts(mine, other_a, other_b):
     rows, width = mine.shape
     blocks = 8
     return pl.pallas_call(
         add_body,
-        in_specs=[IN_VMEM] * 2,
+        in_specs=[IN_VMEM] * 3,
         out_specs=pl.BlockSpec(memory_space=pltpu.HBM),
         out_shape=pltpu.HBM(mine.shape, BF16),
         scratch_shapes=[
@@ -318,7 +329,17 @@
         compiler_params=pltpu.CompilerParams(vmem_limit_bytes=8 * 1024 * 1024),
         name="add_parts",
         cost_estimate=cost(mine.size, 6 * mine.size),
-    )(mine, other)
+    )(mine, other_a, other_b)
+
+
+def tick_body(in_ref, out_ref):
+    out_ref[...] = in_ref[...]
+
+
+def tick(array):
+    return pl.pallas_call(
+        tick_body, out_shape=jax.ShapeDtypeStruct(array.shape, array.dtype), name="tick"
+    )(array)
 
 
 def product_body(left_ref, right_ref, out_ref):
@@ -336,12 +357,28 @@
     return on_chip(body, outs, flops, 8, left, right, *part)[0]
 
 
-def mixer_body(core_ref, grad_ref, peer_ref, proj_ref, gate_ref, conv_ref, delta_ref, out_ref):
+def mixer_body(
+    core_ref, grad_hbm, peer_hbm, proj_hbm, gate_ref, conv_ref, delta_ref, out_ref,
+    grad_ref, peer_ref, proj_ref, sems,
+):
     width = grad_ref.shape[1]
     mine = pl.multiple_of(core_ref[0] * width, width)
     other = pl.multiple_of((1 - core_ref[0]) * width, width)
-    mixer_grad = dot_nn(grad_ref[...], proj_ref[pl.ds(mine, width), :])
-    mixer_grad = mixer_grad + dot_nn(peer_ref[...], proj_ref[pl.ds(other, width), :])
+    moves = (
+        (proj_hbm.at[pl.ds(mine, width), :], proj_ref.at[0]),
+        (grad_hbm, grad_ref),
+        (proj_hbm.at[pl.ds(other, width), :], proj_ref.at[1]),
+        (peer_hbm, peer_ref),
+    )
+    copies = [pltpu.make_async_copy(a, b, sems.at[i]) for i, (a, b) in enumerate(moves)]
+    for copy in copies:
+        copy.start()
+    copies[0].wait()
+    copies[1].wait()
+    mixer_grad = dot_nn(grad_ref[...], proj_ref[0])
+    copies[2].wait()
+    copies[3].wait()
+    mixer_grad = mixer_grad + dot_nn(peer_ref[...], proj_ref[1])
     delta_ref[...] = mixer_grad * gate_ref[...].astype(F32)
     out_ref[...] = (mixer_grad * conv_ref[...]).astype(BF16)
 
@@ -351,42 +388,53 @@
     channels = proj.shape[1]
     return pl.pallas_call(
         mixer_body,
-        in_specs=[pl.BlockSpec(memory_space=pltpu.SMEM)] + [IN_VMEM] * 5,
+        in_specs=[IN_SMEM] + [IN_HBM] * 3 + [IN_VMEM] * 2,
         out_specs=[IN_VMEM] * 2,
         out_shape=[
             jax.ShapeDtypeStruct((rows, channels), F32),
             jax.ShapeDtypeStruct((rows, channels), BF16),
         ],
+        scratch_shapes=[
+            pltpu.VMEM((rows, width), BF16),
+            pltpu.VMEM((rows, width), BF16),
+            pltpu.VMEM((2, width, channels), BF16),
+            pltpu.SemaphoreType.DMA((4,)),
+        ],
         compiler_params=pltpu.CompilerParams(vmem_limit_bytes=12 * 1024 * 1024),
         name="mixer_back",
         cost_estimate=cost(4 * rows * width * channels, 8 * 1024 * 1024),
-    )(core, grad, peer, proj, gate, conv)
+    )(core, in_hbm(grad), in_hbm(peer), in_hbm(proj), gate, conv)
 
 
 def weights_body(
-    core_ref, own_x, own_y, peer_x, peer_y, hidden_ref, gate_ref, up_ref,
+    core_ref, own_x, own_y, peer_x, peer_y, hidden_a, hidden_b, gate_a, gate_b, up_a, up_b,
     gate_out, up_out, down_out,
 ):
-    def emit(x, y):
-        gate_out[...] = dot_tn(x, gate_ref[...])
-        up_out[...] = dot_tn(x, up_ref[...])
-        down_out[...] = dot_tn(hidden_ref[...], y)
-
-    half = pl.num_programs(0) // 2
-
-    @pl.when(pl.program_id(0) < half)
+    half = hidden_a.shape[0]
+
+    def emit(x_ref, y_ref):
+        x_a, x_b = x_ref[:half, :], x_ref[half:, :]
+        gate_out[...] = dot_tn(x_a, gate_a[...]) + dot_tn(x_b, gate_b[...])
+        up_out[...] = dot_tn(x_a, up_a[...]) + dot_tn(x_b, up_b[...])
+        down_out[...] = dot_tn(hidden_a[...], y_ref[:half, :]) + dot_tn(
+            hidden_b[...], y_ref[half:, :]
+        )
+
+    steps = pl.num_programs(0) // 2
+
+    @pl.when(pl.program_id(0) < steps)
     def _():
-        emit(own_x[...], own_y[...])
-
-    @pl.when(pl.program_id(0) >= half)
+        emit(own_x, own_y)
+
+    @pl.when(pl.program_id(0) >= steps)
     def _():
-        emit(peer_x[...], peer_y[...])
-
-
-def weight_grads(core, own, peer, hidden, gate_pre, up_pre):
+        emit(peer_x, peer_y)
+
+
+def weight_grads(core, own, peer, *halves):
     rows, double = own.shape
     width = double // 2
-    units = hidden.shape[1]
+    units = halves[0].shape[1]
     chunk = 256
     half = width // chunk
 
@@ -400,7 +448,7 @@
         side = jnp.where(s < half, c[0], 1 - c[0])
         return side * half + jnp.where(s < half, s, s - half)
 
-    whole = pl.BlockSpec((rows, units), lambda s, c: (0, 0))
+    whole = pl.BlockSpec((rows // 2, units), lambda s, c: (0, 0))
     tall = pl.BlockSpec((chunk, units), lambda s, c: (place(s, c), 0))
     wide = pl.BlockSpec((units, chunk), lambda s, c: (0, place(s, c)))
     return pl.pallas_call(
@@ -408,7 +456,7 @@
         grid_spec=pltpu.PrefetchScalarGridSpec(
             num_scalar_prefetch=1,
             grid=(2 * half,),
-            in_specs=[own_at(0), own_at(half), peer_at(0), peer_at(half), whole, whole, whole],
+            in_specs=[own_at(0), own_at(half), peer_at(0), peer_at(half)] + [whole] * 6,
             out_specs=[tall, tall, wide],
         ),
         out_shape=[
@@ -419,7 +467,7 @@
         compiler_params=pltpu.CompilerParams(vmem_limit_bytes=VMEM),
         name="weight_grads",
         cost_estimate=cost(12 * rows * width * units, 24 * width * units),
-    )(core, own, own, peer, peer, hidden, gate_pre, up_pre)
+    )(core, own, own, peer, peer, *halves)
 
 
 def stage(
@@ -448,9 +496,11 @@
 
     squares, target = find_slots(stream, routes.T, experts, capacity)
     peer_squares = swap(squares)
-    rows, selector = grad_rows(target, route_weights.T, cotangent, slots, 4)
-    rows = input_rows(squares, peer_squares, selector, stream, gain_row, rows, 4)
-    own = exchange(rows.reshape(experts, capacity, 2 * width), SP).reshape(slots, 2 * width)
+    rows, selector, inverse_row = build_rows(
+        target, route_weights.T, squares, peer_squares, stream, cotangent, gain_row, slots
+    )
+    own = exchange(rows.reshape(experts, capacity, 2 * width), SP)
+    own = own.reshape(slots, 2 * width)
 
     input_float = conv_input.astype(F32)
     cgate_float = conv_cgate.astype(F32)
@@ -465,7 +515,6 @@
         + conv_taps[2][None, :] * extended[2:]
     )
     mixer_out = (bgate_float * conv_out).astype(BF16)
-    own, mixer_out = lax.optimization_barrier((own, mixer_out))
     line = lax.axis_size("sp_0")
     spot = lax.axis_index("sp_0")
     token_half = tok_count // 2
@@ -474,6 +523,7 @@
     def half_of(array, which, dim):
         return lax.dynamic_slice_in_dim(array, which * token_half, token_half, dim)
 
+    inverse_row = tick(inverse_row)
     peer = swap(own)
     around = [mixer_out]
     for step in range(1, line):
@@ -481,14 +531,16 @@
     gate_part, up_part, grad_part, gate_own, up_own, gate_peer, up_peer, down_peer = expert_own(
         core_arg, own, gate_weight[0], up_weight[0], down_weight[0]
     )
-    hidden, gate_pre, up_pre, part_theirs = expert_peer(
-        peer, gate_peer, up_peer, down_peer, gate_part, up_part, grad_part
-    )
-    other = swap(part_theirs)
-    part_mine = expert_mine(gate_pre, up_pre, gate_own, up_own)
-    row_grads = add_parts(part_mine, other)
+    more = (gate_peer, up_peer, down_peer, gate_part, up_part, grad_part)
+    hidden_a, gate_a, up_a, theirs_a = expert_peer(0, peer, *more)
+    other_a = swap(theirs_a)
+    hidden_b, gate_b, up_b, theirs_b = expert_peer(slots // 2, peer, *more)
+    other_b = swap(theirs_b)
+    part_mine = expert_mine(gate_a, gate_b, up_a, up_b, gate_own, up_own)
+    row_grads = add_parts(part_mine, other_a, other_b)
     returned = exchange(row_grads.reshape(experts, capacity, width), SP).reshape(slots, width)
-    grads_w = weight_grads(core_arg, own, peer, hidden, gate_pre, up_pre)
+    halves = (hidden_a, hidden_b, gate_a, gate_b, up_a, up_b)
+    grads_w = weight_grads(core_arg, own, peer, *halves)
     around = jnp.stack(around)
     mixers = jnp.concatenate(
         [lax.dynamic_slice_in_dim(around, (spot - k) % line, 1, 0) for k in range(line)], axis=0
@@ -502,7 +554,7 @@
     normed_grad = dot_tn(selector, returned)
     stream_float = stream.astype(F32)
     cot_float = cotangent.astype(F32)
-    inverse = lax.rsqrt((squares + peer_squares)[0] / D + EPSILON)[:, None]
+    inverse = inverse_row[0][:, None]
     cross_part = jnp.sum(stream_float * gain_row * normed_grad, axis=1)
     cross = cross_part + swap(cross_part)
     stream_grad = (
@@ -519,15 +571,16 @@
     parts = [low[:, :quarter], low[:, quarter:], high[:, :quarter], high[:, quarter:]]
     sent = jnp.stack(parts)
     grads_mine = exchange(sent, "sp_0").reshape(line * token_half, quarter)
+    delta, bgate_grad = mixer_back(core_arg, stream_grad, grad_peer, out_proj, conv_bgate, conv_out)
+    next_rim = shifted(delta[:2], SP, -1)
+    last_rows = tick(delta[-8:])
     grads_theirs = swap(grads_mine)
     proj_part = product(grads_theirs, mixers_theirs, product(grads_mine, mixers_mine))
     plane = lax.axis_size(("sp_1", "sp_2"))
     arrived = exchange(proj_part.reshape(plane, quarter // plane, channels), ("sp_1", "sp_2"))
     proj_grad = arrived.sum(axis=0)
 
-    delta, bgate_grad = mixer_back(core_arg, stream_grad, grad_peer, out_proj, conv_bgate, conv_out)
-    next_rim = shifted(delta[:2], SP, -1)
-    extended_back = jnp.concatenate([delta, next_rim], axis=0)
+    extended_back = jnp.concatenate([delta[:-8], last_rows, next_rim], axis=0)
     gated_grad = (
         conv_taps[2][None, :] * extended_back[:-2]
         + conv_taps[1][None, :] * extended_back[1:-1]

time: 213 us -> 211 us (level)
  blocking collectives: 12.6 us -> 77.2 us
  waiting for transfers between devices: 104 us -> 46.9 us
  starting transfers between devices: 37.5 us -> 24 us
  other arithmetic: 4.83 us -> 8.01 us
  Pallas kernels: 46.6 us -> 48.8 us
    all_to_all x1 -> x2, blocking collectives: 12.6 us -> 77.2 us  [exchange(): return lax.all_to_all(value, axis, split_axis=0, concat_axis=0, tiled=True)]
    ppermute x2, waiting for transfers between devices: 55.3 us -> 7.25 us  [shifted(): lax.ppermute(value, axis, [(source, source + steps) for source in range(l...]
    all_to_all x3 -> x2, starting transfers between devices: 27.5 us -> 14.6 us  [exchange(): return lax.all_to_all(value, axis, split_axis=0, concat_axis=0, tiled=True)]
    pallas_call x5 -> x8, Pallas kernels: 16.9 us -> 27.9 us  [the longest x2 9.78 us: expert_peer(): pl.pallas_call(body, in_specs=[IN_HBM] + [IN_VMEM] * 6, out_specs=[IN_HBM...]
    pallas_call x4 -> x3, Pallas kernels: 13 us -> 4.29 us  [on_chip(): pl.pallas_call(body, in_specs=[IN_VMEM] * len(args), out_specs=[IN_VMEM]...]
    all_to_all x3 -> x2, waiting for transfers between devices: 8.19 us -> 0.71 us  [exchange(): return lax.all_to_all(value, axis, split_axis=0, concat_axis=0, tiled=True)]
    ppermute x6 -> x7, waiting for transfers between devices: 7.26 us -> 6.11 us  [swap(): return lax.ppermute(value, 'tp', [(0, 1), (1, 0)])]
  transfers between devices with their start and end apart: 14 -> 14, of which waited for: 12 -> 9; matrix products, arithmetic and copies ran while one was open for 2% -> 2% of each run, Pallas kernels for 14% -> 17%
where the time goes in v4:
time: 211 us; the launch traced here: 210 us
  blocking collectives  77.2 us (37%)
  Pallas kernels  48.8 us (23%)
  waiting for transfers between devices  46.9 us (22%)
  starting transfers between devices  24 us (11%)
  other arithmetic  8.01 us (4%)
  matrix products  2.59 us (1%)
    all_to_all x2, blocking collectives, exchange(): return lax.all_to_all(value, axis, split_axis=0, concat_axis=0, tiled=True)  77.2 us
    ppermute x3, waiting for transfers between devices, turned(): lax.ppermute(value, axis, [(i, (i + steps) % count) for i in range(count)])  32.8 us
    all_to_all x2, starting transfers between devices, exchange(): return lax.all_to_all(value, axis, split_axis=0, concat_axis=0, tiled=True)  14.6 us
    pallas_call x1, Pallas kernels, weight_grads(): pl.pallas_call(weights_body, grid_spec=pltpu.PrefetchScalarGridSpec(num_s...  14.6 us
    pallas_call x2, Pallas kernels, expert_peer(): pl.pallas_call(body, in_specs=[IN_HBM] + [IN_VMEM] * 6, out_specs=[IN_HBM...  9.78 us
    ppermute x2, waiting for transfers between devices, shifted(): lax.ppermute(value, axis, [(source, source + steps) for source in range(l...  7.25 us
    ppermute x7, waiting for transfers between devices, swap(): return lax.ppermute(value, 'tp', [(0, 1), (1, 0)])  6.11 us
    pallas_call x1, Pallas kernels, expert_own(): pl.pallas_call(own_body, in_specs=[IN_SMEM] + [IN_HBM] * 4, out_specs=[IN...  5.95 us
  transfers between devices with their start and end apart: 14, of which 9 were waited for; matrix products, arithmetic and copies ran while one was open for 2% of the time, Pallas kernels for 17%

profile of v4, /device:TPU:0, one launch (start us, length us, event | category | flops | bytes accessed | tf_op | source)
XLA Modules:
  0.0 210.2 jit_solution(11749050551788840262)
XLA Ops:
  0.6 2.1 find_slots.1
  4.6 4.8 %build_rows.1 = (bf16[1024,2048]{1,0:T(8,128)(2,1)}, bf16[1024,256]{1,0:T(8,128)(2,1)}, f32[1,256]{1,0:T(1,128)}) custom-call(s32[2,256]{1,0:T(2,128)} %get-tuple-element.40.target_ref, f32[2,256]{1,0:T(2,128)} %bitcast.64, f32[1,256]{1,0:T(1,128)} %get-tuple-element.41.own_ref, f32[1,256]{1,0:T(1,128)} %copy-done.13, bf16[256,1024]{1,0:T(8,128)(2,1)} %stream_ref.1, ...), custom_call_target="tpu_custom_call" | custom-call | flops 1073741824 | bytes 4194304 | tf_op jit(solution)/shard_map/build_rows/pallas_call | solution.py:127
  9.4 64.5 %all_to_all.20 = bf16[64,16,2048]{2,1,0:T(8,128)(2,1)} all-to-all(bf16[64,16,2048]{2,1,0:T(8,128)(2,1)} %bitcast.47), channel_id=1, replica_groups=mesh['sp_0'=4,'sp_1'=4,'sp_2'=4,'tp'=2] {'sp_0','sp_1','sp_2'}, dimensions={0} | all-to-all | bytes 8388608 | tf_op jit(solution)/shard_map/all_to_all | solution.py:42
  73.9 6.0 %expert_own.1 = (f32[1024,512]{1,0:T(8,128)S(1)}, f32[1024,512]{1,0:T(8,128)S(1)}, f32[1024,512]{1,0:T(8,128)S(1)}, bf16[1024,512]{1,0:T(8,128)(2,1)S(1)}, bf16[...) custom-call(s32[1]{0:T(128)} %bitcast.6.core_ref, ...), custom_call_target="tpu_custom_call" | custom-call | flops 3221225472 | bytes 10485760 | tf_op jit(solution)/shard_map/expert_own/pallas_call | solution.py:270
  79.9 1.5 collective-permute-done.1.refs_0_.peer_x.peer_y
  81.4 4.7 %expert_peer.2 = (bf16[512,512]{1,0:T(8,128)(2,1)}, bf16[512,512]{1,0:T(8,128)(2,1)S(1)}, bf16[512,512]{1,0:T(8,128)(2,1)S(1)}, bf16[512,1024]{1,0:T(8,128)(2,1)S(1)}) custom-call(bf16[1024,2048]{1,0:T(8,128)(2,1)} %collective-permute-done.1.refs_0_.peer_x.peer_y, bf16[1024,512]{1,0:T(8,128)(2,1)S(1)} %get-tuple-element.45.refs_1_, ...), custom_call_target="tpu_custom_call" | custom-call | flops 2684354560 | bytes 8388608 | tf_op jit(solution)/shard_map/expert_peer/pallas_call | solution.py:294
  86.4 5.0 %expert_peer.3 = (bf16[512,512]{1,0:T(8,128)(2,1)}, bf16[512,512]{1,0:T(8,128)(2,1)S(1)}, bf16[512,512]{1,0:T(8,128)(2,1)S(1)}, bf16[512,1024]{1,0:T(8,128)(2,1)S(1)}) custom-call(bf16[1024,2048]{1,0:T(8,128)(2,1)} %collective-permute-done.1.refs_0_.peer_x.peer_y, bf16[1024,512]{1,0:T(8,128)(2,1)S(1)} %get-tuple-element.45.refs_1_, ...), custom_call_target="tpu_custom_call" | custom-call | flops 2684354560 | bytes 8388608 | tf_op jit(solution)/shard_map/expert_peer/pallas_call | solution.py:294
  91.7 2.6 %collective-permute-start.4 = (bf16[2,2,512]{2,1,0:T(2,128)(2,1)S(1)}, bf16[2,2,512]{2,1,0:T(2,128)(2,1)S(1)}, u32[]{:S(2)}, u32[]{:S(2)}) collective-permute-start(bf16[2,2,512]{2,1,0:T(2,128)(2,1)S(1)} %pad_maximum_fusion.5), channel_id=1, source_target_pairs={{0,2},{2,4},{4,6},{6,8},{8,10},{10,12},{12,14},{14,16},{16,18},{18... | collective-permute-start | bytes 12296 | tf_op jit(solution)/shard_map/ppermute | solution.py:48
  94.4 2.4 %shard_map.188.mine_ref = bf16[1024,1024]{1,0:T(8,128)(2,1)S(1)} custom-call(bf16[512,512]{1,0:T(8,128)(2,1)S(1)} %get-tuple-element.51.gate_a, bf16[512,512]{1,0:T(8,128)(2,1)S(1)} %get-tuple-element.52.gate_b, bf16[512,512]{1,0:T(8,128)(2,1)S(1)} %get-tuple-element.53.up_a, bf16[512,512]{1,0:T(8,128)(2,1)S(1)} %get-tuple-element.54.up_b, ...), custom_call_target="tpu_custom_call" | custom-call | flops 2147483648 | bytes 16777216 | tf_op jit(solution)/shard_map/pallas_call | solution.py:255
  96.8 1.5 add_parts.1
  98.4 8.6 %all-to-all-start.1 = ((bf16[64,16,1024]{2,1,0:T(8,128)(2,1)}), bf16[64,16,1024]{2,1,0:T(8,128)(2,1)}, u32[]{:S(2)}, u32[]{:S(2)}) async-start(bf16[64,16,1024]{2,1,0:T(8,128)(2,1)} %bitcast.46), calls=%async_computation.1 | async-start | bytes 4194304 | tf_op jit(solution)/shard_map/all_to_all | solution.py:42
  107.3 3.0 %collective-permute-start.7 = (bf16[256,512]{1,0:T(8,128)(2,1)S(1)}, bf16[256,512]{1,0:T(8,128)(2,1)S(1)}, u32[]{:S(2)}, u32[]{:S(2)}) collective-permute-start(bf16[256,512]{1,0:T(8,128)(2,1)S(1)} %get-tuple-element.74), channel_id=1, source_target_pairs={{0,96},{32,0},{64,32},{96,64},{1,97},{33,1},{65,33},{97,65},{2,98}... | collective-permute-start | bytes 786440 | tf_op jit(solution)/shard_map/ppermute | solution.py:53
  111.9 25.9 %collective-permute-done.7 = bf16[256,512]{1,0:T(8,128)(2,1)S(1)} collective-permute-done((bf16[256,512]{1,0:T(8,128)(2,1)S(1)}, bf16[256,512]{1,0:T(8,128)(2,1)S(1)}, u32[]{:S(2)}, u32[]{:S(2)}) %collective-permute-start.7) | collective-permute-done | bytes 262176 | tf_op jit(solution)/shard_map/ppermute | solution.py:53
  137.8 1.9 collective-permute-done.6
  139.6 5.1 %collective-permute-done.5 = bf16[256,512]{1,0:T(8,128)(2,1)S(1)} collective-permute-done((bf16[256,512]{1,0:T(8,128)(2,1)S(1)}, bf16[256,512]{1,0:T(8,128)(2,1)S(1)}, u32[]{:S(2)}, u32[]{:S(2)}) %collective-permute-start.5) | collective-permute-done | bytes 262176 | tf_op jit(solution)/shard_map/ppermute | solution.py:53
  145.2 14.6 %weight_grads.1 = (f32[2048,512]{1,0:T(8,128)}, f32[2048,512]{1,0:T(8,128)}, f32[512,2048]{1,0:T(8,128)}) custom-call(s32[1]{0:T(128)} %bitcast.6.core_ref, bf16[1024,2048]{1,0:T(8,128)(2,1)} %bitcast.5.own_hbm.own_x.own_y, bf16[1024,2048]{1,0:T(8,128)(2,1)} %bitcast.5.own_hbm.own_x.own_y, bf16[1024,2048]{1,0:T(8,128)(2,1)} %collective-permute-done.1.refs_0_.peer_x.peer_y, ...), custom_call_target="tpu_custom_call" | custom-call | flops 6442450944 | bytes 12582912 | tf_op jit(solution)/shard_map/weight_grads/pallas_call | solution.py:454
  159.8 2.6 %fusion.7 = (f32[256]{0:T(256)S(1)}, f32[256,1024]{1,0:T(8,128)S(1)}) fusion(bf16[256,1024]{1,0:T(8,128)(2,1)S(1)} %copy-done.5, f32[1024]{0:T(1024)S(1)} %copy-done.11, bf16[1024,256]{1,0:T(8,128)(2,1)} %get-tuple-element.43, bf16[1024,1024]{1,0:T(8,128)(2,1)} %bitcast.11), kind=kOutput, calls=%fused_computation.9 | convolution fusion | flops 537919232 | bytes 4199424 | tf_op jit(solution)/shard_map/dot_general | solution.py:30
  163.7 2.3 %fusion.5.grad_hbm = bf16[256,1024]{1,0:T(8,128)(2,1)} fusion(bf16[256,1024]{1,0:T(8,128)(2,1)S(1)} %copy-done.5, f32[256,1024]{1,0:T(8,128)S(1)} %get-tuple-element.92, bf16[256,1024]{1,0:T(8,128)(2,1)} %cot_ref.1, f32[256]{0:T(256)S(1)} %add.67, f32[1024]{0:T(1024)S(1)} %copy-done.11, f32[256]{0:T(256)} %bitcast.59), kind=kLoop, calls=%fused_computation.7 | loop fusion | flops 3145728 | bytes 2627584 | tf_op jit(solution)/shard_map/convert_element_type | solution.py:564
  166.5 1.7 collective-permute-done.9.peer_hbm
  169.7 12.7 %all_to_all.21 = bf16[4,128,512]{2,1,0:T(8,128)(2,1)S(1)} all-to-all(bf16[4,128,512]{2,1,0:T(8,128)(2,1)S(1)} %pad_maximum_fusion.4), channel_id=1, replica_groups=mesh['sp_0'=4,'sp_1'=4,'sp_2'=4,'tp'=2] {'sp_0'}, dimensions={0} | all-to-all | bytes 1048576 | tf_op jit(solution)/shard_map/all_to_all | solution.py:42
  185.7 5.9 %all-to-all-start.3 = ((f32[16,32,512]{2,1,0:T(8,128)}), f32[16,32,512]{2,1,0:T(8,128)S(1)}, u32[]{:S(2)}, u32[]{:S(2)}) async-start(f32[16,32,512]{2,1,0:T(8,128)} %bitcast.29), calls=%async_computation.3 | async-start | bytes 2097152 | tf_op jit(solution)/shard_map/all_to_all | solution.py:42
  191.7 3.3 %mixer_back.1 = (f32[256,512]{1,0:T(8,128)S(1)}, bf16[256,512]{1,0:T(8,128)(2,1)}) custom-call(s32[1]{0:T(128)} %bitcast.6.core_ref, bf16[256,1024]{1,0:T(8,128)(2,1)} %fusion.5.grad_hbm, bf16[256,1024]{1,0:T(8,128)(2,1)} %copy-done.6, bf16[2048,512]{1,0:T(8,128)(2,1)} %proj_hbm.1, bf16[256,512]{1,0:T(8,128)(2,1)S(1)} %copy-done, ...), custom_call_target="tpu_custom_call" | custom-call | flops 536870912 | bytes 8388608 | tf_op jit(solution)/shard_map/mixer_back/pallas_call | solution.py:389
  198.3 7.2 %collective-permute-done.11 = f32[2,512]{1,0:T(2,128)S(1)} collective-permute-done((f32[2,512]{1,0:T(2,128)S(1)}, f32[2,512]{1,0:T(2,128)S(1)}, u32[]{:S(2)}, u32[]{:S(2)}) %collective-permute-start.11) | collective-permute-done | bytes 4128 | tf_op jit(solution)/shard_map/ppermute | solution.py:48
  206.4 1.6 fusion.13
  (71 shorter events, 17.5 us)
Async XLA Ops:
  2.7 1.4 collective-permute-start
  73.9 7.5 %collective-permute-start.1 = (bf16[1024,2048]{1,0:T(8,128)(2,1)}, bf16[1024,2048]{1,0:T(8,128)(2,1)}, u32[]{:S(2)}, u32[]{:S(2)}) collective-permute-start(bf16[1024,2048]{1,0:T(8,128)(2,1)} %bitcast.5.own_hbm.own_x.own_y), channel_id=1, source_target_pairs={{0,1},{1,0},{2,3},{3,2},{4,5},{5,4},{6,7},{7,6},{8,9},{9,8},{10,11... | collective-permute-start | bytes 12582920 | tf_op jit(solution)/shard_map/ppermute | solution.py:38
  86.2 8.2 %copy-start.1 = (bf16[512,512]{1,0:T(8,128)(2,1)}, bf16[512,512]{1,0:T(8,128)(2,1)S(1)}, u32[]{:S(2)}) copy-start(bf16[512,512]{1,0:T(8,128)(2,1)S(1)} %get-tuple-element.51.gate_a) | copy-start | bytes 1572868
  86.2 8.2 %copy-start.2 = (bf16[512,512]{1,0:T(8,128)(2,1)}, bf16[512,512]{1,0:T(8,128)(2,1)S(1)}, u32[]{:S(2)}) copy-start(bf16[512,512]{1,0:T(8,128)(2,1)S(1)} %get-tuple-element.53.up_a) | copy-start | bytes 1572868
  86.2 5.5 %copy-start.7 = (bf16[256,512]{1,0:T(8,128)(2,1)S(1)}, bf16[256,512]{1,0:T(8,128)(2,1)}, u32[]{:S(2)}) copy-start(bf16[256,512]{1,0:T(8,128)(2,1)} %param.18) | copy-start | bytes 786436
  86.2 10.6 %collective-permute-start.2 = (bf16[512,1024]{1,0:T(8,128)(2,1)S(1)}, bf16[512,1024]{1,0:T(8,128)(2,1)S(1)}, u32[]{:S(2)}, u32[]{:S(2)}) collective-permute-start(bf16[512,1024]{1,0:T(8,128)(2,1)S(1)} %get-tuple-element.57), channel_id=1, source_target_pairs={{0,1},{1,0},{2,3},{3,2},{4,5},{5,4},{6,7},{7,6},{8,9},{9,8},{10,11... | collective-permute-start | bytes 3145736 | tf_op jit(solution)/shard_map/ppermute | solution.py:38
  91.5 5.3 %collective-permute-start.3 = (bf16[512,1024]{1,0:T(8,128)(2,1)S(1)}, bf16[512,1024]{1,0:T(8,128)(2,1)S(1)}, u32[]{:S(2)}, u32[]{:S(2)}) collective-permute-start(bf16[512,1024]{1,0:T(8,128)(2,1)S(1)} %get-tuple-element.58), channel_id=1, source_target_pairs={{0,1},{1,0},{2,3},{3,2},{4,5},{5,4},{6,7},{7,6},{8,9},{9,8},{10,11... | collective-permute-start | bytes 3145736 | tf_op jit(solution)/shard_map/ppermute | solution.py:38
  91.7 15.3 %collective-permute-start.4 = (bf16[2,2,512]{2,1,0:T(2,128)(2,1)S(1)}, bf16[2,2,512]{2,1,0:T(2,128)(2,1)S(1)}, u32[]{:S(2)}, u32[]{:S(2)}) collective-permute-start(bf16[2,2,512]{2,1,0:T(2,128)(2,1)S(1)} %pad_maximum_fusion.5), channel_id=1, source_target_pairs={{0,2},{2,4},{4,6},{6,8},{8,10},{10,12},{12,14},{14,16},{16,18},{18... | collective-permute-start | bytes 12296 | tf_op jit(solution)/shard_map/ppermute | solution.py:48
  98.3 8.7 %copy-start.12 = (f32[3,512]{1,0:T(4,128)S(1)}, f32[3,512]{1,0:T(4,128)}, u32[]{:S(2)}) copy-start(f32[3,512]{1,0:T(4,128)} %param.21) | copy-start | bytes 18436
  98.4 8.7 %copy-start = (bf16[256,512]{1,0:T(8,128)(2,1)S(1)}, bf16[256,512]{1,0:T(8,128)(2,1)}, u32[]{:S(2)}) copy-start(bf16[256,512]{1,0:T(8,128)(2,1)} %gate_ref.1) | copy-start | bytes 786436
  98.4 61.4 %all-to-all-start.1 = ((bf16[64,16,1024]{2,1,0:T(8,128)(2,1)}), bf16[64,16,1024]{2,1,0:T(8,128)(2,1)}, u32[]{:S(2)}, u32[]{:S(2)}) async-start(bf16[64,16,1024]{2,1,0:T(8,128)(2,1)} %bitcast.46), calls=%async_computation.1 | async-start | bytes 4194304 | tf_op jit(solution)/shard_map/all_to_all | solution.py:42
  107.3 30.5 %collective-permute-start.7 = (bf16[256,512]{1,0:T(8,128)(2,1)S(1)}, bf16[256,512]{1,0:T(8,128)(2,1)S(1)}, u32[]{:S(2)}, u32[]{:S(2)}) collective-permute-start(bf16[256,512]{1,0:T(8,128)(2,1)S(1)} %get-tuple-element.74), channel_id=1, source_target_pairs={{0,96},{32,0},{64,32},{96,64},{1,97},{33,1},{65,33},{97,65},{2,98}... | collective-permute-start | bytes 786440 | tf_op jit(solution)/shard_map/ppermute | solution.py:53
  110.3 29.4 %collective-permute-start.6 = (bf16[256,512]{1,0:T(8,128)(2,1)S(1)}, bf16[256,512]{1,0:T(8,128)(2,1)S(1)}, u32[]{:S(2)}, u32[]{:S(2)}) collective-permute-start(bf16[256,512]{1,0:T(8,128)(2,1)S(1)} %get-tuple-element.74), channel_id=1, source_target_pairs={{0,64},{32,96},{64,0},{96,32},{1,65},{33,97},{65,1},{97,33},{2,66}... | collective-permute-start | bytes 786440 | tf_op jit(solution)/shard_map/ppermute | solution.py:53
  110.9 33.8 %collective-permute-start.5 = (bf16[256,512]{1,0:T(8,128)(2,1)S(1)}, bf16[256,512]{1,0:T(8,128)(2,1)S(1)}, u32[]{:S(2)}, u32[]{:S(2)}) collective-permute-start(bf16[256,512]{1,0:T(8,128)(2,1)S(1)} %get-tuple-element.74), channel_id=1, source_target_pairs={{0,32},{32,64},{64,96},{96,0},{1,33},{33,65},{65,97},{97,1},{2,34}... | collective-permute-start | bytes 786440 | tf_op jit(solution)/shard_map/ppermute | solution.py:53
  145.2 14.6 %copy-start.5 = (bf16[256,1024]{1,0:T(8,128)(2,1)S(1)}, bf16[256,1024]{1,0:T(8,128)(2,1)}, u32[]{:S(2)}) copy-start(bf16[256,1024]{1,0:T(8,128)(2,1)} %stream_ref.1) | copy-start | bytes 1572868
  145.2 14.6 %copy-start.11 = (f32[1024]{0:T(1024)S(1)}, f32[1024]{0:T(1024)}, u32[]{:S(2)}) copy-start(f32[1024]{0:T(1024)} %param.14) | copy-start | bytes 12292
  162.4 1.3 collective-permute-start.8
  166.0 2.2 %collective-permute-start.9 = (bf16[256,1024]{1,0:T(8,128)(2,1)}, bf16[256,1024]{1,0:T(8,128)(2,1)S(1)}, u32[]{:S(2)}, u32[]{:S(2)}) collective-permute-start(bf16[256,1024]{1,0:T(8,128)(2,1)} %fusion.5.grad_hbm), channel_id=1, source_target_pairs={{0,1},{1,0},{2,3},{3,2},{4,5},{5,4},{6,7},{7,6},{8,9},{9,8},{10,11... | collective-permute-start | bytes 1572872 | tf_op jit(solution)/shard_map/ppermute | solution.py:38
  168.3 14.1 %copy-start.6 = (bf16[256,1024]{1,0:T(8,128)(2,1)}, bf16[256,1024]{1,0:T(8,128)(2,1)S(1)}, u32[]{:S(2)}) copy-start(bf16[256,1024]{1,0:T(8,128)(2,1)S(1)} %collective-permute-done.9.peer_hbm) | copy-start | bytes 1572868
  182.3 1.9 collective-permute-start.10
  185.7 23.7 %all-to-all-start.3 = ((f32[16,32,512]{2,1,0:T(8,128)}), f32[16,32,512]{2,1,0:T(8,128)S(1)}, u32[]{:S(2)}, u32[]{:S(2)}) async-start(f32[16,32,512]{2,1,0:T(8,128)} %bitcast.29), calls=%async_computation.3 | async-start | bytes 2097152 | tf_op jit(solution)/shard_map/all_to_all | solution.py:42
  191.7 14.7 %copy-start.8 = (bf16[256,512]{1,0:T(8,128)(2,1)S(1)}, bf16[256,512]{1,0:T(8,128)(2,1)}, u32[]{:S(2)}) copy-start(bf16[256,512]{1,0:T(8,128)(2,1)} %param.18) | copy-start | bytes 786436
  195.0 10.6 %collective-permute-start.11 = (f32[2,512]{1,0:T(2,128)S(1)}, f32[2,512]{1,0:T(2,128)S(1)}, u32[]{:S(2)}, u32[]{:S(2)}) collective-permute-start(f32[2,512]{1,0:T(2,128)S(1)} %slice.74), channel_id=1, source_target_pairs={{2,0},{4,2},{6,4},{8,6},{10,8},{12,10},{14,12},{16,14},{18,16},{20... | collective-permute-start | bytes 12296 | tf_op jit(solution)/shard_map/ppermute | solution.py:48
  197.0 11.0 %copy-start.10 = (bf16[256,512]{1,0:T(8,128)(2,1)S(1)}, bf16[256,512]{1,0:T(8,128)(2,1)}, u32[]{:S(2)}) copy-start(bf16[256,512]{1,0:T(8,128)(2,1)} %param.20) | copy-start | bytes 786436
  (4 other events, 16.7 us)

commit v5 on v4

--- a/solution.py
+++ b/solution.py
@@ -118,7 +118,7 @@
 
 def build_rows(target, weights, own_squares, peer_squares, stream, cot, gain, slots):
     tokens, width = stream.shape
-    steps = 4
+    steps = 2
     rows = slots // steps
 
     def whole(*shape):
@@ -197,20 +197,20 @@
 ):
     rows, double = peer_ref.shape
     width = double // 2
-    half = rows // 2
+    at = pl.ds(start, rows)
     copies = []
     for i in range(2):
-        source = peer_hbm.at[pl.ds(start + i * half, half), :]
+        part = pl.ds(i * width, width)
         copies.append(
-            pltpu.make_async_copy(source, peer_ref.at[pl.ds(i * half, half), :], sems.at[i])
+            pltpu.make_async_copy(peer_hbm.at[at, part], peer_ref.at[:, part], sems.at[i])
         )
         copies[i].start()
-    for copy in copies:
-        copy.wait()
-    at = pl.ds(start, rows)
-    x, y = peer_ref[:, :width], peer_ref[:, width:]
+    copies[0].wait()
+    x = peer_ref[:, :width]
     gate_lin = gate_in[at, :] + dot_nn(x, gate_w[...])
     up_lin = up_in[at, :] + dot_nn(x, up_w[...])
+    copies[1].wait()
+    y = peer_ref[:, width:]
     hidden_grad = grad_in[at, :] + dot_nt(y, down_w[...])
     sig = jax.nn.sigmoid(gate_lin)
     silu = gate_lin * sig
@@ -316,7 +316,7 @@
 
 def add_parts(mine, other_a, other_b):
     rows, width = mine.shape
-    blocks = 8
+    blocks = 4
     return pl.pallas_call(
         add_body,
         in_specs=[IN_VMEM] * 3,
@@ -338,7 +338,7 @@
 
 def tick(array):
     return pl.pallas_call(
-        tick_body, out_shape=jax.ShapeDtypeStruct(array.shape, array.dtype), name="tick"
+        tick_body, out_shape=jax.ShapeDtypeStruct(array.shape, array.dtype), name="carry"
     )(array)
 
 
@@ -347,14 +347,41 @@
 
 
 def product_more_body(left_ref, right_ref, part_ref, out_ref):
-    out_ref[...] = part_ref[...] + dot_tn(left_ref[...], right_ref[...])
+    out_ref[...] = (part_ref[...] + dot_tn(left_ref[...], right_ref[...])).astype(BF16)
 
 
 def product(left, right, *part):
     body = product_more_body if part else product_body
-    outs = [((left.shape[1], right.shape[1]), F32)]
+    outs = [((left.shape[1], right.shape[1]), BF16 if part else F32)]
     flops = 2 * left.size * right.shape[1]
     return on_chip(body, outs, flops, 8, left, right, *part)[0]
+
+
+def conv_body(
+    delta_ref, rim_ref, taps_ref, gate_ref, input_ref, input_grad_ref, gate_grad_ref
+):
+    delta = delta_ref[...]
+    rows = delta.shape[0]
+    row = lax.broadcasted_iota(jnp.int32, delta.shape, 0)
+    first, second = rim_ref[0:1, :], rim_ref[1:2, :]
+    next_one = jnp.where(row == rows - 1, first, pltpu.roll(delta, rows - 1, 0))
+    next_two = jnp.where(row == rows - 2, first, pltpu.roll(delta, rows - 2, 0))
+    next_two = jnp.where(row == rows - 1, second, next_two)
+    grad = taps_ref[2:3, :] * delta + taps_ref[1:2, :] * next_one + taps_ref[0:1, :] * next_two
+    input_grad_ref[...] = (grad * gate_ref[...].astype(F32)).astype(BF16)
+    gate_grad_ref[...] = (grad * input_ref[...].astype(F32)).astype(BF16)
+
+
+def conv_back(delta, rim, taps, gate, inputs):
+    return pl.pallas_call(
+        conv_body,
+        in_specs=[IN_VMEM] * 5,
+        out_specs=[IN_VMEM] * 2,
+        out_shape=[jax.ShapeDtypeStruct(delta.shape, BF16)] * 2,
+        compiler_params=pltpu.CompilerParams(vmem_limit_bytes=12 * 1024 * 1024),
+        name="conv_back",
+        cost_estimate=cost(12 * delta.size, 12 * delta.size),
+    )(delta, rim, taps, gate, inputs)
 
 
 def mixer_body(
@@ -573,21 +600,14 @@
     grads_mine = exchange(sent, "sp_0").reshape(line * token_half, quarter)
     delta, bgate_grad = mixer_back(core_arg, stream_grad, grad_peer, out_proj, conv_bgate, conv_out)
     next_rim = shifted(delta[:2], SP, -1)
-    last_rows = tick(delta[-8:])
+    late_taps = tick(conv_taps)
     grads_theirs = swap(grads_mine)
     proj_part = product(grads_theirs, mixers_theirs, product(grads_mine, mixers_mine))
     plane = lax.axis_size(("sp_1", "sp_2"))
     arrived = exchange(proj_part.reshape(plane, quarter // plane, channels), ("sp_1", "sp_2"))
-    proj_grad = arrived.sum(axis=0)
-
-    extended_back = jnp.concatenate([delta[:-8], last_rows, next_rim], axis=0)
-    gated_grad = (
-        conv_taps[2][None, :] * extended_back[:-2]
-        + conv_taps[1][None, :] * extended_back[1:-1]
-        + conv_taps[0][None, :] * extended_back[2:]
-    )
-    input_grad = (gated_grad * cgate_float).astype(BF16)
-    cgate_grad = (gated_grad * input_float).astype(BF16)
+    proj_grad = arrived.astype(F32).sum(axis=0)
+
+    input_grad, cgate_grad = conv_back(delta, next_rim, late_taps, conv_cgate, conv_input)
     return (
         stream_grad,
         proj_grad,

time: 211 us -> 207 us (0.981); the launches traced: 210 us -> 203 us
  other arithmetic: 8.01 us -> 3.3 us
  waiting for transfers between devices: 46.9 us -> 43 us
    ppermute x2, waiting for transfers between devices: 7.25 us -> 2.9 us  [shifted(): lax.ppermute(value, axis, [(source, source + steps) for source in range(l...]
    convert_element_type x2 -> x0, other arithmetic: 2.4 us -> none  [the longest x1 1.63 us: stage(): cgate_grad = (gated_grad * input_float).astype(BF16)]
  transfers between devices with their start and end apart: 14 -> 14, of which waited for: 9 -> 9; matrix products, arithmetic and copies ran while one was open for 2% -> 0% of each run, Pallas kernels for 17% -> 18%
where the time goes in v5:
time: 207 us; the launch traced here: 203 us
  blocking collectives  77.2 us (37%)
  Pallas kernels  48.7 us (24%)
  waiting for transfers between devices  43 us (21%)
  starting transfers between devices  24.1 us (12%)
  matrix products  3.33 us (2%)
  other arithmetic  3.3 us (2%)
  local copies, waits for them, and re-layouts  2.19 us (1%)
    all_to_all x2, blocking collectives, exchange(): return lax.all_to_all(value, axis, split_axis=0, concat_axis=0, tiled=True)  77.2 us
    ppermute x3, waiting for transfers between devices, turned(): lax.ppermute(value, axis, [(i, (i + steps) % count) for i in range(count)])  32.9 us
    pallas_call x1, Pallas kernels, weight_grads(): pl.pallas_call(weights_body, grid_spec=pltpu.PrefetchScalarGridSpec(num_s...  14.6 us
    all_to_all x2, starting transfers between devices, exchange(): return lax.all_to_all(value, axis, split_axis=0, concat_axis=0, tiled=True)  14.6 us
    pallas_call x2, Pallas kernels, expert_peer(): pl.pallas_call(body, in_specs=[IN_HBM] + [IN_VMEM] * 6, out_specs=[IN_HBM...  9.38 us
    pallas_call x1, Pallas kernels, expert_own(): pl.pallas_call(own_body, in_specs=[IN_SMEM] + [IN_HBM] * 4, out_specs=[IN...  5.95 us
    ppermute x7, waiting for transfers between devices, swap(): return lax.ppermute(value, 'tp', [(0, 1), (1, 0)])  5.89 us
    ppermute x3, starting transfers between devices, turned(): lax.ppermute(value, axis, [(i, (i + steps) % count) for i in range(count)])  4.59 us
  transfers between devices with their start and end apart: 14, of which 9 were waited for; matrix products, arithmetic and copies ran while one was open for 0% of the time, Pallas kernels for 18%

profile of v5, /device:TPU:0, one launch (start us, length us, event | category | flops | bytes accessed | tf_op | source)
XLA Modules:
  0.0 202.8 jit_solution(3139157830313166859)
XLA Ops:
  0.6 2.1 %find_slots.1 = (f32[1,256]{1,0:T(1,128)}, s32[2,256]{1,0:T(2,128)}) custom-call(bf16[256,1024]{1,0:T(8,128)(2,1)} %stream_ref.1, s32[2,256]{1,0:T(2,128)} %bitcast.57), custom_call_target="tpu_custom_call" | custom-call | flops 100000000 | bytes 524288 | tf_op jit(solution)/shard_map/find_slots/pallas_call | solution.py:85
  4.6 4.2 %build_rows.1 = (bf16[1024,2048]{1,0:T(8,128)(2,1)}, bf16[1024,256]{1,0:T(8,128)(2,1)}, f32[1,256]{1,0:T(1,128)}) custom-call(s32[2,256]{1,0:T(2,128)} %get-tuple-element.42.target_ref, f32[2,256]{1,0:T(2,128)} %bitcast.61, f32[1,256]{1,0:T(1,128)} %get-tuple-element.43.own_ref, f32[1,256]{1,0:T(1,128)} %copy-done.14, bf16[256,1024]{1,0:T(8,128)(2,1)} %stream_ref.1, ...), custom_call_target="tpu_custom_call" | custom-call | flops 1073741824 | bytes 4194304 | tf_op jit(solution)/shard_map/build_rows/pallas_call | solution.py:127
  8.9 64.5 %all_to_all.20 = bf16[64,16,2048]{2,1,0:T(8,128)(2,1)} all-to-all(bf16[64,16,2048]{2,1,0:T(8,128)(2,1)} %bitcast.47), channel_id=1, replica_groups=mesh['sp_0'=4,'sp_1'=4,'sp_2'=4,'tp'=2] {'sp_0','sp_1','sp_2'}, dimensions={0} | all-to-all | bytes 8388608 | tf_op jit(solution)/shard_map/all_to_all | solution.py:42
  73.4 6.0 %expert_own.1 = (f32[1024,512]{1,0:T(8,128)S(1)}, f32[1024,512]{1,0:T(8,128)S(1)}, f32[1024,512]{1,0:T(8,128)S(1)}, bf16[1024,512]{1,0:T(8,128)(2,1)S(1)}, bf16[...) custom-call(s32[1]{0:T(128)} %bitcast.6.core_ref, ...), custom_call_target="tpu_custom_call" | custom-call | flops 3221225472 | bytes 10485760 | tf_op jit(solution)/shard_map/expert_own/pallas_call | solution.py:270
  79.3 1.5 collective-permute-done.1.refs_0_.peer_x.peer_y
  80.9 4.5 %expert_peer.2 = (bf16[512,512]{1,0:T(8,128)(2,1)}, bf16[512,512]{1,0:T(8,128)(2,1)S(1)}, bf16[512,512]{1,0:T(8,128)(2,1)S(1)}, bf16[512,1024]{1,0:T(8,128)(2,1)S(1)}) custom-call(bf16[1024,2048]{1,0:T(8,128)(2,1)} %collective-permute-done.1.refs_0_.peer_x.peer_y, bf16[1024,512]{1,0:T(8,128)(2,1)S(1)} %get-tuple-element.47.refs_1_, ...), custom_call_target="tpu_custom_call" | custom-call | flops 2684354560 | bytes 8388608 | tf_op jit(solution)/shard_map/expert_peer/pallas_call | solution.py:294
  85.7 4.8 %expert_peer.3 = (bf16[512,512]{1,0:T(8,128)(2,1)}, bf16[512,512]{1,0:T(8,128)(2,1)S(1)}, bf16[512,512]{1,0:T(8,128)(2,1)S(1)}, bf16[512,1024]{1,0:T(8,128)(2,1)S(1)}) custom-call(bf16[1024,2048]{1,0:T(8,128)(2,1)} %collective-permute-done.1.refs_0_.peer_x.peer_y, bf16[1024,512]{1,0:T(8,128)(2,1)S(1)} %get-tuple-element.47.refs_1_, ...), custom_call_target="tpu_custom_call" | custom-call | flops 2684354560 | bytes 8388608 | tf_op jit(solution)/shard_map/expert_peer/pallas_call | solution.py:294
  90.8 2.6 %collective-permute-start.4 = (bf16[2,2,512]{2,1,0:T(2,128)(2,1)S(1)}, bf16[2,2,512]{2,1,0:T(2,128)(2,1)S(1)}, u32[]{:S(2)}, u32[]{:S(2)}) collective-permute-start(bf16[2,2,512]{2,1,0:T(2,128)(2,1)S(1)} %pad_maximum_fusion.4), channel_id=1, source_target_pairs={{0,2},{2,4},{4,6},{6,8},{8,10},{10,12},{12,14},{14,16},{16,18},{18... | collective-permute-start | bytes 12296 | tf_op jit(solution)/shard_map/ppermute | solution.py:48
  93.5 2.4 %shard_map.188.mine_ref = bf16[1024,1024]{1,0:T(8,128)(2,1)S(1)} custom-call(bf16[512,512]{1,0:T(8,128)(2,1)S(1)} %get-tuple-element.53.gate_a, bf16[512,512]{1,0:T(8,128)(2,1)S(1)} %get-tuple-element.54.gate_b, bf16[512,512]{1,0:T(8,128)(2,1)S(1)} %get-tuple-element.55.up_a, bf16[512,512]{1,0:T(8,128)(2,1)S(1)} %get-tuple-element.56.up_b, ...), custom_call_target="tpu_custom_call" | custom-call | flops 2147483648 | bytes 16777216 | tf_op jit(solution)/shard_map/pallas_call | solution.py:255
  95.9 1.5 add_parts.1
  97.5 8.6 %all-to-all-start.1 = ((bf16[64,16,1024]{2,1,0:T(8,128)(2,1)}), bf16[64,16,1024]{2,1,0:T(8,128)(2,1)}, u32[]{:S(2)}, u32[]{:S(2)}) async-start(bf16[64,16,1024]{2,1,0:T(8,128)(2,1)} %bitcast.46), calls=%async_computation.1 | async-start | bytes 4194304 | tf_op jit(solution)/shard_map/all_to_all | solution.py:42
  106.4 3.0 %collective-permute-start.7 = (bf16[256,512]{1,0:T(8,128)(2,1)S(1)}, bf16[256,512]{1,0:T(8,128)(2,1)S(1)}, u32[]{:S(2)}, u32[]{:S(2)}) collective-permute-start(bf16[256,512]{1,0:T(8,128)(2,1)S(1)} %get-tuple-element.76), channel_id=1, source_target_pairs={{0,96},{32,0},{64,32},{96,64},{1,97},{33,1},{65,33},{97,65},{2,98}... | collective-permute-start | bytes 786440 | tf_op jit(solution)/shard_map/ppermute | solution.py:53
  111.0 25.9 %collective-permute-done.7 = bf16[256,512]{1,0:T(8,128)(2,1)S(1)} collective-permute-done((bf16[256,512]{1,0:T(8,128)(2,1)S(1)}, bf16[256,512]{1,0:T(8,128)(2,1)S(1)}, u32[]{:S(2)}, u32[]{:S(2)}) %collective-permute-start.7) | collective-permute-done | bytes 262176 | tf_op jit(solution)/shard_map/ppermute | solution.py:53
  136.8 1.9 collective-permute-done.6
  138.7 5.1 %collective-permute-done.5 = bf16[256,512]{1,0:T(8,128)(2,1)S(1)} collective-permute-done((bf16[256,512]{1,0:T(8,128)(2,1)S(1)}, bf16[256,512]{1,0:T(8,128)(2,1)S(1)}, u32[]{:S(2)}, u32[]{:S(2)}) %collective-permute-start.5) | collective-permute-done | bytes 262176 | tf_op jit(solution)/shard_map/ppermute | solution.py:53
  144.3 14.6 %weight_grads.1 = (f32[2048,512]{1,0:T(8,128)}, f32[2048,512]{1,0:T(8,128)}, f32[512,2048]{1,0:T(8,128)}) custom-call(s32[1]{0:T(128)} %bitcast.6.core_ref, bf16[1024,2048]{1,0:T(8,128)(2,1)} %bitcast.5.own_hbm.own_x.own_y, bf16[1024,2048]{1,0:T(8,128)(2,1)} %bitcast.5.own_hbm.own_x.own_y, bf16[1024,2048]{1,0:T(8,128)(2,1)} %collective-permute-done.1.refs_0_.peer_x.peer_y, ...), custom_call_target="tpu_custom_call" | custom-call | flops 6442450944 | bytes 12582912 | tf_op jit(solution)/shard_map/weight_grads/pallas_call | solution.py:481
  158.9 3.3 %fusion.7 = (f32[256]{0:T(256)S(1)}, f32[256,1024]{1,0:T(8,128)}) fusion(bf16[256,1024]{1,0:T(8,128)(2,1)S(1)} %copy-done.8, f32[1024]{0:T(1024)S(1)} %copy-done.12, bf16[1024,256]{1,0:T(8,128)(2,1)S(1)} %copy-done.11, bf16[1024,1024]{1,0:T(8,128)(2,1)} %bitcast.11), kind=kOutput, calls=%fused_computation.9 | convolution fusion | flops 537919232 | bytes 4199424 | tf_op jit(solution)/shard_map/dot_general | solution.py:30
  163.5 1.8 fusion.5.grad_hbm
  165.9 1.5 collective-permute-done.9.peer_hbm
  168.4 12.7 %all_to_all.21 = bf16[4,128,512]{2,1,0:T(8,128)(2,1)S(1)} all-to-all(bf16[4,128,512]{2,1,0:T(8,128)(2,1)S(1)} %pad_maximum_fusion.3), channel_id=1, replica_groups=mesh['sp_0'=4,'sp_1'=4,'sp_2'=4,'tp'=2] {'sp_0'}, dimensions={0} | all-to-all | bytes 1048576 | tf_op jit(solution)/shard_map/all_to_all | solution.py:42
  181.6 1.4 collective-permute-done.10.left_ref
  184.3 6.0 %all-to-all-start.3 = ((bf16[16,32,512]{2,1,0:T(8,128)(2,1)}), bf16[16,32,512]{2,1,0:T(8,128)(2,1)S(1)}, u32[]{:S(2)}, u32[]{:S(2)}) async-start(bf16[16,32,512]{2,1,0:T(8,128)(2,1)} %bitcast.29), calls=%async_computation.3 | async-start | bytes 1048576 | tf_op jit(solution)/shard_map/all_to_all | solution.py:42
  190.2 3.3 %mixer_back.1 = (f32[256,512]{1,0:T(8,128)S(1)}, bf16[256,512]{1,0:T(8,128)(2,1)}) custom-call(s32[1]{0:T(128)} %bitcast.6.core_ref, bf16[256,1024]{1,0:T(8,128)(2,1)} %copy-done.9, bf16[256,1024]{1,0:T(8,128)(2,1)} %copy-done.10, bf16[2048,512]{1,0:T(8,128)(2,1)} %proj_hbm.1, bf16[256,512]{1,0:T(8,128)(2,1)S(1)} %copy-done.2, ...), custom_call_target="tpu_custom_call" | custom-call | flops 536870912 | bytes 8388608 | tf_op jit(solution)/shard_map/mixer_back/pallas_call | solution.py:416
  196.1 2.9 %collective-permute-done.11.rim_ref = f32[2,512]{1,0:T(2,128)S(1)} collective-permute-done((f32[2,512]{1,0:T(2,128)S(1)}, f32[2,512]{1,0:T(2,128)S(1)}, u32[]{:S(2)}, u32[]{:S(2)}) %collective-permute-start.11) | collective-permute-done | bytes 4128 | tf_op jit(solution)/shard_map/ppermute | solution.py:48
  (69 shorter events, 15.5 us)
Async XLA Ops:
  2.7 1.4 collective-permute-start
  73.4 7.5 %collective-permute-start.1 = (bf16[1024,2048]{1,0:T(8,128)(2,1)}, bf16[1024,2048]{1,0:T(8,128)(2,1)}, u32[]{:S(2)}, u32[]{:S(2)}) collective-permute-start(bf16[1024,2048]{1,0:T(8,128)(2,1)} %bitcast.5.own_hbm.own_x.own_y), channel_id=1, source_target_pairs={{0,1},{1,0},{2,3},{3,2},{4,5},{5,4},{6,7},{7,6},{8,9},{9,8},{10,11... | collective-permute-start | bytes 12582920 | tf_op jit(solution)/shard_map/ppermute | solution.py:38
  85.4 8.0 %copy-start.4 = (bf16[512,512]{1,0:T(8,128)(2,1)}, bf16[512,512]{1,0:T(8,128)(2,1)S(1)}, u32[]{:S(2)}) copy-start(bf16[512,512]{1,0:T(8,128)(2,1)S(1)} %get-tuple-element.53.gate_a) | copy-start | bytes 1572868
  85.4 8.0 %copy-start.5 = (bf16[512,512]{1,0:T(8,128)(2,1)}, bf16[512,512]{1,0:T(8,128)(2,1)S(1)}, u32[]{:S(2)}) copy-start(bf16[512,512]{1,0:T(8,128)(2,1)S(1)} %get-tuple-element.55.up_a) | copy-start | bytes 1572868
  85.5 10.4 %collective-permute-start.2 = (bf16[512,1024]{1,0:T(8,128)(2,1)S(1)}, bf16[512,1024]{1,0:T(8,128)(2,1)S(1)}, u32[]{:S(2)}, u32[]{:S(2)}) collective-permute-start(bf16[512,1024]{1,0:T(8,128)(2,1)S(1)} %get-tuple-element.59), channel_id=1, source_target_pairs={{0,1},{1,0},{2,3},{3,2},{4,5},{5,4},{6,7},{7,6},{8,9},{9,8},{10,11... | collective-permute-start | bytes 3145736 | tf_op jit(solution)/shard_map/ppermute | solution.py:38
  90.5 5.3 %copy-start.6 = (bf16[512,512]{1,0:T(8,128)(2,1)}, bf16[512,512]{1,0:T(8,128)(2,1)S(1)}, u32[]{:S(2)}) copy-start(bf16[512,512]{1,0:T(8,128)(2,1)S(1)} %get-tuple-element.54.gate_b) | copy-start | bytes 1572868
  90.5 5.3 %copy-start.7 = (bf16[512,512]{1,0:T(8,128)(2,1)}, bf16[512,512]{1,0:T(8,128)(2,1)S(1)}, u32[]{:S(2)}) copy-start(bf16[512,512]{1,0:T(8,128)(2,1)S(1)} %get-tuple-element.56.up_b) | copy-start | bytes 1572868
  90.5 5.3 %collective-permute-start.3 = (bf16[512,1024]{1,0:T(8,128)(2,1)S(1)}, bf16[512,1024]{1,0:T(8,128)(2,1)S(1)}, u32[]{:S(2)}, u32[]{:S(2)}) collective-permute-start(bf16[512,1024]{1,0:T(8,128)(2,1)S(1)} %get-tuple-element.60), channel_id=1, source_target_pairs={{0,1},{1,0},{2,3},{3,2},{4,5},{5,4},{6,7},{7,6},{8,9},{9,8},{10,11... | collective-permute-start | bytes 3145736 | tf_op jit(solution)/shard_map/ppermute | solution.py:38
  90.8 15.3 %collective-permute-start.4 = (bf16[2,2,512]{2,1,0:T(2,128)(2,1)S(1)}, bf16[2,2,512]{2,1,0:T(2,128)(2,1)S(1)}, u32[]{:S(2)}, u32[]{:S(2)}) collective-permute-start(bf16[2,2,512]{2,1,0:T(2,128)(2,1)S(1)} %pad_maximum_fusion.4), channel_id=1, source_target_pairs={{0,2},{2,4},{4,6},{6,8},{8,10},{10,12},{12,14},{14,16},{16,18},{18... | collective-permute-start | bytes 12296 | tf_op jit(solution)/shard_map/ppermute | solution.py:48
  97.4 8.6 %copy-start.13 = (f32[3,512]{1,0:T(4,128)S(1)}, f32[3,512]{1,0:T(4,128)}, u32[]{:S(2)}) copy-start(f32[3,512]{1,0:T(4,128)} %in_ref.1) | copy-start | bytes 18436
  97.5 8.7 %copy-start.2 = (bf16[256,512]{1,0:T(8,128)(2,1)S(1)}, bf16[256,512]{1,0:T(8,128)(2,1)}, u32[]{:S(2)}) copy-start(bf16[256,512]{1,0:T(8,128)(2,1)} %gate_ref.2) | copy-start | bytes 786436
  97.5 61.4 %all-to-all-start.1 = ((bf16[64,16,1024]{2,1,0:T(8,128)(2,1)}), bf16[64,16,1024]{2,1,0:T(8,128)(2,1)}, u32[]{:S(2)}, u32[]{:S(2)}) async-start(bf16[64,16,1024]{2,1,0:T(8,128)(2,1)} %bitcast.46), calls=%async_computation.1 | async-start | bytes 4194304 | tf_op jit(solution)/shard_map/all_to_all | solution.py:42
  106.4 30.5 %collective-permute-start.7 = (bf16[256,512]{1,0:T(8,128)(2,1)S(1)}, bf16[256,512]{1,0:T(8,128)(2,1)S(1)}, u32[]{:S(2)}, u32[]{:S(2)}) collective-permute-start(bf16[256,512]{1,0:T(8,128)(2,1)S(1)} %get-tuple-element.76), channel_id=1, source_target_pairs={{0,96},{32,0},{64,32},{96,64},{1,97},{33,1},{65,33},{97,65},{2,98}... | collective-permute-start | bytes 786440 | tf_op jit(solution)/shard_map/ppermute | solution.py:53
  109.3 29.4 %collective-permute-start.6 = (bf16[256,512]{1,0:T(8,128)(2,1)S(1)}, bf16[256,512]{1,0:T(8,128)(2,1)S(1)}, u32[]{:S(2)}, u32[]{:S(2)}) collective-permute-start(bf16[256,512]{1,0:T(8,128)(2,1)S(1)} %get-tuple-element.76), channel_id=1, source_target_pairs={{0,64},{32,96},{64,0},{96,32},{1,65},{33,97},{65,1},{97,33},{2,66}... | collective-permute-start | bytes 786440 | tf_op jit(solution)/shard_map/ppermute | solution.py:53
  110.0 33.8 %collective-permute-start.5 = (bf16[256,512]{1,0:T(8,128)(2,1)S(1)}, bf16[256,512]{1,0:T(8,128)(2,1)S(1)}, u32[]{:S(2)}, u32[]{:S(2)}) collective-permute-start(bf16[256,512]{1,0:T(8,128)(2,1)S(1)} %get-tuple-element.76), channel_id=1, source_target_pairs={{0,32},{32,64},{64,96},{96,0},{1,33},{33,65},{65,97},{97,1},{2,34}... | collective-permute-start | bytes 786440 | tf_op jit(solution)/shard_map/ppermute | solution.py:53
  144.3 14.6 %copy-start.8 = (bf16[256,1024]{1,0:T(8,128)(2,1)S(1)}, bf16[256,1024]{1,0:T(8,128)(2,1)}, u32[]{:S(2)}) copy-start(bf16[256,1024]{1,0:T(8,128)(2,1)} %stream_ref.1) | copy-start | bytes 1572868
  144.3 14.6 %copy-start.11 = (bf16[1024,256]{1,0:T(8,128)(2,1)S(1)}, bf16[1024,256]{1,0:T(8,128)(2,1)}, u32[]{:S(2)}) copy-start(bf16[1024,256]{1,0:T(8,128)(2,1)} %get-tuple-element.45) | copy-start | bytes 1572868
  144.3 14.6 %copy-start.12 = (f32[1024]{0:T(1024)S(1)}, f32[1024]{0:T(1024)}, u32[]{:S(2)}) copy-start(f32[1024]{0:T(1024)} %param.14) | copy-start | bytes 12292
  162.2 1.2 collective-permute-start.8
  165.3 15.7 %copy-start.9 = (bf16[256,1024]{1,0:T(8,128)(2,1)}, bf16[256,1024]{1,0:T(8,128)(2,1)S(1)}, u32[]{:S(2)}) copy-start(bf16[256,1024]{1,0:T(8,128)(2,1)S(1)} %fusion.5.grad_hbm) | copy-start | bytes 1572868
  165.4 2.1 %collective-permute-start.9 = (bf16[256,1024]{1,0:T(8,128)(2,1)S(1)}, bf16[256,1024]{1,0:T(8,128)(2,1)S(1)}, u32[]{:S(2)}, u32[]{:S(2)}) collective-permute-start(bf16[256,1024]{1,0:T(8,128)(2,1)S(1)} %fusion.5.grad_hbm), channel_id=1, source_target_pairs={{0,1},{1,0},{2,3},{3,2},{4,5},{5,4},{6,7},{7,6},{8,9},{9,8},{10,11... | collective-permute-start | bytes 1572872 | tf_op jit(solution)/shard_map/ppermute | solution.py:38
  181.1 1.9 collective-permute-start.10
  184.3 17.8 %all-to-all-start.3 = ((bf16[16,32,512]{2,1,0:T(8,128)(2,1)}), bf16[16,32,512]{2,1,0:T(8,128)(2,1)S(1)}, u32[]{:S(2)}, u32[]{:S(2)}) async-start(bf16[16,32,512]{2,1,0:T(8,128)(2,1)} %bitcast.29), calls=%async_computation.3 | async-start | bytes 1048576 | tf_op jit(solution)/shard_map/all_to_all | solution.py:42
  193.5 5.5 %collective-permute-start.11 = (f32[2,512]{1,0:T(2,128)S(1)}, f32[2,512]{1,0:T(2,128)S(1)}, u32[]{:S(2)}, u32[]{:S(2)}) collective-permute-start(f32[2,512]{1,0:T(2,128)S(1)} %slice.55), channel_id=1, source_target_pairs={{2,0},{4,2},{6,4},{8,6},{10,8},{12,10},{14,12},{16,14},{18,16},{20... | collective-permute-start | bytes 12296 | tf_op jit(solution)/shard_map/ppermute | solution.py:48
  (5 other events, 12.7 us)
